TPU v7x, 512 devices: a whole 4x8x8 slice. The times are simulated.
512 devices in a mesh: sp: 32 (over z, x), tp: 16 (over y, core).
Axes of the slice: x: 4, y: 8, z: 8, core: 2. Of those that a mesh axis runs over, the one named last changes fastest.
Arguments:
- cotangent: bfloat16 [4096, 2048], P('sp'), may hold values from -6 to 6
- stream: bfloat16 [4096, 2048], P('sp'), may hold values from -6 to 6
- routes: int32 [4096, 2], P('sp'), may hold values from 0 to 15, all different within a row; in each aligned block of 128 rows (0 to 127, 128 to 255, ...) at most 24 rows name the same one
- route_weights: float32 [4096, 2], P('sp'), may hold values from 0.25 to 1
- gate_weight: bfloat16 [32, 2048, 2048], P('sp', None, 'tp'), may hold values from -0.125 to 0.125
- up_weight: bfloat16 [32, 2048, 2048], P('sp', None, 'tp'), may hold values from -0.125 to 0.125
- down_weight: bfloat16 [32, 2048, 2048], P('sp', 'tp'), may hold values from -0.09375 to 0.09375
- outer_gate: bfloat16 [4096, 1024], P('sp', 'tp'), may hold values from -6 to 6
- inner_gate: bfloat16 [4096, 1024], P('sp', 'tp'), may hold values from -6 to 6
- conv_input: bfloat16 [4096, 1024], P('sp', 'tp'), may hold values from -6 to 6
- conv_taps: bfloat16 [3, 1024], P(None, 'tp'), may hold values from -1 to 1
- out_weight: bfloat16 [2048, 1024], P(None, 'tp'), may hold values from -0.1875 to 0.1875
Outputs:
- gate_grad: bfloat16 [32, 2048, 2048], P('sp', None, 'tp')
- up_grad: bfloat16 [32, 2048, 2048], P('sp', None, 'tp')
- down_grad: bfloat16 [32, 2048, 2048], P('sp', 'tp')
- out_grad: float32 [2048, 1024], P('sp', 'tp')
- outer_grad: bfloat16 [4096, 1024], P('sp', 'tp')
- inner_grad: bfloat16 [4096, 1024], P('sp', 'tp')
- input_grad: bfloat16 [4096, 1024], P('sp', 'tp')
Inputs may be any that keep to these rules, and one draw needn't show every extreme that they name: `routes`: each token names two different experts. Among the 128 tokens of one index of sp no expert is named by more than 24 tokens, a bound that some block of them reaches in every draw.
All inputs are finite; a program needn't handle non-finite values.
Results may differ from a plain program's by a relative error of at most 0.02.
Values may be sent and summed in bfloat16 or wider, within the bound.
No kernel may reach another device: no remote copies, remote signals or barrier semaphores. Data moves between devices by JAX's collectives and lax.ppermute only.
A program may use at most 64 MiB of HBM per device.

v0:
```python
import jax
import jax.numpy as jnp
from jax import lax
from jax.sharding import PartitionSpec as P


def side_by_side(arrays, axis, split_dim, concat_dim, along):
    both = jnp.concatenate(arrays, axis=along)
    result, at, gathered = (
        lax.all_to_all(both, axis, split_axis=split_dim, concat_axis=concat_dim, tiled=True),
        0,
        [],
    )
    for a in arrays:
        gathered.append(lax.slice_in_dim(result, at, at + a.shape[along], axis=along))
        at += a.shape[along]
    return tuple(gathered)


def sent_together(arrays, axis, dim, along):
    widths = [a.shape[along] for a in arrays]
    both = jnp.concatenate(arrays, axis=along)
    result = lax.all_gather(both, axis, axis=dim, tiled=True)
    return tuple(jnp.split(result, [sum(widths[:k]) for k in range(1, len(widths))], axis=along))


def from_behind(block, axis, distance):
    devices = range(lax.axis_size(axis))
    route = [(i - distance, i) for i in devices if i - distance in devices]
    return lax.ppermute(block, axis, route)


def in_blocks(shard, dim, devices):
    before, after = (shard.shape[:dim], shard.shape[dim + 1 :])
    return jnp.moveaxis(shard.reshape(*before, devices, -1, *after), dim, 0)


def sent_and_summed(shard, axis, dim):
    tiles = in_blocks(shard, dim, lax.axis_size(axis))
    arrived = lax.all_to_all(tiles, axis, split_axis=0, concat_axis=0, tiled=True)
    return arrived.astype(jnp.float32).sum(axis=0)


def per_device(
    cotangent,
    stream,
    routes,
    route_weights,
    gate_weight,
    up_weight,
    down_weight,
    outer_gate,
    inner_gate,
    conv_input,
    conv_taps,
    out_weight,
):
    groups = lax.axis_size("sp")
    tp_count = lax.axis_size("tp")
    experts = groups // 2
    tok_rows = stream.shape[0]
    model_width = stream.shape[1]
    capacity = 3 * tok_rows // experts
    slot_total = experts * capacity
    contract_first = (((0,), (0,)), ((), ()))
    contract_last = (((1,), (1,)), ((), ()))
    flat_routes = routes.reshape(-1)
    choose = (flat_routes[:, None] == jnp.arange(experts, dtype=jnp.int32)[None, :]).astype(
        jnp.int32
    )
    before = jnp.cumsum(choose, axis=0) - choose
    slot_place = flat_routes * capacity + jnp.sum(before * choose, axis=1)
    slot_table = (jnp.arange(slot_total, dtype=jnp.int32)[:, None] == slot_place[None, :]).astype(
        jnp.float32
    )
    select = jnp.sum(slot_table.reshape(slot_total, tok_rows, 2), axis=2).astype(jnp.bfloat16)
    slot_weight = jnp.sum(slot_table * route_weights.reshape(-1)[None, :], axis=1)
    block_width = model_width // tp_count
    offset = lax.axis_index("tp") * block_width
    rows_part = lax.dynamic_slice_in_dim(stream, offset, block_width, 1)
    cot_part = lax.dynamic_slice_in_dim(cotangent, offset, block_width, 1)
    sent_rows = jnp.dot(select, rows_part, preferred_element_type=jnp.float32).astype(jnp.bfloat16)
    sent_cot = (
        jnp.dot(select, cot_part, preferred_element_type=jnp.float32) * slot_weight[:, None]
    ).astype(jnp.bfloat16)
    sent_rows = jnp.repeat(sent_rows.reshape(experts, capacity, -1), 2, axis=0)
    sent_cot = jnp.repeat(sent_cot.reshape(experts, capacity, -1), 2, axis=0)
    recv_rows, recv_cot = side_by_side((sent_rows, sent_cot), "sp", 0, 0, 1)
    recv_rows, recv_cot = sent_together((recv_rows, recv_cot), "tp", 2, 0)
    slots = groups * capacity
    routed_rows = recv_rows.reshape(slots, model_width)
    routed_cot = recv_cot.reshape(slots, model_width)
    gate_local = gate_weight[0]
    up_local = up_weight[0]
    down_local = down_weight[0]
    gate_pre = jnp.dot(routed_rows, gate_local, preferred_element_type=jnp.float32)
    up_pre = jnp.dot(routed_rows, up_local, preferred_element_type=jnp.float32)
    hidden_grad = lax.dot_general(
        routed_cot, down_local, contract_last, preferred_element_type=jnp.float32
    )
    sigma = jax.nn.sigmoid(gate_pre)
    silu_gate = gate_pre * sigma
    hidden = (silu_gate * up_pre).astype(jnp.bfloat16)
    up_delta = (hidden_grad * silu_gate).astype(jnp.bfloat16)
    gate_delta = (hidden_grad * up_pre * sigma * (1.0 + gate_pre * (1.0 - sigma))).astype(
        jnp.bfloat16
    )
    gate_grad = lax.dot_general(
        routed_rows, gate_delta, contract_first, preferred_element_type=jnp.float32
    ).astype(jnp.bfloat16)[None]
    up_grad = lax.dot_general(
        routed_rows, up_delta, contract_first, preferred_element_type=jnp.float32
    ).astype(jnp.bfloat16)[None]
    down_grad = lax.dot_general(
        hidden, routed_cot, contract_first, preferred_element_type=jnp.float32
    ).astype(jnp.bfloat16)[None]
    row_partial = lax.dot_general(
        gate_delta, gate_local, contract_last, preferred_element_type=jnp.float32
    )
    row_partial = row_partial + lax.dot_general(
        up_delta, up_local, contract_last, preferred_element_type=jnp.float32
    )
    half_sums = lax.psum_scatter(
        row_partial.astype(jnp.bfloat16), "tp", scatter_dimension=1, tiled=True
    ).astype(jnp.float32)
    block_width = half_sums.shape[1]
    half_grad = half_sums.reshape(groups, capacity, block_width).astype(jnp.bfloat16)
    returned = lax.all_to_all(half_grad, "sp", split_axis=0, concat_axis=0, tiled=True)
    returned = returned.reshape(experts, 2, capacity, block_width)
    select_three = select.reshape(experts, capacity, tok_rows)
    moe_part = jnp.einsum(
        "ecr,emcd->rd", select_three, returned, preferred_element_type=jnp.float32
    ).astype(jnp.bfloat16)
    moe_grad = lax.all_gather(moe_part, "tp", axis=1, tiled=True)
    stream_grad = (cotangent.astype(jnp.float32) + moe_grad.astype(jnp.float32)).astype(
        jnp.bfloat16
    )
    taps = conv_taps.astype(jnp.float32)
    outer_f = outer_gate.astype(jnp.float32)
    inner_f = inner_gate.astype(jnp.float32)
    input_f = conv_input.astype(jnp.float32)
    mixed = inner_f * input_f
    earlier = from_behind(mixed[-2:], "sp", 1)
    padded = jnp.concatenate([earlier, mixed], axis=0)
    conv_sum = taps[0] * padded[:-2] + taps[1] * padded[1:-1] + taps[2] * padded[2:]
    conv_out = (outer_f * conv_sum).astype(jnp.bfloat16)
    out_grad = sent_and_summed(
        lax.dot_general(
            stream_grad, conv_out, contract_first, preferred_element_type=jnp.float32
        ).astype(jnp.bfloat16),
        "sp",
        0,
    )
    conv_grad = jnp.dot(stream_grad, out_weight, preferred_element_type=jnp.float32)
    outer_grad = (conv_grad * conv_sum).astype(jnp.bfloat16)
    scaled = conv_grad * outer_f
    later = from_behind(scaled[:2], "sp", -1)
    extended = jnp.concatenate([scaled, later], axis=0)
    mixed_grad = taps[2] * extended[:-2] + taps[1] * extended[1:-1] + taps[0] * extended[2:]
    inner_grad = (mixed_grad * input_f).astype(jnp.bfloat16)
    input_grad = (mixed_grad * inner_f).astype(jnp.bfloat16)
    return (gate_grad, up_grad, down_grad, out_grad, outer_grad, inner_grad, input_grad)


def solution(mesh):
    placed = (
        P("sp", None),
        P("sp", None),
        P("sp", None),
        P("sp", None),
        P("sp", None, "tp"),
        P("sp", None, "tp"),
        P("sp", "tp", None),
        P("sp", "tp"),
        P("sp", "tp"),
        P("sp", "tp"),
        P(None, "tp"),
        P(None, "tp"),
    )
    return jax.shard_map(
        per_device,
        mesh=mesh,
        in_specs=placed,
        out_specs=(
            P("sp", None, "tp"),
            P("sp", None, "tp"),
            P("sp", "tp", None),
            P("sp", "tp"),
            P("sp", "tp"),
            P("sp", "tp"),
            P("sp", "tp"),
        ),
        check_vma=False,
    )
```

profile of v0, /device:TPU:6, one launch (start us, length us, event | category | flops | bytes accessed | tf_op | source)
XLA Modules:
  0.0 244.0 jit_solution(4913655211570042298)
XLA Ops:
  7.2 0.0 copy-start
  7.2 0.0 all-gather.2.cloned.1.call-start
  7.2 0.8 copy.45
  8.1 0.1 eq.46
  8.2 0.1 eq.50
  8.4 0.6 reduce-window.6
  8.9 0.2 slice_reduce_fusion
  9.2 0.1 fusion.35
  9.3 0.1 reduce_sum.48
  9.4 0.1 copy.48
  9.5 0.7 multiply_add_fusion.1
  10.2 0.1 convert_reduce_fusion.2
  10.3 0.8 copy.49
  11.0 0.1 mul.132
  11.2 0.1 select_reduce_fusion
  11.3 0.9 convolution_convert_fusion.4
  12.3 0.9 fusion.3
  13.3 27.2 %all_to_all.15 = bf16[32,48,128]{2,1,0:T(8,128)(2,1)S(1)} all-to-all(bf16[32,48,128]{2,1,0:T(8,128)(2,1)S(1)} %pad_maximum_fusion), channel_id=1, replica_groups=mesh['sp'=32,'tp'=16] {'sp'}, dimensions={0} | all-to-all | bytes 786432 | tf_op jit(solution)/shard_map/all_to_all | solution.py:10
  40.6 0.8 pad_maximum_fusion.1
  41.4 0.0 all-gather.2.cloned.1.call-update
  41.4 0.0 reduce-scatter.4.cloned.1.call-start
  41.4 56.3 %all-gather.2.cloned.1.call-done = bf16[64,24,2048]{2,1,0:T(8,128)(2,1)} async-done(((bf16[64,24,128]{2,1,0:T(8,128)(2,1)}), bf16[64,24,2048]{2,1,0:T(8,128)(2,1)}) %all-gather.2.cloned.1.call-update) | async-done | bytes 6291472 | tf_op jit(solution)/shard_map/all_gather | solution.py:23
  97.7 3.4 %fusion.42 = (bf16[32,24,2048]{2,1,0:T(8,128)(2,1)S(1)}, bf16[32,24,2048]{2,1,0:T(8,128)(2,1)S(1)}) fusion(bf16[64,24,2048]{2,1,0:T(8,128)(2,1)} %all-gather.2.cloned.1.call-done), kind=kLoop, calls=%fused_computation.81 | loop fusion | bytes 12582912 | tf_op jit(solution)/shard_map/split | solution.py:24
  101.2 0.0 copy-start.1
  101.2 0.0 copy-start.2
  101.2 0.0 copy-start.5
  101.2 1.0 fusion.7
  102.2 0.4 copy-done.5
  102.6 1.0 fusion.10
  103.6 0.2 copy-done.2
  103.8 0.2 copy-done.11
  104.0 1.0 multiply_convert_fusion.1
  105.0 1.0 fusion.5
  106.0 2.6 %add_convert_fusion = bf16[768,2048]{1,0:T(8,128)(2,1)} fusion(f32[768,2048]{1,0:T(8,128)S(1)} %fusion.5, bf16[768,128]{1,0:T(8,128)(2,1)S(1)} %get-tuple-element.34, bf16[1,2048,128]{2,1,0:T(8,128)(2,1)S(1)} %copy-done.5), kind=kOutput, calls=%fused_computation | convolution fusion | flops 405798912 | bytes 10158080 | tf_op jit(solution)/shard_map/dot_general | solution.py:120
  108.6 4.7 %copy.53 = bf16[768,2048]{0,1:T(8,128)(2,1)} copy(bf16[768,2048]{1,0:T(8,128)(2,1)} %add_convert_fusion) | data formatting | bytes 6291456
  113.4 0.0 reduce-scatter.4.cloned.1.call-update
  113.4 0.7 copy-done.8
  114.1 0.0 copy-done.9
  114.1 0.1 slice.58
  114.2 3.5 %collective-permute-start = (f32[2,64]{0,1:T(8,128)S(1)}, f32[2,64]{0,1:T(8,128)S(1)}, u32[]{:S(2)}, u32[]{:S(2)}) collective-permute-start(f32[2,64]{0,1:T(8,128)S(1)} %slice.58), channel_id=1, source_target_pairs={{0,16},{16,32},{32,48},{48,64},{64,80},{80,96},{96,112},{112,128},... | collective-permute-start | bytes 1544 | tf_op jit(solution)/shard_map/ppermute | solution.py:30
  117.7 59.1 %reduce-scatter.4.cloned.1.call-done = bf16[128,768]{1,0:T(8,128)(2,1)} async-done(((bf16[2048,768]{1,0:T(8,128)(2,1)}), bf16[128,768]{1,0:T(8,128)(2,1)}) %reduce-scatter.4.cloned.1.call-update) | async-done | bytes 196624
  176.9 1.7 copy.54
  178.6 10.5 %all-to-all-start.1 = ((bf16[32,24,128]{2,1,0:T(8,128)(2,1)}), bf16[32,24,128]{2,1,0:T(8,128)(2,1)S(1)}, u32[]{:S(2)}, u32[]{:S(2)}) async-start(bf16[32,24,128]{2,1,0:T(8,128)(2,1)} %bitcast.14), calls=%async_computation.1 | async-start | bytes 393216 | tf_op jit(solution)/shard_map/all_to_all | solution.py:128
  189.1 3.9 %fusion = bf16[1,2048,128]{2,1,0:T(8,128)(2,1)} fusion(bf16[768,2048]{1,0:T(8,128)(2,1)} %bitcast.88, bf16[768,128]{1,0:T(8,128)(2,1)S(1)} %get-tuple-element.35), kind=kOutput, calls=%fused_computation.4 | convolution fusion | flops 402915328 | bytes 3866624 | tf_op jit(solution)/shard_map/dot_general | solution.py:108
  193.0 1.4 fusion.2
  194.5 4.0 %all-to-all-done.1 = bf16[32,24,128]{2,1,0:T(8,128)(2,1)S(1)} async-done(((bf16[32,24,128]{2,1,0:T(8,128)(2,1)}), bf16[32,24,128]{2,1,0:T(8,128)(2,1)S(1)}, u32[]{:S(2)}, u32[]{:S(2)}) %all-to-all-start.1) | async-done | bytes 196640 | tf_op jit(solution)/shard_map/all_to_all | solution.py:128
  198.5 0.2 fusion.4
  198.7 16.9 %all_gather.7 = bf16[128,2048]{1,0:T(8,128)(2,1)S(1)} all-gather(bf16[128,128]{1,0:T(8,128)(2,1)S(1)} %fusion.4), channel_id=1, replica_groups=mesh['sp'=32,'tp'=16] {'tp'}, dimensions={1}, use_global_device_ids=true | all-gather | bytes 557056 | tf_op jit(solution)/shard_map/all_gather | solution.py:134
  215.6 0.0 collective-permute-done
  215.6 0.9 multiply_convert_fusion.4
  216.6 0.3 convolution_convert_fusion.3
  216.8 0.5 reshape.88
  217.4 0.2 copy.59
  217.6 1.1 reshape.94
  218.7 5.6 %all-to-all-start.2 = ((bf16[32,2,2048]{2,1,0:T(2,128)(2,1)}), bf16[32,2,2048]{2,1,0:T(2,128)(2,1)S(1)}, u32[]{:S(2)}, u32[]{:S(2)}) async-start(bf16[32,2,2048]{2,1,0:T(2,128)(2,1)} %reshape.94), calls=%async_computation.2 | async-start | bytes 524288 | tf_op jit(solution)/shard_map/all_to_all | solution.py:40
  224.2 2.8 %collective-permute-start.1 = (f32[2,64]{0,1:T(8,128)S(1)}, f32[2,64]{0,1:T(8,128)S(1)}, u32[]{:S(2)}, u32[]{:S(2)}) collective-permute-start(f32[2,64]{0,1:T(8,128)S(1)} %bitcast.100), channel_id=1, source_target_pairs={{16,0},{32,16},{48,32},{64,48},{80,64},{96,80},{112,96},{128,112},... | collective-permute-start | bytes 1544 | tf_op jit(solution)/shard_map/ppermute | solution.py:30
  227.0 3.7 %fusion.1 = bf16[1,2048,128]{2,1,0:T(8,128)(2,1)} fusion(bf16[768,2048]{1,0:T(8,128)(2,1)} %bitcast.89, bf16[768,128]{1,0:T(8,128)(2,1)S(1)} %get-tuple-element.34), kind=kOutput, calls=%fused_computation.5 | convolution fusion | flops 402915328 | bytes 3866624 | tf_op jit(solution)/shard_map/dot_general | solution.py:111
  230.7 2.2 collective-permute-done.1
  232.9 0.7 fusion.18
  233.7 0.6 fusion.19
  234.3 1.7 all-to-all-done.2
  236.0 0.4 reshape.95
  236.4 0.1 convert_reduce_fusion
  236.5 0.7 copy.52
  (27 shorter events, 0.3 us)
Async XLA Ops:
  7.2 94.0 %copy-start = (bf16[1,2048,128]{2,1,0:T(8,128)(2,1)S(1)}, bf16[1,2048,128]{2,1,0:T(8,128)(2,1)}, u32[]{:S(2)}) copy-start(bf16[1,2048,128]{2,1,0:T(8,128)(2,1)} %param.16) | copy-start | bytes 1572868
  7.2 90.5 %all-gather.2.cloned.1.call-start = ((), (), s32[]{:S(2)}) async-start(), calls=%async_computation.4 | async-start | bytes 6684672 | tf_op jit(solution)/shard_map/all_gather | solution.py:23
  41.4 135.5 %reduce-scatter.4.cloned.1.call-start = ((), (), s32[]{:S(2)}) async-start(), calls=%async_computation.5 | async-start | bytes 3342336
  101.2 2.4 %copy-start.1 = (bf16[32,24,2048]{2,1,0:T(8,128)(2,1)}, bf16[32,24,2048]{2,1,0:T(8,128)(2,1)S(1)}, u32[]{:S(2)}) copy-start(bf16[32,24,2048]{2,1,0:T(8,128)(2,1)S(1)} %get-tuple-element.33) | copy-start | bytes 9437188
  101.2 2.6 %copy-start.2 = (bf16[32,24,2048]{2,1,0:T(8,128)(2,1)}, bf16[32,24,2048]{2,1,0:T(8,128)(2,1)S(1)}, u32[]{:S(2)}) copy-start(bf16[32,24,2048]{2,1,0:T(8,128)(2,1)S(1)} %get-tuple-element.32) | copy-start | bytes 9437188
  101.2 1.4 copy-start.5
  102.6 1.4 copy-start.11
  113.4 0.7 copy-start.8
  113.4 0.7 copy-start.9
  113.4 4.4 %copy-start.10 = (bf16[3,64]{1,0:T(4,128)(2,1)S(1)}, bf16[3,64]{1,0:T(4,128)(2,1)}, u32[]{:S(2)}) copy-start(bf16[3,64]{1,0:T(4,128)(2,1)} %param.22) | copy-start | bytes 1156
  114.2 101.5 %collective-permute-start = (f32[2,64]{0,1:T(8,128)S(1)}, f32[2,64]{0,1:T(8,128)S(1)}, u32[]{:S(2)}, u32[]{:S(2)}) collective-permute-start(f32[2,64]{0,1:T(8,128)S(1)} %slice.58), channel_id=1, source_target_pairs={{0,16},{16,32},{32,48},{48,64},{64,80},{80,96},{96,112},{112,128},... | collective-permute-start | bytes 1544 | tf_op jit(solution)/shard_map/ppermute | solution.py:30
  178.6 19.9 %all-to-all-start.1 = ((bf16[32,24,128]{2,1,0:T(8,128)(2,1)}), bf16[32,24,128]{2,1,0:T(8,128)(2,1)S(1)}, u32[]{:S(2)}, u32[]{:S(2)}) async-start(bf16[32,24,128]{2,1,0:T(8,128)(2,1)} %bitcast.14), calls=%async_computation.1 | async-start | bytes 393216 | tf_op jit(solution)/shard_map/all_to_all | solution.py:128
  189.1 3.9 %copy-start.3 = (bf16[32,24,2048]{2,1,0:T(8,128)(2,1)S(1)}, bf16[32,24,2048]{2,1,0:T(8,128)(2,1)}, u32[]{:S(2)}) copy-start(bf16[32,24,2048]{2,1,0:T(8,128)(2,1)} %copy-done.2) | copy-start | bytes 9437188
  193.0 22.6 %copy-start.4 = (bf16[128,2048]{1,0:T(8,128)(2,1)S(1)}, bf16[128,2048]{1,0:T(8,128)(2,1)}, u32[]{:S(2)}) copy-start(bf16[128,2048]{1,0:T(8,128)(2,1)} %param.12) | copy-start | bytes 1572868
  193.0 22.6 %copy-start.6 = (bf16[2048,64]{0,1:T(8,128)(2,1)S(1)}, bf16[2048,64]{0,1:T(8,128)(2,1)}, u32[]{:S(2)}) copy-start(bf16[2048,64]{0,1:T(8,128)(2,1)} %param.23) | copy-start | bytes 786436
  193.0 22.6 %copy-start.7 = (bf16[128,64]{0,1:T(8,128)(2,1)S(1)}, bf16[128,64]{0,1:T(8,128)(2,1)}, u32[]{:S(2)}) copy-start(bf16[128,64]{0,1:T(8,128)(2,1)} %param.19) | copy-start | bytes 49156
  218.7 17.3 %all-to-all-start.2 = ((bf16[32,2,2048]{2,1,0:T(2,128)(2,1)}), bf16[32,2,2048]{2,1,0:T(2,128)(2,1)S(1)}, u32[]{:S(2)}, u32[]{:S(2)}) async-start(bf16[32,2,2048]{2,1,0:T(2,128)(2,1)} %reshape.94), calls=%async_computation.2 | async-start | bytes 524288 | tf_op jit(solution)/shard_map/all_to_all | solution.py:40
  224.2 8.7 %collective-permute-start.1 = (f32[2,64]{0,1:T(8,128)S(1)}, f32[2,64]{0,1:T(8,128)S(1)}, u32[]{:S(2)}, u32[]{:S(2)}) collective-permute-start(f32[2,64]{0,1:T(8,128)S(1)} %bitcast.100), channel_id=1, source_target_pairs={{16,0},{32,16},{48,32},{64,48},{80,64},{96,80},{112,96},{128,112},... | collective-permute-start | bytes 1544 | tf_op jit(solution)/shard_map/ppermute | solution.py:30
Sparse Core Ops, SparseCore 0:
  41.5 56.1 all-gather.1
  113.5 63.3 reduce-scatter.3
where the time goes:
time: 246 us; the launch traced here: 244 us
  waiting for transfers between devices  123 us (50%)
  blocking collectives  44.1 us (18%)
  starting transfers between devices  22.4 us (9%)
  matrix products  18.8 us (8%)
  local copies, waits for them, and re-layouts  17 us (7%)
  between operations  14.3 us (6%)
  other arithmetic  3.96 us (2%)
    unnamed x3, waiting for transfers between devices  59.2 us
    all_gather x1, waiting for transfers between devices, sent_together(): result = lax.all_gather(both, axis, axis=dim, tiled=True)  56.3 us
    all_to_all x1, blocking collectives, side_by_side(): lax.all_to_all(both, axis, split_axis=split_dim, concat_axis=concat_dim,...  27.2 us
    all_gather x1, blocking collectives, per_device(): moe_grad = lax.all_gather(moe_part, 'tp', axis=1, tiled=True)  16.9 us
    unnamed x31, local copies, waits for them, and re-layouts  11.8 us
    all_to_all x1, starting transfers between devices, per_device(): lax.all_to_all(half_grad, 'sp', split_axis=0, concat_axis=0, tiled=True)  10.5 us
    ppermute x2, starting transfers between devices, from_behind(): return lax.ppermute(block, axis, route)  6.3 us
    all_to_all x1, starting transfers between devices, sent_and_summed(): lax.all_to_all(tiles, axis, split_axis=0, concat_axis=0, tiled=True)  5.57 us
  transfers between devices with their start and end apart: 6, of which 5 were waited for; matrix products, arithmetic and copies ran while one was open for 5% of the time, Pallas kernels for 0%

commit v1 on v0

v1 whole, which is shorter than its diff:
```python
import functools

import jax
import jax.numpy as jnp
from jax import lax
from jax.experimental import pallas as pl
from jax.experimental.pallas import tpu as pltpu
from jax.sharding import Mesh, PartitionSpec as P

BF16, F32, I32 = jnp.bfloat16, jnp.float32, jnp.int32
TP = ("y", "c")
NT = (((1,), (1,)), ((), ()))
TN = (((0,), (0,)), ((), ()))
LANES = 128
VMEM = pl.BlockSpec(memory_space=pltpu.VMEM)


def mm(a, b, dims=None):
    if dims is None:
        return jnp.dot(a, b, preferred_element_type=F32)
    return lax.dot_general(a, b, dims, preferred_element_type=F32)


def call(body, out, cost, **kw):
    flops, moved = cost
    return pl.pallas_call(
        body,
        out_shape=out,
        cost_estimate=pl.CostEstimate(flops=flops, bytes_accessed=moved, transcendentals=0),
        compiler_params=pltpu.CompilerParams(vmem_limit_bytes=48 * 1024 * 1024),
        **kw,
    )


def shape(dims, kind):
    return jax.ShapeDtypeStruct(dims, kind)


def select_body(experts, capacity, at_ref, routes_ref, weights_ref, rows_ref, cot_ref, send_ref, select_ref):
    tokens = routes_ref.shape[1]
    number = lax.broadcasted_iota(I32, (experts, tokens), 0)
    first = routes_ref[0:1, :] == number
    second = routes_ref[1:2, :] == number
    hit = jnp.where(first | second, 1.0, 0.0).astype(F32)
    weight = jnp.where(first, weights_ref[0:1, :], jnp.where(second, weights_ref[1:2, :], 0.0))
    earlier = lax.broadcasted_iota(I32, (tokens, tokens), 0) < lax.broadcasted_iota(I32, (tokens, tokens), 1)
    place = mm(hit.astype(BF16), jnp.where(earlier, 1.0, 0.0).astype(BF16))
    place = jnp.where(hit > 0.0, place, -1.0)
    slot = lax.broadcasted_iota(I32, (capacity, tokens), 0).astype(F32)
    picked, scales = [], []
    for e in range(experts):
        one = jnp.where(slot == place[e : e + 1, :], 1.0, 0.0)
        scale = jnp.sum(one * weight[e : e + 1, :], axis=1, keepdims=True)
        picked += [one, one]
        scales += [scale, scale]
    select = jnp.concatenate(picked, axis=0).astype(BF16)
    scale = jnp.concatenate(scales, axis=0)
    select_ref[...] = select
    send_ref[:, :LANES] = mm(select, rows_ref[...]).astype(BF16)
    send_ref[:, LANES:] = (mm(select, cot_ref[...]) * scale).astype(BF16)


def expert_body(steps, core_ref, got_ref, gate_ref, up_ref, down_ref, delta_ref, hidden_ref, own_ref, other_ref, both):
    @pl.when(pl.program_id(0) == 0)
    def _():
        both[:, :LANES] = gate_ref[...]
        both[:, LANES:] = up_ref[...]

    rows = got_ref.shape[1]
    pre = jnp.zeros((rows, 2 * LANES), F32)
    back = jnp.zeros((rows, LANES), F32)
    for k in range(steps):
        ch = slice(k * 2 * LANES, (k + 1) * 2 * LANES)
        x = jnp.concatenate([got_ref[2 * k, :, :LANES], got_ref[2 * k + 1, :, :LANES]], axis=1)
        d = jnp.concatenate([got_ref[2 * k, :, LANES:], got_ref[2 * k + 1, :, LANES:]], axis=1)
        pre = pre + mm(x, both[ch, :])
        back = back + mm(d, down_ref[:, ch], NT)
    gate, up = pre[:, :LANES], pre[:, LANES:]
    sigma = jax.nn.sigmoid(gate)
    silu = gate * sigma
    hidden_ref[...] = (silu * up).astype(BF16)
    delta = jnp.concatenate(
        [
            (back * up * sigma * (1.0 + gate * (1.0 - sigma))).astype(BF16),
            (back * silu).astype(BF16),
        ],
        axis=1,
    )
    delta_ref[...] = delta
    core = core_ref[0]
    for y in range(0, steps, 2):
        for ref, c in ((other_ref, 1 - core), (own_ref, core)):
            lo = both[pl.ds(pl.multiple_of((2 * y + c) * LANES, LANES), LANES), :]
            hi = both[pl.ds(pl.multiple_of((2 * y + 2 + c) * LANES, LANES), LANES), :]
            part = mm(delta, jnp.concatenate([lo, hi], axis=0), NT).astype(BF16)
            ref[y] = part[:, :LANES]
            ref[y + 1] = part[:, LANES:]


def weight_body(got_ref, delta_ref, hidden_ref, gate_ref, up_ref, down_ref):
    x = jnp.concatenate([got_ref[0, :, :LANES], got_ref[1, :, :LANES]], axis=1)
    d = jnp.concatenate([got_ref[0, :, LANES:], got_ref[1, :, LANES:]], axis=1)
    grads = mm(x, delta_ref[...], TN)
    gate_ref[...] = grads[:, :LANES].astype(BF16)
    up_ref[...] = grads[:, LANES:].astype(BF16)
    down_ref[...] = mm(hidden_ref[...], d, TN).astype(BF16)


def token_body(at_ref, back_ref, select_ref, cot_ref, conv_ref, grad_ref, out_ref):
    moe = mm(select_ref[...], back_ref[...], TN).astype(BF16)
    grad = (cot_ref[...].astype(F32) + moe.astype(F32)).astype(BF16)
    grad_ref[...] = grad
    flipped = grad.astype(F32).T.astype(BF16)
    count, width, tokens = conv_ref.shape
    half = width // 2
    left = jnp.concatenate([flipped[r * width : r * width + half] for r in range(2)], axis=0)
    right = jnp.concatenate([flipped[r * width + half : (r + 1) * width] for r in range(2)], axis=0)
    lhs = jnp.concatenate([left, right], axis=1)
    blank = jnp.zeros((width, tokens), BF16)
    for j in range(0, count, 2):
        rhs = []
        for k in (j, j + 1):
            rhs += [jnp.concatenate([conv_ref[k], blank], axis=1), jnp.concatenate([blank, conv_ref[k]], axis=1)]
        part = mm(lhs, jnp.concatenate(rhs, axis=0), NT).astype(BF16)
        for r in range(2):
            rows = part[r * half : (r + 1) * half]
            out_ref[r * count + j] = rows[:, :LANES]
            out_ref[r * count + j + 1] = rows[:, LANES:]


def conv_body(steps, grads_ref, weight_ref, sum_ref, outer_ref, outer_grad_ref, scaled_ref):
    total = jnp.zeros(sum_ref.shape, F32)
    for k in range(steps):
        g = jnp.concatenate([grads_ref[2 * k], grads_ref[2 * k + 1]], axis=1)
        total = total + mm(weight_ref[:, k * 2 * LANES : (k + 1) * 2 * LANES], g, NT)
    outer_grad_ref[...] = (total * sum_ref[...]).astype(BF16)
    scaled_ref[...] = total * outer_ref[...].astype(F32)


def per_device(
    cotangent,
    stream,
    routes,
    route_weights,
    gate_weight,
    up_weight,
    down_weight,
    outer_gate,
    inner_gate,
    conv_input,
    conv_taps,
    out_weight,
):
    groups = lax.axis_size("sp")
    ys = lax.axis_size("y")
    tps = 2 * ys
    experts = groups // 2
    tokens, width = stream.shape
    capacity = 3 * tokens // experts
    slots = groups * capacity
    units = gate_weight.shape[2]
    channels = outer_gate.shape[1]
    core = lax.axis_index("c").astype(I32).reshape(1)
    at = (2 * lax.axis_index("y") + lax.axis_index("c")).astype(I32).reshape(1)
    swap = [(0, 1), (1, 0)]

    block = pl.BlockSpec((tokens, LANES), lambda i, at: (0, at[0]))
    whole = lambda *dims: pl.BlockSpec(dims, lambda i, at: (0,) * len(dims))
    send, select = call(
        functools.partial(select_body, experts, capacity),
        (shape((slots, 2 * LANES), BF16), shape((slots, LANES), BF16)),
        (2 * slots * tokens * 2 * LANES, 2**20),
        grid_spec=pltpu.PrefetchScalarGridSpec(
            num_scalar_prefetch=1,
            grid=(1,),
            in_specs=[whole(2, tokens), whole(2, tokens), block, block],
            out_specs=[whole(slots, 2 * LANES), whole(slots, LANES)],
        ),
    )(at, routes.T, route_weights.T, stream, cotangent)
    recv = lax.all_to_all(
        send.reshape(groups, capacity, 2 * LANES), "sp", split_axis=0, concat_axis=0, tiled=True
    ).reshape(slots, 2 * LANES)

    outer_t, inner_t, input_t, taps_t = (a.T for a in (outer_gate, inner_gate, conv_input, conv_taps))
    recv, inner_t = lax.optimization_barrier((recv, inner_t))
    got = lax.all_gather(recv, TP)
    outer_f, inner_f, input_f, taps = (a.astype(F32) for a in (outer_t, inner_t, input_t, taps_t))
    mixed = inner_f * input_f
    before = lax.ppermute(mixed[:, -2:], "sp", [(i - 1, i) for i in range(1, groups)])
    padded = jnp.concatenate([before, mixed], axis=1)
    conv_sum = taps[:, 0:1] * padded[:, :-2] + taps[:, 1:2] * padded[:, 1:-1] + taps[:, 2:3] * padded[:, 2:]
    conv_out = (outer_f * conv_sum).astype(BF16)
    conv_all = lax.all_gather(conv_out, TP)

    rows = 2 * LANES
    full = lambda *dims: pl.BlockSpec(dims, lambda i, at: (0,) * len(dims))
    delta, hidden, own, other = call(
        functools.partial(expert_body, ys),
        (
            shape((slots, 2 * units), BF16),
            shape((slots, units), BF16),
            shape((ys, slots, LANES), BF16),
            shape((ys, slots, LANES), BF16),
        ),
        (10 * slots * width * units, 2**24),
        grid_spec=pltpu.PrefetchScalarGridSpec(
            num_scalar_prefetch=1,
            grid=(slots // rows,),
            in_specs=[
                pl.BlockSpec((tps, rows, 2 * LANES), lambda i, at: (0, i, 0)),
                full(width, units),
                full(width, units),
                full(units, width),
            ],
            out_specs=[
                pl.BlockSpec((rows, 2 * units), lambda i, at: (i, 0)),
                pl.BlockSpec((rows, units), lambda i, at: (i, 0)),
                pl.BlockSpec((ys, rows, LANES), lambda i, at: (0, i, 0)),
                pl.BlockSpec((ys, rows, LANES), lambda i, at: (0, i, 0)),
            ],
            scratch_shapes=[pltpu.VMEM((width, 2 * units), BF16)],
        ),
    )(core, got, gate_weight[0], up_weight[0], down_weight[0])
    partner = lax.ppermute(other, "c", swap)
    chip = (own.astype(F32) + partner.astype(F32)).astype(BF16)
    half_sums = lax.psum_scatter(chip, "y", scatter_dimension=0)

    fixed = lambda *dims: pl.BlockSpec(dims, lambda i: (0,) * len(dims))
    gate_grad, up_grad, down_grad = call(
        weight_body,
        (shape((width, units), BF16), shape((width, units), BF16), shape((units, width), BF16)),
        (6 * slots * width * units, 2**24),
        grid=(ys,),
        in_specs=[
            pl.BlockSpec((2, slots, 2 * LANES), lambda i: (i, 0, 0)),
            fixed(slots, 2 * units),
            fixed(slots, units),
        ],
        out_specs=[
            pl.BlockSpec((2 * LANES, units), lambda i: (i, 0)),
            pl.BlockSpec((2 * LANES, units), lambda i: (i, 0)),
            pl.BlockSpec((units, 2 * LANES), lambda i: (0, i)),
        ],
    )(got, delta, hidden)

    returned = lax.all_to_all(
        half_sums.reshape(groups, capacity, LANES), "sp", split_axis=0, concat_axis=0, tiled=True
    )
    stream_block, out_parts = call(
        token_body,
        (shape((tokens, LANES), BF16), shape((groups, channels // 2, LANES), BF16)),
        (2 * slots * tokens * LANES, 2**21),
        grid_spec=pltpu.PrefetchScalarGridSpec(
            num_scalar_prefetch=1,
            grid=(1,),
            in_specs=[whole(slots, LANES), whole(slots, LANES), block, whole(tps, channels, tokens)],
            out_specs=[whole(tokens, LANES), whole(groups, channels // 2, LANES)],
        ),
    )(at, returned.reshape(slots, LANES), select, cotangent, conv_all)

    out_tiles = lax.all_to_all(out_parts, "sp", split_axis=0, concat_axis=0, tiled=True)
    stream_all = lax.all_gather(stream_block, TP)
    outer_grad, scaled = call(
        functools.partial(conv_body, ys),
        (shape((channels, tokens), BF16), shape((channels, tokens), F32)),
        (2 * tokens * width * channels, 2**20),
        in_specs=[VMEM] * 4,
        out_specs=[VMEM] * 2,
    )(stream_all, out_weight.T, conv_sum, outer_t)
    later = lax.ppermute(scaled[:, :2], "sp", [(i, i - 1) for i in range(1, groups)])
    extended = jnp.concatenate([scaled, later], axis=1)
    mixed_grad = taps[:, 2:3] * extended[:, :-2] + taps[:, 1:2] * extended[:, 1:-1] + taps[:, 0:1] * extended[:, 2:]
    inner_grad = (mixed_grad * input_f).astype(BF16)
    input_grad = (mixed_grad * inner_f).astype(BF16)

    moves = [
        ((r * tps + j) * tps + t, (2 * t + r) * tps + j) for r in range(2) for j in range(tps) for t in range(tps)
    ]
    tile = lax.ppermute(out_tiles.astype(F32).sum(axis=0), ("sp", "y", "c"), moves)
    out_grad = jnp.concatenate([tile[:, :channels], tile[:, channels:]], axis=0)
    return (gate_grad[None], up_grad[None], down_grad[None], out_grad, outer_grad.T, inner_grad.T, input_grad.T)


def solution(mesh):
    groups, tps = mesh.devices.shape
    fine = Mesh(mesh.devices.reshape(groups, tps // 2, 2), ("sp", "y", "c"))
    placed = (
        P("sp", None),
        P("sp", None),
        P("sp", None),
        P("sp", None),
        P("sp", None, TP),
        P("sp", None, TP),
        P("sp", TP, None),
        P("sp", TP),
        P("sp", TP),
        P("sp", TP),
        P(None, TP),
        P(None, TP),
    )
    return jax.shard_map(
        per_device,
        mesh=fine,
        in_specs=placed,
        out_specs=(
            P("sp", None, TP),
            P("sp", None, TP),
            P("sp", TP, None),
            P("sp", TP),
            P("sp", TP),
            P("sp", TP),
            P("sp", TP),
        ),
        check_vma=False,
    )
```

time: 246 us -> 231 us (0.939)
  waiting for transfers between devices: 123 us -> 99.9 us
  matrix products: 18.8 us -> 0 us
  Pallas kernels: 0 us -> 16.2 us
  blocking collectives: 44.1 us -> 59.9 us
  local copies, waits for them, and re-layouts: 17 us -> 4.33 us
  starting transfers between devices: 22.4 us -> 30.7 us
    unnamed x3 -> x2, waiting for transfers between devices: 59.2 us -> 0.03 us
    reduce_scatter x0 -> x1, waiting for transfers between devices: none -> 37.7 us  [per_device(): half_sums = lax.psum_scatter(chip, 'y', scatter_dimension=0)]
    dot_general x13 -> x0, matrix products: 18.8 us -> none  [the longest x1 3.87 us: per_device(): lax.dot_general(routed_rows, gate_delta, contract_first, preferred_elemen...]
    pallas_call x0 -> x5, Pallas kernels: none -> 16.2 us  [the longest x1 7.83 us: per_device(): call(weight_body, (shape((width, units), BF16), shape((width, units), BF1...]
    all_gather x1 -> x2, blocking collectives: 16.9 us -> 32.4 us  [the longest x1 16.3 us: per_device(): conv_all = lax.all_gather(conv_out, TP)]
    ppermute x2 -> x4, waiting for transfers between devices: 2.2 us -> 16.8 us  [the longest x1 8.53 us: per_device(): lax.ppermute(out_tiles.astype(F32).sum(axis=0), ('sp', 'y', 'c'), moves)]
    all_gather x1, waiting for transfers between devices: 56.3 us -> 45.4 us  [per_device(): got = lax.all_gather(recv, TP)]
    unnamed x31 -> x27, local copies, waits for them, and re-layouts: 11.8 us -> 4.18 us
  transfers between devices with their start and end apart: 6 -> 8, of which waited for: 5 -> 5; matrix products, arithmetic and copies ran while one was open for 5% -> 1% of each run, Pallas kernels for 0% -> 4%
where the time goes in v1:
time: 231 us; the launch traced here: 229 us
  waiting for transfers between devices  99.9 us (43%)
  blocking collectives  59.9 us (26%)
  starting transfers between devices  30.7 us (13%)
  Pallas kernels  16.2 us (7%)
  between operations  14.2 us (6%)
  local copies, waits for them, and re-layouts  4.33 us (2%)
  other arithmetic  3.69 us (2%)
    all_gather x1, waiting for transfers between devices, per_device(): got = lax.all_gather(recv, TP)  45.4 us
    reduce_scatter x1, waiting for transfers between devices, per_device(): half_sums = lax.psum_scatter(chip, 'y', scatter_dimension=0)  37.7 us
    all_to_all x1, blocking collectives, per_device(): lax.all_to_all(send.reshape(groups, capacity, 2 * LANES), 'sp', split_axi...  27.5 us
    all_gather x1, blocking collectives, per_device(): conv_all = lax.all_gather(conv_out, TP)  16.3 us
    all_gather x1, blocking collectives, per_device(): stream_all = lax.all_gather(stream_block, TP)  16.1 us
    all_to_all x1, starting transfers between devices, per_device(): lax.all_to_all(half_sums.reshape(groups, capacity, LANES), 'sp', split_ax...  10.5 us
    all_to_all x1, starting transfers between devices, per_device(): lax.all_to_all(out_parts, 'sp', split_axis=0, concat_axis=0, tiled=True)  9.76 us
    ppermute x1, waiting for transfers between devices, per_device(): lax.ppermute(out_tiles.astype(F32).sum(axis=0), ('sp', 'y', 'c'), moves)  8.53 us
  transfers between devices with their start and end apart: 8, of which 5 were waited for; matrix products, arithmetic and copies ran while one was open for 1% of the time, Pallas kernels for 4%

profile of v1, /device:TPU:6, one launch (start us, length us, event | category | flops | bytes accessed | tf_op | source)
XLA Modules:
  0.0 228.9 jit_solution(10381118057277815928)
XLA Ops:
  7.2 0.0 all-gather.5.cloned.1.call-start
  7.2 0.0 copy-start
  7.2 1.0 copy-done
  8.3 0.0 copy-start.5
  8.3 1.0 copy-done.5
  9.3 0.0 copy-start.8
  9.3 0.7 copy-done.8
  10.0 0.0 copy-start.9
  10.0 0.7 copy-done.9
  10.7 0.0 copy-start.2
  10.7 0.0 copy-start.3
  10.7 0.0 copy-start.4
  10.7 0.4 shard_map.171
  11.1 27.5 %all_to_all.15 = bf16[32,24,256]{2,1,0:T(8,128)(2,1)} all-to-all(bf16[32,24,256]{2,1,0:T(8,128)(2,1)S(1)} %bitcast.48), channel_id=1, replica_groups=mesh['sp'=32,'y'=8,'c'=2] {'sp'}, dimensions={0} | all-to-all | bytes 786432 | tf_op jit(solution)/shard_map/all_to_all | solution.py:180
  38.6 0.0 all-gather.5.cloned.1.call-update
  38.6 0.0 reduce-scatter.2.cloned.1.call-start
  38.7 45.4 %all-gather.5.cloned.1.call-done = bf16[12288,256]{1,0:T(8,128)(2,1)} async-done(((bf16[768,256]{1,0:T(8,128)(2,1)}), bf16[12288,256]{1,0:T(8,128)(2,1)}) %all-gather.5.cloned.1.call-update) | async-done | bytes 6291472 | tf_op jit(solution)/shard_map/all_gather | solution.py:186
  84.1 0.0 copy-done.2
  84.1 0.0 copy-done.3
  84.1 0.0 copy-done.4
  84.1 5.6 %shard_map.172 = (bf16[768,256]{1,0:T(8,128)(2,1)S(1)}, bf16[768,128]{1,0:T(8,128)(2,1)S(1)}, bf16[8,768,128]{2,1,0:T(8,128)(2,1)S(1)}, bf16[8,768,128]{2,1,0:T(8,128)(2,1)S(1)}) custom-call(s32[1]{0:T(128)} %bitcast.7.core_ref, bf16[16,768,256]{2,1,0:T(8,128)(2,1)} %bitcast.54, bf16[2048,128]{1,0:T(8,128)(2,1)S(1)} %bitcast.45, ...), custom_call_target="tpu_custom_call" | custom-call | flops 2013265920 | bytes 16777216 | tf_op jit(solution)/shard_map/pallas_call | solution.py:197
  89.7 2.1 collective-permute-start
  91.9 3.2 %collective-permute-done = bf16[8,768,128]{2,1,0:T(8,128)(2,1)S(1)} collective-permute-done((bf16[8,768,128]{2,1,0:T(8,128)(2,1)S(1)}, bf16[8,768,128]{2,1,0:T(8,128)(2,1)S(1)}, u32[]{:S(2)}, u32[]{:S(2)}) %collective-permute-start) | collective-permute-done | bytes 1572896 | tf_op jit(solution)/shard_map/ppermute | solution.py:224
  95.0 1.6 add_convert_fusion
  96.6 0.0 copy-start.12
  96.6 0.0 copy-start.10
  96.6 0.0 copy-start.11
  96.6 0.0 copy-start.7
  96.6 0.0 reduce-scatter.2.cloned.1.call-update
  96.6 0.6 copy-done.12
  97.3 0.1 copy-done.10
  97.3 0.0 copy-done.11
  97.3 0.1 slice.47
  97.4 3.5 %collective-permute-start.1 = (f32[64,2]{1,0:T(8,128)S(1)}, f32[64,2]{1,0:T(8,128)S(1)}, u32[]{:S(2)}, u32[]{:S(2)}) collective-permute-start(f32[64,2]{1,0:T(8,128)S(1)} %slice.47), channel_id=1, source_target_pairs={{0,16},{16,32},{32,48},{48,64},{64,80},{80,96},{96,112},{112,128},... | collective-permute-start | bytes 1544 | tf_op jit(solution)/shard_map/ppermute | solution.py:189
  101.0 37.7 %reduce-scatter.2.cloned.1.call-done = bf16[1,768,128]{2,1,0:T(8,128)(2,1)} async-done(((bf16[8,768,128]{2,1,0:T(8,128)(2,1)}), bf16[1,768,128]{2,1,0:T(8,128)(2,1)}) %reduce-scatter.2.cloned.1.call-update) | async-done | bytes 196624 | tf_op jit(solution)/shard_map/reduce_scatter | solution.py:226
  138.6 10.5 %all-to-all-start.1 = ((bf16[32,24,128]{2,1,0:T(8,128)(2,1)}), bf16[32,24,128]{2,1,0:T(8,128)(2,1)S(1)}, u32[]{:S(2)}, u32[]{:S(2)}) async-start(bf16[32,24,128]{2,1,0:T(8,128)(2,1)} %bitcast.57), calls=%async_computation.2 | async-start | bytes 393216 | tf_op jit(solution)/shard_map/all_to_all | solution.py:246
  149.1 0.0 collective-permute-done.1
  149.1 0.0 copy-done.7
  149.2 0.1 multiply_convert_fusion
  149.3 16.3 %all-gather.1 = bf16[1024,128]{1,0:T(8,128)(2,1)S(1)} all-gather(bf16[64,128]{1,0:T(8,128)(2,1)S(1)} %get-tuple-element.39), channel_id=3, replica_groups=mesh['sp'=32,'y'=8,'c'=2] {'y','c'}, dimensions={0}, use_global_device_ids=true | all-gather | bytes 278528 | tf_op jit(solution)/shard_map/all_gather | solution.py:193
  165.6 0.0 copy-start.1
  165.6 7.8 %shard_map.173 = (bf16[2048,128]{1,0:T(8,128)(2,1)}, bf16[2048,128]{1,0:T(8,128)(2,1)}, bf16[128,2048]{1,0:T(8,128)(2,1)}) custom-call(bf16[16,768,256]{2,1,0:T(8,128)(2,1)} %bitcast.55, bf16[768,256]{1,0:T(8,128)(2,1)S(1)} %get-tuple-element.24.delta_ref, bf16[768,128]{1,0:T(8,128)(2,1)S(1)} %get-tuple-element.25.hidden_ref), custom_call_target="tpu_custom_call" | custom-call | flops 1207959552 | bytes 16777216 | tf_op jit(solution)/shard_map/pallas_call | solution.py:229
  173.5 0.0 copy-start.6
  173.5 0.0 all-to-all-done.1
  173.5 0.0 copy-done.1
  173.5 1.4 shard_map.174
  174.9 9.8 %all-to-all-start.2 = ((bf16[32,32,128]{2,1,0:T(8,128)(2,1)}), bf16[32,32,128]{2,1,0:T(8,128)(2,1)S(1)}, u32[]{:S(2)}, u32[]{:S(2)}) async-start(bf16[32,32,128]{2,1,0:T(8,128)(2,1)} %get-tuple-element.33), calls=%async_computation.3 | async-start | bytes 524288 | tf_op jit(solution)/shard_map/all_to_all | solution.py:261
  184.6 16.1 %all-gather.2 = bf16[2048,128]{1,0:T(8,128)(2,1)S(1)} all-gather(bf16[128,128]{1,0:T(8,128)(2,1)S(1)} %get-tuple-element.34), channel_id=4, replica_groups=mesh['sp'=32,'y'=8,'c'=2] {'y','c'}, dimensions={0}, use_global_device_ids=true | all-gather | bytes 557056 | tf_op jit(solution)/shard_map/all_gather | solution.py:262
  200.7 0.0 copy-done.6
  200.7 0.9 shard_map.175
  201.6 2.8 %collective-permute-start.3 = (f32[64,2]{1,0:T(8,128)S(1)}, f32[64,2]{1,0:T(8,128)S(1)}, u32[]{:S(2)}, u32[]{:S(2)}) collective-permute-start(f32[64,2]{1,0:T(8,128)S(1)} %bitcast.50), channel_id=1, source_target_pairs={{16,0},{32,16},{48,32},{64,48},{80,64},{96,80},{112,96},{128,112},... | collective-permute-start | bytes 1544 | tf_op jit(solution)/shard_map/ppermute | solution.py:270
  204.4 5.1 %collective-permute-done.3 = f32[64,2]{1,0:T(8,128)S(1)} collective-permute-done((f32[64,2]{1,0:T(8,128)S(1)}, f32[64,2]{1,0:T(8,128)S(1)}, u32[]{:S(2)}, u32[]{:S(2)}) %collective-permute-start.3) | collective-permute-done | bytes 544 | tf_op jit(solution)/shard_map/ppermute | solution.py:270
  209.5 0.7 fusion.10
  210.2 0.0 all-to-all-done.2
  210.3 1.9 collective-permute-start.2
  212.2 0.6 fusion.9
  212.8 8.5 %collective-permute-done.2 = f32[32,128]{1,0:T(8,128)S(1)} collective-permute-done((f32[32,128]{1,0:T(8,128)S(1)}, f32[32,128]{1,0:T(8,128)S(1)}, u32[]{:S(2)}, u32[]{:S(2)}) %collective-permute-start.2) | collective-permute-done | bytes 16416 | tf_op jit(solution)/shard_map/ppermute | solution.py:279
  221.4 0.1 fusion.13
  221.4 0.6 pad_maximum_fusion.1
  (6 shorter events, 0.1 us)
Async XLA Ops:
  7.2 76.9 %all-gather.5.cloned.1.call-start = ((), (), s32[]{:S(2)}) async-start(), calls=%async_computation.5 | async-start | bytes 6684672 | tf_op jit(solution)/shard_map/all_gather | solution.py:186
  7.2 1.0 copy-start
  8.3 1.0 copy-start.5
  9.3 0.7 copy-start.8
  10.0 0.7 copy-start.9
  10.7 73.4 %copy-start.2 = (bf16[1,2048,128]{2,1,0:T(8,128)(2,1)S(1)}, bf16[1,2048,128]{2,1,0:T(8,128)(2,1)}, u32[]{:S(2)}) copy-start(bf16[1,2048,128]{2,1,0:T(8,128)(2,1)} %param.16) | copy-start | bytes 1572868
  10.7 73.4 %copy-start.3 = (bf16[1,2048,128]{2,1,0:T(8,128)(2,1)S(1)}, bf16[1,2048,128]{2,1,0:T(8,128)(2,1)}, u32[]{:S(2)}) copy-start(bf16[1,2048,128]{2,1,0:T(8,128)(2,1)} %param.17) | copy-start | bytes 1572868
  10.7 73.4 %copy-start.4 = (bf16[1,128,2048]{2,1,0:T(8,128)(2,1)S(1)}, bf16[1,128,2048]{2,1,0:T(8,128)(2,1)}, u32[]{:S(2)}) copy-start(bf16[1,128,2048]{2,1,0:T(8,128)(2,1)} %param.18) | copy-start | bytes 1572868
  38.6 100.0 %reduce-scatter.2.cloned.1.call-start = ((), (), s32[]{:S(2)}) async-start(), calls=%async_computation.4 | async-start | bytes 1769472 | tf_op jit(solution)/shard_map/reduce_scatter | solution.py:226
  89.7 5.3 %collective-permute-start = (bf16[8,768,128]{2,1,0:T(8,128)(2,1)S(1)}, bf16[8,768,128]{2,1,0:T(8,128)(2,1)S(1)}, u32[]{:S(2)}, u32[]{:S(2)}) collective-permute-start(bf16[8,768,128]{2,1,0:T(8,128)(2,1)S(1)} %get-tuple-element.30), channel_id=1, source_target_pairs={{0,1},{1,0},{2,3},{3,2},{4,5},{5,4},{6,7},{7,6},{8,9},{9,8},{10,11... | collective-permute-start | bytes 4718600 | tf_op jit(solution)/shard_map/ppermute | solution.py:224
  96.6 0.7 copy-start.12
  96.6 0.7 copy-start.10
  96.6 0.7 copy-start.11
  96.6 52.6 %copy-start.7 = (bf16[128,64]{0,1:T(8,128)(2,1)S(1)}, bf16[128,64]{0,1:T(8,128)(2,1)}, u32[]{:S(2)}) copy-start(bf16[128,64]{0,1:T(8,128)(2,1)} %param.19) | copy-start | bytes 49156
  97.4 51.7 %collective-permute-start.1 = (f32[64,2]{1,0:T(8,128)S(1)}, f32[64,2]{1,0:T(8,128)S(1)}, u32[]{:S(2)}, u32[]{:S(2)}) collective-permute-start(f32[64,2]{1,0:T(8,128)S(1)} %slice.47), channel_id=1, source_target_pairs={{0,16},{16,32},{32,48},{48,64},{64,80},{80,96},{96,112},{112,128},... | collective-permute-start | bytes 1544 | tf_op jit(solution)/shard_map/ppermute | solution.py:189
  138.6 34.8 %all-to-all-start.1 = ((bf16[32,24,128]{2,1,0:T(8,128)(2,1)}), bf16[32,24,128]{2,1,0:T(8,128)(2,1)S(1)}, u32[]{:S(2)}, u32[]{:S(2)}) async-start(bf16[32,24,128]{2,1,0:T(8,128)(2,1)} %bitcast.57), calls=%async_computation.2 | async-start | bytes 393216 | tf_op jit(solution)/shard_map/all_to_all | solution.py:246
  165.6 7.8 %copy-start.1 = (bf16[128,2048]{1,0:T(8,128)(2,1)S(1)}, bf16[128,2048]{1,0:T(8,128)(2,1)}, u32[]{:S(2)}) copy-start(bf16[128,2048]{1,0:T(8,128)(2,1)} %cot_ref.3) | copy-start | bytes 1572868
  173.5 27.3 %copy-start.6 = (bf16[2048,64]{0,1:T(8,128)(2,1)S(1)}, bf16[2048,64]{0,1:T(8,128)(2,1)}, u32[]{:S(2)}) copy-start(bf16[2048,64]{0,1:T(8,128)(2,1)} %param.23) | copy-start | bytes 786436
  174.9 35.4 %all-to-all-start.2 = ((bf16[32,32,128]{2,1,0:T(8,128)(2,1)}), bf16[32,32,128]{2,1,0:T(8,128)(2,1)S(1)}, u32[]{:S(2)}, u32[]{:S(2)}) async-start(bf16[32,32,128]{2,1,0:T(8,128)(2,1)} %get-tuple-element.33), calls=%async_computation.3 | async-start | bytes 524288 | tf_op jit(solution)/shard_map/all_to_all | solution.py:261
  201.6 7.9 %collective-permute-start.3 = (f32[64,2]{1,0:T(8,128)S(1)}, f32[64,2]{1,0:T(8,128)S(1)}, u32[]{:S(2)}, u32[]{:S(2)}) collective-permute-start(f32[64,2]{1,0:T(8,128)S(1)} %bitcast.50), channel_id=1, source_target_pairs={{16,0},{32,16},{48,32},{64,48},{80,64},{96,80},{112,96},{128,112},... | collective-permute-start | bytes 1544 | tf_op jit(solution)/shard_map/ppermute | solution.py:270
  210.3 11.1 %collective-permute-start.2 = (f32[32,128]{1,0:T(8,128)S(1)}, f32[32,128]{1,0:T(8,128)S(1)}, u32[]{:S(2)}, u32[]{:S(2)}) collective-permute-start(f32[32,128]{1,0:T(8,128)S(1)} %convert_reduce_fusion), channel_id=1, source_target_pairs={{0,0},{1,32},{2,64},{3,96},{4,128},{5,160},{6,192},{7,224},{8,256}... | collective-permute-start | bytes 49160 | tf_op jit(solution)/shard_map/ppermute | solution.py:279
Sparse Core Ops, SparseCore 0:
  38.7 45.3 all-gather.4
  96.7 41.8 reduce-scatter.1

commit v2 on v1

--- a/solution.py
+++ b/solution.py
@@ -21,13 +21,13 @@
     return lax.dot_general(a, b, dims, preferred_element_type=F32)
 
 
-def call(body, out, cost, **kw):
+def call(body, out, cost, room=48 * 1024 * 1024, **kw):
     flops, moved = cost
     return pl.pallas_call(
         body,
         out_shape=out,
         cost_estimate=pl.CostEstimate(flops=flops, bytes_accessed=moved, transcendentals=0),
-        compiler_params=pltpu.CompilerParams(vmem_limit_bytes=48 * 1024 * 1024),
+        compiler_params=pltpu.CompilerParams(vmem_limit_bytes=room),
         **kw,
     )
 
@@ -60,12 +60,15 @@
     send_ref[:, LANES:] = (mm(select, cot_ref[...]) * scale).astype(BF16)
 
 
-def expert_body(steps, core_ref, got_ref, gate_ref, up_ref, down_ref, delta_ref, hidden_ref, own_ref, other_ref, both):
-    @pl.when(pl.program_id(0) == 0)
-    def _():
-        both[:, :LANES] = gate_ref[...]
-        both[:, LANES:] = up_ref[...]
-
+def share(delta, gate_ref, up_ref, y, c):
+    picked = []
+    for k in (y, y + 1):
+        at = pl.ds(pl.multiple_of((2 * k + c) * LANES, LANES), LANES)
+        picked.append(jnp.concatenate([gate_ref[at, :], up_ref[at, :]], axis=1))
+    return mm(delta, jnp.concatenate(picked, axis=0), NT)
+
+
+def expert_body(steps, core_ref, got_ref, gate_ref, up_ref, down_ref, delta_ref, hidden_ref, other_ref):
     rows = got_ref.shape[1]
     pre = jnp.zeros((rows, 2 * LANES), F32)
     back = jnp.zeros((rows, LANES), F32)
@@ -73,7 +76,7 @@
         ch = slice(k * 2 * LANES, (k + 1) * 2 * LANES)
         x = jnp.concatenate([got_ref[2 * k, :, :LANES], got_ref[2 * k + 1, :, :LANES]], axis=1)
         d = jnp.concatenate([got_ref[2 * k, :, LANES:], got_ref[2 * k + 1, :, LANES:]], axis=1)
-        pre = pre + mm(x, both[ch, :])
+        pre = pre + mm(x, jnp.concatenate([gate_ref[ch, :], up_ref[ch, :]], axis=1))
         back = back + mm(d, down_ref[:, ch], NT)
     gate, up = pre[:, :LANES], pre[:, LANES:]
     sigma = jax.nn.sigmoid(gate)
@@ -87,14 +90,18 @@
         axis=1,
     )
     delta_ref[...] = delta
-    core = core_ref[0]
     for y in range(0, steps, 2):
-        for ref, c in ((other_ref, 1 - core), (own_ref, core)):
-            lo = both[pl.ds(pl.multiple_of((2 * y + c) * LANES, LANES), LANES), :]
-            hi = both[pl.ds(pl.multiple_of((2 * y + 2 + c) * LANES, LANES), LANES), :]
-            part = mm(delta, jnp.concatenate([lo, hi], axis=0), NT).astype(BF16)
-            ref[y] = part[:, :LANES]
-            ref[y + 1] = part[:, LANES:]
+        part = share(delta, gate_ref, up_ref, y, 1 - core_ref[0]).astype(BF16)
+        other_ref[y] = part[:, :LANES]
+        other_ref[y + 1] = part[:, LANES:]
+
+
+def chip_body(steps, core_ref, delta_ref, gate_ref, up_ref, partner_ref, chip_ref):
+    delta = delta_ref[...]
+    for y in range(0, steps, 2):
+        part = share(delta, gate_ref, up_ref, y, core_ref[0])
+        chip_ref[y] = (part[:, :LANES] + partner_ref[y].astype(F32)).astype(BF16)
+        chip_ref[y + 1] = (part[:, LANES:] + partner_ref[y + 1].astype(F32)).astype(BF16)
 
 
 def weight_body(got_ref, delta_ref, hidden_ref, gate_ref, up_ref, down_ref):
@@ -109,7 +116,8 @@
 def token_body(at_ref, back_ref, select_ref, cot_ref, conv_ref, grad_ref, out_ref):
     moe = mm(select_ref[...], back_ref[...], TN).astype(BF16)
     grad = (cot_ref[...].astype(F32) + moe.astype(F32)).astype(BF16)
-    grad_ref[...] = grad
+    grad_ref[0] = grad
+    grad_ref[1] = grad
     flipped = grad.astype(F32).T.astype(BF16)
     count, width, tokens = conv_ref.shape
     half = width // 2
@@ -131,7 +139,7 @@
 def conv_body(steps, grads_ref, weight_ref, sum_ref, outer_ref, outer_grad_ref, scaled_ref):
     total = jnp.zeros(sum_ref.shape, F32)
     for k in range(steps):
-        g = jnp.concatenate([grads_ref[2 * k], grads_ref[2 * k + 1]], axis=1)
+        g = jnp.concatenate([grads_ref[2 * k, 0], grads_ref[2 * k + 1, 0]], axis=1)
         total = total + mm(weight_ref[:, k * 2 * LANES : (k + 1) * 2 * LANES], g, NT)
     outer_grad_ref[...] = (total * sum_ref[...]).astype(BF16)
     scaled_ref[...] = total * outer_ref[...].astype(F32)
@@ -170,6 +178,7 @@
         functools.partial(select_body, experts, capacity),
         (shape((slots, 2 * LANES), BF16), shape((slots, LANES), BF16)),
         (2 * slots * tokens * 2 * LANES, 2**20),
+        room=67_043_328,
         grid_spec=pltpu.PrefetchScalarGridSpec(
             num_scalar_prefetch=1,
             grid=(1,),
@@ -190,19 +199,18 @@
     padded = jnp.concatenate([before, mixed], axis=1)
     conv_sum = taps[:, 0:1] * padded[:, :-2] + taps[:, 1:2] * padded[:, 1:-1] + taps[:, 2:3] * padded[:, 2:]
     conv_out = (outer_f * conv_sum).astype(BF16)
-    conv_all = lax.all_gather(conv_out, TP)
+    got, conv_out, conv_sum = lax.optimization_barrier((got, conv_out, conv_sum))
 
     rows = 2 * LANES
     full = lambda *dims: pl.BlockSpec(dims, lambda i, at: (0,) * len(dims))
-    delta, hidden, own, other = call(
+    delta, hidden, other = call(
         functools.partial(expert_body, ys),
         (
             shape((slots, 2 * units), BF16),
             shape((slots, units), BF16),
             shape((ys, slots, LANES), BF16),
-            shape((ys, slots, LANES), BF16),
-        ),
-        (10 * slots * width * units, 2**24),
+        ),
+        (8 * slots * width * units, 2**24),
         grid_spec=pltpu.PrefetchScalarGridSpec(
             num_scalar_prefetch=1,
             grid=(slots // rows,),
@@ -216,14 +224,29 @@
                 pl.BlockSpec((rows, 2 * units), lambda i, at: (i, 0)),
                 pl.BlockSpec((rows, units), lambda i, at: (i, 0)),
                 pl.BlockSpec((ys, rows, LANES), lambda i, at: (0, i, 0)),
+            ],
+        ),
+    )(core, got, gate_weight[0], up_weight[0], down_weight[0])
+    partner = lax.ppermute(other, "c", swap)
+    chip = call(
+        functools.partial(chip_body, ys),
+        shape((ys, slots, LANES), BF16),
+        (2 * slots * width * units, 2**22),
+        grid_spec=pltpu.PrefetchScalarGridSpec(
+            num_scalar_prefetch=1,
+            grid=(slots // rows,),
+            in_specs=[
+                pl.BlockSpec((rows, 2 * units), lambda i, at: (i, 0)),
+                full(width, units),
+                full(width, units),
                 pl.BlockSpec((ys, rows, LANES), lambda i, at: (0, i, 0)),
             ],
-            scratch_shapes=[pltpu.VMEM((width, 2 * units), BF16)],
-        ),
-    )(core, got, gate_weight[0], up_weight[0], down_weight[0])
-    partner = lax.ppermute(other, "c", swap)
-    chip = (own.astype(F32) + partner.astype(F32)).astype(BF16)
+            out_specs=pl.BlockSpec((ys, rows, LANES), lambda i, at: (0, i, 0)),
+        ),
+    )(core, delta, gate_weight[0], up_weight[0], partner)
+    chip, delta, conv_out = lax.optimization_barrier((chip, delta, conv_out))
     half_sums = lax.psum_scatter(chip, "y", scatter_dimension=0)
+    conv_all = lax.all_gather(conv_out, TP)
 
     fixed = lambda *dims: pl.BlockSpec(dims, lambda i: (0,) * len(dims))
     gate_grad, up_grad, down_grad = call(
@@ -243,18 +266,21 @@
         ],
     )(got, delta, hidden)
 
+    half_sums, gate_grad, up_grad, down_grad, conv_all = lax.optimization_barrier(
+        (half_sums, gate_grad, up_grad, down_grad, conv_all)
+    )
     returned = lax.all_to_all(
         half_sums.reshape(groups, capacity, LANES), "sp", split_axis=0, concat_axis=0, tiled=True
     )
     stream_block, out_parts = call(
         token_body,
-        (shape((tokens, LANES), BF16), shape((groups, channels // 2, LANES), BF16)),
+        (shape((2, tokens, LANES), BF16), shape((groups, channels // 2, LANES), BF16)),
         (2 * slots * tokens * LANES, 2**21),
         grid_spec=pltpu.PrefetchScalarGridSpec(
             num_scalar_prefetch=1,
             grid=(1,),
             in_specs=[whole(slots, LANES), whole(slots, LANES), block, whole(tps, channels, tokens)],
-            out_specs=[whole(tokens, LANES), whole(groups, channels // 2, LANES)],
+            out_specs=[whole(2, tokens, LANES), whole(groups, channels // 2, LANES)],
         ),
     )(at, returned.reshape(slots, LANES), select, cotangent, conv_all)
 

time: 231 us -> 213 us (0.922)
  blocking collectives: 59.9 us -> 79.7 us
  starting transfers between devices: 30.7 us -> 11 us
  waiting for transfers between devices: 99.9 us -> 82 us
  Pallas kernels: 16.2 us -> 19.4 us
    all_to_all x0 -> x2, blocking collectives: none -> 34.8 us  [the longest x1 19.8 us: per_device(): lax.all_to_all(half_sums.reshape(groups, capacity, LANES), 'sp', split_ax...]
    reduce_scatter x1, waiting for transfers between devices: 37.7 us -> 17.3 us  [per_device(): half_sums = lax.psum_scatter(chip, 'y', scatter_dimension=0)]
    all_to_all x2 -> x0, starting transfers between devices: 20.3 us -> none  [the longest x1 10.5 us: per_device(): lax.all_to_all(half_sums.reshape(groups, capacity, LANES), 'sp', split_ax...]
    all_gather x1 -> x0, blocking collectives: 16.1 us -> none  [per_device(): stream_all = lax.all_gather(stream_block, TP)]
    all_gather x1, waiting for transfers between devices: 45.4 us -> 37.3 us  [per_device(): got = lax.all_gather(recv, TP)]
    all_gather x0 -> x1, waiting for transfers between devices: none -> 7.87 us  [per_device(): stream_all = lax.all_gather(stream_block, TP)]
  transfers between devices with their start and end apart: 8 -> 7, of which waited for: 5 -> 7; matrix products, arithmetic and copies ran while one was open for 1% -> 1% of each run, Pallas kernels for 4% -> 4%
where the time goes in v2:
time: 213 us
  waiting for transfers between devices  82 us (38%)
  blocking collectives  79.7 us (37%)
  Pallas kernels  19.4 us (9%)
  between operations  13.9 us (7%)
  starting transfers between devices  11 us (5%)
  other arithmetic  4.26 us (2%)
  local copies, waits for them, and re-layouts  2.46 us (1%)
    all_gather x1, waiting for transfers between devices, per_device(): got = lax.all_gather(recv, TP)  37.3 us
    all_to_all x1, blocking collectives, per_device(): lax.all_to_all(send.reshape(groups, capacity, 2 * LANES), 'sp', split_axi...  27.7 us
    all_to_all x1, blocking collectives, per_device(): lax.all_to_all(half_sums.reshape(groups, capacity, LANES), 'sp', split_ax...  19.8 us
    all_gather x1, blocking collectives, per_device(): conv_all = lax.all_gather(conv_out, TP)  17.3 us
    reduce_scatter x1, waiting for transfers between devices, per_device(): half_sums = lax.psum_scatter(chip, 'y', scatter_dimension=0)  17.3 us
    all_to_all x1, blocking collectives, per_device(): lax.all_to_all(out_parts, 'sp', split_axis=0, concat_axis=0, tiled=True)  15 us
    ppermute x1, waiting for transfers between devices, per_device(): lax.ppermute(out_tiles.astype(F32).sum(axis=0), ('sp', 'y', 'c'), moves)  9.47 us
    all_gather x1, waiting for transfers between devices, per_device(): stream_all = lax.all_gather(stream_block, TP)  7.87 us
  transfers between devices with their start and end apart: 7, of which 7 were waited for; matrix products, arithmetic and copies ran while one was open for 1% of the time, Pallas kernels for 4%

profile of v2, /device:TPU:6, one launch (start us, length us, event | category | flops | bytes accessed | tf_op | source)
XLA Modules:
  0.0 212.6 jit_solution(1876452283108506540)
XLA Ops:
  7.2 0.0 all-gather.6.cloned.1.call-start
  7.2 2.0 shard_map.171
  9.2 0.0 copy-start
  9.2 0.0 copy-start.1
  9.2 27.7 %all_to_all.15 = bf16[32,24,256]{2,1,0:T(8,128)(2,1)} all-to-all(bf16[32,24,256]{2,1,0:T(8,128)(2,1)} %bitcast.57), channel_id=1, replica_groups=mesh['sp'=32,'y'=8,'c'=2] {'sp'}, dimensions={0} | all-to-all | bytes 786432 | tf_op jit(solution)/shard_map/all_to_all | solution.py:189
  36.9 0.0 all-gather.6.cloned.1.call-update
  36.9 0.0 reduce-scatter.2.cloned.1.call-start
  36.9 0.7 convert_bitcast_fusion
  37.6 0.7 convert_multiply_fusion.1
  38.4 0.1 slice.47
  38.4 4.1 %collective-permute-start = (f32[64,2]{1,0:T(8,128)S(1)}, f32[64,2]{1,0:T(8,128)S(1)}, u32[]{:S(2)}, u32[]{:S(2)}) collective-permute-start(f32[64,2]{1,0:T(8,128)S(1)} %slice.47), channel_id=1, source_target_pairs={{0,16},{16,32},{32,48},{48,64},{64,80},{80,96},{96,112},{112,128},... | collective-permute-start | bytes 1544 | tf_op jit(solution)/shard_map/ppermute | solution.py:198
  42.5 1.7 collective-permute-done
  44.2 0.8 multiply_convert_fusion
  45.1 37.3 %all-gather.6.cloned.1.call-done = bf16[12288,256]{1,0:T(8,128)(2,1)} async-done(((bf16[768,256]{1,0:T(8,128)(2,1)}), bf16[12288,256]{1,0:T(8,128)(2,1)}) %all-gather.6.cloned.1.call-update) | async-done | bytes 6291472 | tf_op jit(solution)/shard_map/all_gather | solution.py:195
  82.4 0.0 copy-done
  82.4 0.0 copy-done.1
  82.4 0.0 copy-start.4
  82.4 1.0 copy-done.4
  83.4 5.1 %shard_map.172 = (bf16[768,256]{1,0:T(8,128)(2,1)S(1)}, bf16[768,128]{1,0:T(8,128)(2,1)S(1)}, bf16[8,768,128]{2,1,0:T(8,128)(2,1)S(1)}) custom-call(s32[1]{0:T(128)} %bitcast.core_ref, bf16[16,768,256]{2,1,0:T(8,128)(2,1)} %bitcast.54, bf16[2048,128]{1,0:T(8,128)(2,1)S(1)} %bitcast.43, bf16[2048,128]{1,0:T(8,128)(2,1)S(1)} %bitcast.45, ...), custom_call_target="tpu_custom_call" | custom-call | flops 1610612736 | bytes 16777216 | tf_op jit(solution)/shard_map/pallas_call | solution.py:206
  88.6 2.1 %collective-permute-start.1 = (bf16[8,768,128]{2,1,0:T(8,128)(2,1)S(1)}, bf16[8,768,128]{2,1,0:T(8,128)(2,1)S(1)}, u32[]{:S(2)}, u32[]{:S(2)}) collective-permute-start(bf16[8,768,128]{2,1,0:T(8,128)(2,1)S(1)} %get-tuple-element.37), channel_id=1, source_target_pairs={{0,1},{1,0},{2,3},{3,2},{4,5},{5,4},{6,7},{7,6},{8,9},{9,8},{10,11... | collective-permute-start | bytes 4718600 | tf_op jit(solution)/shard_map/ppermute | solution.py:230
  90.7 3.1 %collective-permute-done.1.partner_ref = bf16[8,768,128]{2,1,0:T(8,128)(2,1)S(1)} collective-permute-done((bf16[8,768,128]{2,1,0:T(8,128)(2,1)S(1)}, bf16[8,768,128]{2,1,0:T(8,128)(2,1)S(1)}, u32[]{:S(2)}, u32[]{:S(2)}) %collective-permute-start.1) | collective-permute-done | bytes 1572896 | tf_op jit(solution)/shard_map/ppermute | solution.py:230
  93.9 2.4 %shard_map.173 = bf16[8,768,128]{2,1,0:T(8,128)(2,1)} custom-call(s32[1]{0:T(128)} %bitcast.core_ref, bf16[768,256]{1,0:T(8,128)(2,1)S(1)} %get-tuple-element.40.delta_ref, bf16[2048,128]{1,0:T(8,128)(2,1)S(1)} %bitcast.44, bf16[2048,128]{1,0:T(8,128)(2,1)S(1)} %bitcast.46, bf16[8,768,128]{2,1,0:T(8,128)(2,1)S(1)} %collective-permute-done.1.partner_ref), custom_call_target="tpu_custom_call" | custom-call | flops 402653184 | bytes 4194304 | tf_op jit(solution)/shard_map/pallas_call | solution.py:231
  96.2 0.0 reduce-scatter.2.cloned.1.call-update
  96.3 0.0 all-gather.8.cloned.1.call-start
  96.3 0.0 copy-start.2
  96.3 0.0 copy-start.6
  96.3 7.8 %shard_map.174 = (bf16[2048,128]{1,0:T(8,128)(2,1)}, bf16[2048,128]{1,0:T(8,128)(2,1)}, bf16[128,2048]{1,0:T(8,128)(2,1)}) custom-call(bf16[16,768,256]{2,1,0:T(8,128)(2,1)} %bitcast.55, bf16[768,256]{1,0:T(8,128)(2,1)S(1)} %get-tuple-element.40.delta_ref, bf16[768,128]{1,0:T(8,128)(2,1)S(1)} %get-tuple-element.41.hidden_ref), custom_call_target="tpu_custom_call" | custom-call | flops 1207959552 | bytes 16777216 | tf_op jit(solution)/shard_map/pallas_call | solution.py:252
  104.2 0.0 copy-start.5
  104.2 0.0 copy-start.7
  104.2 17.3 %all-gather.1 = bf16[1024,128]{1,0:T(8,128)(2,1)S(1)} all-gather(bf16[64,128]{1,0:T(8,128)(2,1)S(1)} %get-tuple-element.45), channel_id=3, replica_groups=mesh['sp'=32,'y'=8,'c'=2] {'y','c'}, dimensions={0}, use_global_device_ids=true | all-gather | bytes 278528 | tf_op jit(solution)/shard_map/all_gather | solution.py:249
  121.4 17.3 %reduce-scatter.2.cloned.1.call-done = bf16[1,768,128]{2,1,0:T(8,128)(2,1)} async-done(((bf16[8,768,128]{2,1,0:T(8,128)(2,1)}), bf16[1,768,128]{2,1,0:T(8,128)(2,1)}) %reduce-scatter.2.cloned.1.call-update) | async-done | bytes 196624 | tf_op jit(solution)/shard_map/reduce_scatter | solution.py:248
  138.7 19.8 %all_to_all.16 = bf16[32,24,128]{2,1,0:T(8,128)(2,1)S(1)} all-to-all(bf16[32,24,128]{2,1,0:T(8,128)(2,1)} %bitcast.58), channel_id=1, replica_groups=mesh['sp'=32,'y'=8,'c'=2] {'sp'}, dimensions={0} | all-to-all | bytes 393216 | tf_op jit(solution)/shard_map/all_to_all | solution.py:272
  158.5 0.0 copy-done.2
  158.5 0.0 copy-done.6
  158.5 0.0 copy-start.8
  158.5 1.1 shard_map.175
  159.6 0.0 copy-start.9
  159.6 0.0 all-gather.8.cloned.1.call-update
  159.7 15.0 %all_to_all.17 = bf16[32,32,128]{2,1,0:T(8,128)(2,1)S(1)} all-to-all(bf16[32,32,128]{2,1,0:T(8,128)(2,1)S(1)} %get-tuple-element.52), channel_id=1, replica_groups=mesh['sp'=32,'y'=8,'c'=2] {'sp'}, dimensions={0} | all-to-all | bytes 524288 | tf_op jit(solution)/shard_map/all_to_all | solution.py:287
  174.7 1.9 collective-permute-start.2
  176.6 9.5 %collective-permute-done.2 = f32[32,128]{1,0:T(8,128)S(1)} collective-permute-done((f32[32,128]{1,0:T(8,128)S(1)}, f32[32,128]{1,0:T(8,128)S(1)}, u32[]{:S(2)}, u32[]{:S(2)}) %collective-permute-start.2) | collective-permute-done | bytes 16416 | tf_op jit(solution)/shard_map/ppermute | solution.py:305
  186.1 0.1 fusion.13
  186.2 0.6 pad_maximum_fusion.1
  186.8 7.9 %all-gather.8.cloned.1.call-done = bf16[32,128,128]{2,1,0:T(8,128)(2,1)} async-done(((bf16[2,128,128]{2,1,0:T(8,128)(2,1)}), bf16[32,128,128]{2,1,0:T(8,128)(2,1)}) %all-gather.8.cloned.1.call-update) | async-done | bytes 1048592 | tf_op jit(solution)/shard_map/all_gather | solution.py:288
  194.7 0.0 copy-done.5
  194.7 0.0 copy-done.7
  194.7 0.0 copy-start.3
  194.7 1.2 copy-done.3
  195.9 0.9 shard_map.176
  196.8 2.7 %collective-permute-start.3 = (f32[64,2]{1,0:T(8,128)S(1)}, f32[64,2]{1,0:T(8,128)S(1)}, u32[]{:S(2)}, u32[]{:S(2)}) collective-permute-start(f32[64,2]{1,0:T(8,128)S(1)} %bitcast.52), channel_id=1, source_target_pairs={{16,0},{32,16},{48,32},{64,48},{80,64},{96,80},{112,96},{128,112},... | collective-permute-start | bytes 1544 | tf_op jit(solution)/shard_map/ppermute | solution.py:296
  199.5 5.2 %collective-permute-done.3 = f32[64,2]{1,0:T(8,128)S(1)} collective-permute-done((f32[64,2]{1,0:T(8,128)S(1)}, f32[64,2]{1,0:T(8,128)S(1)}, u32[]{:S(2)}, u32[]{:S(2)}) %collective-permute-start.3) | collective-permute-done | bytes 544 | tf_op jit(solution)/shard_map/ppermute | solution.py:296
  204.7 0.0 copy-done.8
  204.7 0.7 fusion.10
  205.4 0.0 copy-done.9
  205.4 0.6 fusion.9
  (4 shorter events, 0.1 us)
Async XLA Ops:
  7.2 75.2 %all-gather.6.cloned.1.call-start = ((), (), s32[]{:S(2)}) async-start(), calls=%async_computation.5 | async-start | bytes 6684672 | tf_op jit(solution)/shard_map/all_gather | solution.py:195
  9.2 73.2 %copy-start = (bf16[1,2048,128]{2,1,0:T(8,128)(2,1)S(1)}, bf16[1,2048,128]{2,1,0:T(8,128)(2,1)}, u32[]{:S(2)}) copy-start(bf16[1,2048,128]{2,1,0:T(8,128)(2,1)} %param.16) | copy-start | bytes 1572868
  9.2 73.2 %copy-start.1 = (bf16[1,2048,128]{2,1,0:T(8,128)(2,1)S(1)}, bf16[1,2048,128]{2,1,0:T(8,128)(2,1)}, u32[]{:S(2)}) copy-start(bf16[1,2048,128]{2,1,0:T(8,128)(2,1)} %param.17) | copy-start | bytes 1572868
  36.9 101.8 %reduce-scatter.2.cloned.1.call-start = ((), (), s32[]{:S(2)}) async-start(), calls=%async_computation.4 | async-start | bytes 1769472 | tf_op jit(solution)/shard_map/reduce_scatter | solution.py:248
  38.4 5.8 %collective-permute-start = (f32[64,2]{1,0:T(8,128)S(1)}, f32[64,2]{1,0:T(8,128)S(1)}, u32[]{:S(2)}, u32[]{:S(2)}) collective-permute-start(f32[64,2]{1,0:T(8,128)S(1)} %slice.47), channel_id=1, source_target_pairs={{0,16},{16,32},{32,48},{48,64},{64,80},{80,96},{96,112},{112,128},... | collective-permute-start | bytes 1544 | tf_op jit(solution)/shard_map/ppermute | solution.py:198
  82.4 1.0 copy-start.4
  88.6 5.3 %collective-permute-start.1 = (bf16[8,768,128]{2,1,0:T(8,128)(2,1)S(1)}, bf16[8,768,128]{2,1,0:T(8,128)(2,1)S(1)}, u32[]{:S(2)}, u32[]{:S(2)}) collective-permute-start(bf16[8,768,128]{2,1,0:T(8,128)(2,1)S(1)} %get-tuple-element.37), channel_id=1, source_target_pairs={{0,1},{1,0},{2,3},{3,2},{4,5},{5,4},{6,7},{7,6},{8,9},{9,8},{10,11... | collective-permute-start | bytes 4718600 | tf_op jit(solution)/shard_map/ppermute | solution.py:230
  96.3 98.4 %all-gather.8.cloned.1.call-start = ((), (), s32[]{:S(2)}) async-start(), calls=%async_computation.6 | async-start | bytes 1114112 | tf_op jit(solution)/shard_map/all_gather | solution.py:288
  96.3 62.2 %copy-start.2 = (bf16[128,2048]{1,0:T(8,128)(2,1)S(1)}, bf16[128,2048]{1,0:T(8,128)(2,1)}, u32[]{:S(2)}) copy-start(bf16[128,2048]{1,0:T(8,128)(2,1)} %cot_ref.3) | copy-start | bytes 1572868
  96.3 62.2 %copy-start.6 = (bf16[768,128]{1,0:T(8,128)(2,1)S(1)}, bf16[768,128]{1,0:T(8,128)(2,1)}, u32[]{:S(2)}) copy-start(bf16[768,128]{1,0:T(8,128)(2,1)} %get-tuple-element.50.select_ref) | copy-start | bytes 589828
  104.2 90.5 %copy-start.5 = (bf16[2048,64]{0,1:T(8,128)(2,1)S(1)}, bf16[2048,64]{0,1:T(8,128)(2,1)}, u32[]{:S(2)}) copy-start(bf16[2048,64]{0,1:T(8,128)(2,1)} %param.23) | copy-start | bytes 786436
  104.2 90.5 %copy-start.7 = (bf16[128,64]{0,1:T(8,128)(2,1)S(1)}, bf16[128,64]{0,1:T(8,128)(2,1)}, u32[]{:S(2)}) copy-start(bf16[128,64]{0,1:T(8,128)(2,1)} %param.19) | copy-start | bytes 49156
  158.5 46.2 %copy-start.8 = (bf16[128,64]{0,1:T(8,128)(2,1)S(1)}, bf16[128,64]{0,1:T(8,128)(2,1)}, u32[]{:S(2)}) copy-start(bf16[128,64]{0,1:T(8,128)(2,1)} %param.20) | copy-start | bytes 49156
  159.6 45.8 %copy-start.9 = (bf16[128,64]{0,1:T(8,128)(2,1)S(1)}, bf16[128,64]{0,1:T(8,128)(2,1)}, u32[]{:S(2)}) copy-start(bf16[128,64]{0,1:T(8,128)(2,1)} %param.21) | copy-start | bytes 49156
  174.7 11.4 %collective-permute-start.2 = (f32[32,128]{1,0:T(8,128)S(1)}, f32[32,128]{1,0:T(8,128)S(1)}, u32[]{:S(2)}, u32[]{:S(2)}) collective-permute-start(f32[32,128]{1,0:T(8,128)S(1)} %convert_reduce_fusion), channel_id=1, source_target_pairs={{0,0},{1,32},{2,64},{3,96},{4,128},{5,160},{6,192},{7,224},{8,256}... | collective-permute-start | bytes 49160 | tf_op jit(solution)/shard_map/ppermute | solution.py:305
  194.7 1.2 copy-start.3
  196.8 7.9 %collective-permute-start.3 = (f32[64,2]{1,0:T(8,128)S(1)}, f32[64,2]{1,0:T(8,128)S(1)}, u32[]{:S(2)}, u32[]{:S(2)}) collective-permute-start(f32[64,2]{1,0:T(8,128)S(1)} %bitcast.52), channel_id=1, source_target_pairs={{16,0},{32,16},{48,32},{64,48},{80,64},{96,80},{112,96},{128,112},... | collective-permute-start | bytes 1544 | tf_op jit(solution)/shard_map/ppermute | solution.py:296
Sparse Core Ops, SparseCore 0:
  37.0 45.2 all-gather.5
  96.4 42.2 reduce-scatter.1
  159.8 34.8 all-gather.7

commit v3 on v1

v3 whole, which is shorter than its diff:
```python
import functools

import jax
import jax.numpy as jnp
from jax import lax
from jax.experimental import pallas as pl
from jax.experimental.pallas import tpu as pltpu
from jax.sharding import Mesh, PartitionSpec as P

BF16, F32, I32 = jnp.bfloat16, jnp.float32, jnp.int32
TP = ("y", "c")
NT = (((1,), (1,)), ((), ()))
TN = (((0,), (0,)), ((), ()))
LANES = 128
VMEM = pl.BlockSpec(memory_space=pltpu.VMEM)


def mm(a, b, dims=None):
    if dims is None:
        return jnp.dot(a, b, preferred_element_type=F32)
    return lax.dot_general(a, b, dims, preferred_element_type=F32)


def call(body, out, cost, room=48 * 1024 * 1024, **kw):
    flops, moved = cost
    return pl.pallas_call(
        body,
        out_shape=out,
        cost_estimate=pl.CostEstimate(flops=flops, bytes_accessed=moved, transcendentals=0),
        compiler_params=pltpu.CompilerParams(vmem_limit_bytes=room),
        **kw,
    )


def shape(dims, kind):
    return jax.ShapeDtypeStruct(dims, kind)


def select_body(experts, capacity, at_ref, routes_ref, weights_ref, rows_ref, cot_ref, send_ref, select_ref):
    tokens = routes_ref.shape[1]
    number = lax.broadcasted_iota(I32, (experts, tokens), 0)
    first = routes_ref[0:1, :] == number
    second = routes_ref[1:2, :] == number
    hit = jnp.where(first | second, 1.0, 0.0).astype(F32)
    weight = jnp.where(first, weights_ref[0:1, :], jnp.where(second, weights_ref[1:2, :], 0.0))
    earlier = lax.broadcasted_iota(I32, (tokens, tokens), 0) < lax.broadcasted_iota(I32, (tokens, tokens), 1)
    place = mm(hit.astype(BF16), jnp.where(earlier, 1.0, 0.0).astype(BF16))
    place = jnp.where(hit > 0.0, place, -1.0)
    slot = lax.broadcasted_iota(I32, (capacity, tokens), 0).astype(F32)
    picked, scales = [], []
    for e in range(experts):
        one = jnp.where(slot == place[e : e + 1, :], 1.0, 0.0)
        scale = jnp.sum(one * weight[e : e + 1, :], axis=1, keepdims=True)
        picked += [one, one]
        scales += [scale, scale]
    select = jnp.concatenate(picked, axis=0).astype(BF16)
    scale = jnp.concatenate(scales, axis=0)
    select_ref[...] = select
    send_ref[:, :LANES] = mm(select, rows_ref[...]).astype(BF16)
    send_ref[:, LANES:] = (mm(select, cot_ref[...]) * scale).astype(BF16)


def expert_body(steps, got_ref, gate_ref, up_ref, down_ref, delta_ref, hidden_ref):
    rows = got_ref.shape[1]
    pre = jnp.zeros((rows, 2 * LANES), F32)
    back = jnp.zeros((rows, LANES), F32)
    for k in range(steps):
        ch = slice(k * 2 * LANES, (k + 1) * 2 * LANES)
        x = jnp.concatenate([got_ref[2 * k, :, :LANES], got_ref[2 * k + 1, :, :LANES]], axis=1)
        d = jnp.concatenate([got_ref[2 * k, :, LANES:], got_ref[2 * k + 1, :, LANES:]], axis=1)
        pre = pre + mm(x, jnp.concatenate([gate_ref[ch, :], up_ref[ch, :]], axis=1))
        back = back + mm(d, down_ref[:, ch], NT)
    gate, up = pre[:, :LANES], pre[:, LANES:]
    sigma = jax.nn.sigmoid(gate)
    silu = gate * sigma
    hidden_ref[...] = (silu * up).astype(BF16)
    delta_ref[:, :LANES] = (back * up * sigma * (1.0 + gate * (1.0 - sigma))).astype(BF16)
    delta_ref[:, LANES:] = (back * silu).astype(BF16)


def chip_body(steps, own_ref, partner_ref, own_weight_ref, partner_weight_ref, chip_ref):
    delta = jnp.concatenate([own_ref[...], partner_ref[...]], axis=1)
    for y in range(0, steps, 2):
        weight = [jnp.concatenate([own_weight_ref[k], partner_weight_ref[k]], axis=1) for k in (y, y + 1)]
        part = mm(delta, jnp.concatenate(weight, axis=0), NT).astype(BF16)
        chip_ref[y] = part[:, :LANES]
        chip_ref[y + 1] = part[:, LANES:]


def weight_body(got_ref, delta_ref, hidden_ref, gate_ref, up_ref, down_ref):
    x = jnp.concatenate([got_ref[0, :, :LANES], got_ref[1, :, :LANES]], axis=1)
    d = jnp.concatenate([got_ref[0, :, LANES:], got_ref[1, :, LANES:]], axis=1)
    grads = mm(x, delta_ref[...], TN)
    gate_ref[...] = grads[:, :LANES].astype(BF16)
    up_ref[...] = grads[:, LANES:].astype(BF16)
    down_ref[...] = mm(hidden_ref[...], d, TN).astype(BF16)


def token_body(at_ref, back_ref, select_ref, cot_ref, grad_ref):
    moe = mm(select_ref[...], back_ref[...], TN).astype(BF16)
    grad_ref[...] = (cot_ref[...].astype(F32) + moe.astype(F32)).astype(BF16)


def conv_body(steps, grads_ref, weight_ref, conv_ref, sum_ref, outer_ref, outer_grad_ref, scaled_ref, out_ref):
    total = jnp.zeros(sum_ref.shape, F32)
    half = conv_ref.shape[0] // 2
    low = lax.broadcasted_iota(I32, (half, LANES), 1) < LANES // 2
    for k in range(steps):
        g = jnp.concatenate([grads_ref[2 * k], grads_ref[2 * k + 1]], axis=1)
        total = total + mm(weight_ref[:, k * 2 * LANES : (k + 1) * 2 * LANES], g, NT)
        parts = mm(conv_ref[...], g)
        for t in range(2):
            top, bottom = (parts[r * half : (r + 1) * half, t * LANES : (t + 1) * LANES] for r in range(2))
            out_ref[4 * k + 2 * t] = jnp.where(low, top, pltpu.roll(bottom, LANES // 2, 1)).astype(BF16)
            out_ref[4 * k + 2 * t + 1] = jnp.where(low, pltpu.roll(top, LANES // 2, 1), bottom).astype(BF16)
    outer_grad_ref[...] = (total * sum_ref[...]).astype(BF16)
    scaled_ref[...] = total * outer_ref[...].astype(F32)


def out_body(tiles_ref, out_ref):
    total = tiles_ref[0].astype(F32)
    for s in range(1, tiles_ref.shape[0]):
        total = total + tiles_ref[s].astype(F32)
    half = LANES // 2
    out_ref[...] = jnp.concatenate([total[:, :half], total[:, half:]], axis=0).T


def per_device(
    cotangent,
    stream,
    routes,
    route_weights,
    gate_weight,
    up_weight,
    down_weight,
    outer_gate,
    inner_gate,
    conv_input,
    conv_taps,
    out_weight,
):
    groups = lax.axis_size("sp")
    ys = lax.axis_size("y")
    tps = 2 * ys
    experts = groups // 2
    tokens, width = stream.shape
    capacity = 3 * tokens // experts
    slots = groups * capacity
    units = gate_weight.shape[2]
    channels = outer_gate.shape[1]
    core = lax.axis_index("c").astype(I32).reshape(1)
    at = (2 * lax.axis_index("y") + lax.axis_index("c")).astype(I32).reshape(1)
    swap = [(0, 1), (1, 0)]

    block = pl.BlockSpec((tokens, LANES), lambda i, at: (0, at[0]))
    whole = lambda *dims: pl.BlockSpec(dims, lambda i, at: (0,) * len(dims))
    send, select = call(
        functools.partial(select_body, experts, capacity),
        (shape((slots, 2 * LANES), BF16), shape((slots, LANES), BF16)),
        (2 * slots * tokens * 2 * LANES, 2**20),
        room=67_043_328,
        grid_spec=pltpu.PrefetchScalarGridSpec(
            num_scalar_prefetch=1,
            grid=(1,),
            in_specs=[whole(2, tokens), whole(2, tokens), block, block],
            out_specs=[whole(slots, 2 * LANES), whole(slots, LANES)],
        ),
    )(at, routes.T, route_weights.T, stream, cotangent)
    recv = lax.all_to_all(
        send.reshape(groups, capacity, 2 * LANES), "sp", split_axis=0, concat_axis=0, tiled=True
    ).reshape(slots, 2 * LANES)

    outer_t, inner_t, input_t, taps_t = (a.T for a in (outer_gate, inner_gate, conv_input, conv_taps))
    recv, inner_t, gate_in, up_in = lax.optimization_barrier((recv, inner_t, gate_weight[0], up_weight[0]))
    got = lax.all_gather(recv, TP)
    by_core = jnp.concatenate([gate_in, up_in], axis=1).reshape(ys, 2, LANES, 2 * units)
    own_weight = lax.dynamic_index_in_dim(by_core, core[0], 1, keepdims=False)
    partner_weight = lax.ppermute(lax.dynamic_index_in_dim(by_core, 1 - core[0], 1, keepdims=False), "c", swap)
    outer_f, inner_f, input_f, taps = (a.astype(F32) for a in (outer_t, inner_t, input_t, taps_t))
    mixed = inner_f * input_f
    before = lax.ppermute(mixed[:, -2:], "sp", [(i - 1, i) for i in range(1, groups)])
    padded = jnp.concatenate([before, mixed], axis=1)
    conv_sum = taps[:, 0:1] * padded[:, :-2] + taps[:, 1:2] * padded[:, 1:-1] + taps[:, 2:3] * padded[:, 2:]
    conv_out = (outer_f * conv_sum).astype(BF16)
    got, conv_out, conv_sum, own_weight, partner_weight = lax.optimization_barrier(
        (got, conv_out, conv_sum, own_weight, partner_weight)
    )

    rows = 2 * LANES
    fixed = lambda *dims: pl.BlockSpec(dims, lambda i: (0,) * len(dims))
    delta_block = pl.BlockSpec((rows, 2 * units), lambda i: (i, 0))
    delta, hidden = call(
        functools.partial(expert_body, ys),
        (shape((slots, 2 * units), BF16), shape((slots, units), BF16)),
        (6 * slots * width * units, 2**24),
        grid=(slots // rows,),
        in_specs=[
            pl.BlockSpec((tps, rows, 2 * LANES), lambda i: (0, i, 0)),
            fixed(width, units),
            fixed(width, units),
            fixed(units, width),
        ],
        out_specs=[delta_block, pl.BlockSpec((rows, units), lambda i: (i, 0))],
    )(got, gate_weight[0], up_weight[0], down_weight[0])
    chip = call(
        functools.partial(chip_body, ys),
        shape((ys, slots, LANES), BF16),
        (4 * slots * width * units, 2**22),
        grid=(slots // rows,),
        in_specs=[delta_block, delta_block, fixed(ys, LANES, 2 * units), fixed(ys, LANES, 2 * units)],
        out_specs=pl.BlockSpec((ys, rows, LANES), lambda i: (0, i, 0)),
    )(delta, lax.ppermute(delta, "c", swap), own_weight, partner_weight)
    chip, delta = lax.optimization_barrier((chip, delta))
    half_sums = lax.psum_scatter(chip, "y", scatter_dimension=0)

    gate_grad, up_grad, down_grad = call(
        weight_body,
        (shape((width, units), BF16), shape((width, units), BF16), shape((units, width), BF16)),
        (6 * slots * width * units, 2**24),
        grid=(ys,),
        in_specs=[
            pl.BlockSpec((2, slots, 2 * LANES), lambda i: (i, 0, 0)),
            fixed(slots, 2 * units),
            fixed(slots, units),
        ],
        out_specs=[
            pl.BlockSpec((2 * LANES, units), lambda i: (i, 0)),
            pl.BlockSpec((2 * LANES, units), lambda i: (i, 0)),
            pl.BlockSpec((units, 2 * LANES), lambda i: (0, i)),
        ],
    )(got, delta, hidden)

    half_sums, gate_grad, up_grad, down_grad = lax.optimization_barrier((half_sums, gate_grad, up_grad, down_grad))
    returned = lax.all_to_all(
        half_sums.reshape(groups, capacity, LANES), "sp", split_axis=0, concat_axis=0, tiled=True
    )
    stream_block = call(
        token_body,
        shape((tokens, LANES), BF16),
        (2 * slots * tokens * LANES, 2**21),
        grid_spec=pltpu.PrefetchScalarGridSpec(
            num_scalar_prefetch=1,
            grid=(1,),
            in_specs=[whole(slots, LANES), whole(slots, LANES), block],
            out_specs=whole(tokens, LANES),
        ),
    )(at, returned.reshape(slots, LANES), select, cotangent)
    outer_grad, scaled, out_parts = call(
        functools.partial(conv_body, ys),
        (
            shape((channels, tokens), BF16),
            shape((channels, tokens), F32),
            shape((groups, channels // 2, LANES), BF16),
        ),
        (4 * tokens * width * channels, 2**20),
        in_specs=[VMEM] * 5,
        out_specs=[VMEM] * 3,
    )(lax.all_gather(stream_block, TP), out_weight.T, conv_out, conv_sum, outer_t)
    out_tiles = lax.all_to_all(out_parts, "sp", split_axis=0, concat_axis=0, tiled=True)
    out_grad = call(
        out_body,
        shape((channels, width // groups), F32),
        (2**17, 2**19),
        in_specs=[VMEM],
        out_specs=VMEM,
    )(out_tiles)
    later = lax.ppermute(scaled[:, :2], "sp", [(i, i - 1) for i in range(1, groups)])
    extended = jnp.concatenate([scaled, later], axis=1)
    mixed_grad = taps[:, 2:3] * extended[:, :-2] + taps[:, 1:2] * extended[:, 1:-1] + taps[:, 0:1] * extended[:, 2:]
    inner_grad = (mixed_grad * input_f).astype(BF16)
    input_grad = (mixed_grad * inner_f).astype(BF16)
    return (gate_grad[None], up_grad[None], down_grad[None], out_grad, outer_grad.T, inner_grad.T, input_grad.T)


def solution(mesh):
    groups, tps = mesh.devices.shape
    fine = Mesh(mesh.devices.reshape(groups, tps // 2, 2), ("sp", "y", "c"))
    placed = (
        P("sp", None),
        P("sp", None),
        P("sp", None),
        P("sp", None),
        P("sp", None, TP),
        P("sp", None, TP),
        P("sp", TP, None),
        P("sp", TP),
        P("sp", TP),
        P("sp", TP),
        P(None, TP),
        P(None, TP),
    )
    return jax.shard_map(
        per_device,
        mesh=fine,
        in_specs=placed,
        out_specs=(
            P("sp", None, TP),
            P("sp", None, TP),
            P("sp", TP, None),
            P("sp", TP),
            P("sp", TP),
            P("sp", TP),
            P("sp", TP),
        ),
        check_vma=False,
    )
```

time: 231 us -> 204 us (0.88)
  waiting for transfers between devices: 99.9 us -> 82.7 us
  starting transfers between devices: 30.7 us -> 18 us
  blocking collectives: 59.9 us -> 64.4 us
  local copies, waits for them, and re-layouts: 4.33 us -> 0.23 us
  Pallas kernels: 16.2 us -> 19.2 us
    all_to_all x0 -> x1, blocking collectives: none -> 19.8 us  [per_device(): lax.all_to_all(half_sums.reshape(groups, capacity, LANES), 'sp', split_ax...]
    all_gather x2 -> x1, blocking collectives: 32.4 us -> 17 us  [per_device(): lax.all_gather(stream_block, TP)]
    all_to_all x1 -> x0, starting transfers between devices: 10.5 us -> none  [per_device(): lax.all_to_all(half_sums.reshape(groups, capacity, LANES), 'sp', split_ax...]
    all_gather x1, waiting for transfers between devices: 45.4 us -> 35.2 us  [per_device(): got = lax.all_gather(recv, TP)]
    ppermute x2, waiting for transfers between devices: 11.7 us -> 1.46 us  [the longest x1 1.46 us: per_device(): lax.ppermute(delta, 'c', swap)]
    all_to_all x1, waiting for transfers between devices: 0.01 us -> 10.1 us  [per_device(): lax.all_to_all(out_parts, 'sp', split_axis=0, concat_axis=0, tiled=True)]
    ppermute x1, waiting for transfers between devices: 5.13 us -> 0.01 us  [per_device(): lax.ppermute(scaled[:, :2], 'sp', [(i, i - 1) for i in range(1, groups)])]
    unnamed x27 -> x19, local copies, waits for them, and re-layouts: 4.18 us -> 0.05 us
  transfers between devices with their start and end apart: 8 -> 7, of which waited for: 5 -> 5; matrix products, arithmetic and copies ran while one was open for 1% -> 2% of each run, Pallas kernels for 4% -> 4%
where the time goes in v3:
time: 204 us; the launch traced here: 202 us
  waiting for transfers between devices  82.7 us (41%)
  blocking collectives  64.4 us (32%)
  Pallas kernels  19.2 us (9%)
  starting transfers between devices  18 us (9%)
  between operations  14.2 us (7%)
  other arithmetic  3.58 us (2%)
    all_gather x1, waiting for transfers between devices, per_device(): got = lax.all_gather(recv, TP)  35.2 us
    reduce_scatter x1, waiting for transfers between devices, per_device(): half_sums = lax.psum_scatter(chip, 'y', scatter_dimension=0)  34.2 us
    all_to_all x1, blocking collectives, per_device(): lax.all_to_all(send.reshape(groups, capacity, 2 * LANES), 'sp', split_axi...  27.5 us
    all_to_all x1, blocking collectives, per_device(): lax.all_to_all(half_sums.reshape(groups, capacity, LANES), 'sp', split_ax...  19.8 us
    all_gather x1, blocking collectives, per_device(): lax.all_gather(stream_block, TP)  17 us
    all_to_all x1, waiting for transfers between devices, per_device(): lax.all_to_all(out_parts, 'sp', split_axis=0, concat_axis=0, tiled=True)  10.1 us
    pallas_call x1, Pallas kernels, per_device(): call(weight_body, (shape((width, units), BF16), shape((width, units), BF1...  7.83 us
    all_to_all x1, starting transfers between devices, per_device(): lax.all_to_all(out_parts, 'sp', split_axis=0, concat_axis=0, tiled=True)  7.26 us
  transfers between devices with their start and end apart: 7, of which 5 were waited for; matrix products, arithmetic and copies ran while one was open for 2% of the time, Pallas kernels for 4%

profile of v3, /device:TPU:6, one launch (start us, length us, event | category | flops | bytes accessed | tf_op | source)
XLA Modules:
  0.0 202.3 jit_solution(17861515924818689523)
XLA Ops:
  7.2 0.0 all-gather.4.cloned.1.call-start
  7.2 2.0 shard_map.171
  9.2 27.5 %all_to_all.15 = bf16[32,24,256]{2,1,0:T(8,128)(2,1)} all-to-all(bf16[32,24,256]{2,1,0:T(8,128)(2,1)} %bitcast.64), channel_id=1, replica_groups=mesh['sp'=32,'y'=8,'c'=2] {'sp'}, dimensions={0} | all-to-all | bytes 786432 | tf_op jit(solution)/shard_map/all_to_all | solution.py:169
  36.7 0.0 all-gather.4.cloned.1.call-update
  36.8 0.0 reduce-scatter.2.cloned.1.call-start
  36.8 0.7 convert_bitcast_fusion
  37.5 0.0 copy-start.7
  37.5 0.0 copy-start.8
  37.5 0.0 copy-start.6
  37.5 0.0 copy-start.1
  37.5 0.0 copy-start.2
  37.5 0.0 copy-start.3
  37.5 1.4 pad_maximum_fusion
  39.0 0.1 dynamic-slice_bitcast_fusion
  39.1 1.9 collective-permute-start.1
  41.0 0.0 copy-done.7
  41.0 0.0 copy-done.8
  41.0 0.1 slice.39
  41.1 4.1 %collective-permute-start = (f32[64,2]{1,0:T(8,128)S(1)}, f32[64,2]{1,0:T(8,128)S(1)}, u32[]{:S(2)}, u32[]{:S(2)}) collective-permute-start(f32[64,2]{1,0:T(8,128)S(1)} %slice.39), channel_id=1, source_target_pairs={{0,16},{16,32},{32,48},{48,64},{64,80},{80,96},{96,112},{112,128},... | collective-permute-start | bytes 1544 | tf_op jit(solution)/shard_map/ppermute | solution.py:181
  45.2 1.7 collective-permute-done
  46.9 0.0 copy-done.6
  46.9 0.1 multiply_convert_fusion
  47.0 0.0 collective-permute-done.1.partner_weight_ref
  47.1 35.2 %all-gather.4.cloned.1.call-done = bf16[12288,256]{1,0:T(8,128)(2,1)} async-done(((bf16[768,256]{1,0:T(8,128)(2,1)}), bf16[12288,256]{1,0:T(8,128)(2,1)}) %all-gather.4.cloned.1.call-update) | async-done | bytes 6291472 | tf_op jit(solution)/shard_map/all_gather | solution.py:175
  82.2 0.0 copy-done.1
  82.2 0.0 copy-done.2
  82.2 0.0 copy-done.3
  82.2 4.6 %shard_map.172 = (bf16[768,256]{1,0:T(8,128)(2,1)S(1)}, bf16[768,128]{1,0:T(8,128)(2,1)S(1)}) custom-call(bf16[16,768,256]{2,1,0:T(8,128)(2,1)} %bitcast.60, bf16[2048,128]{1,0:T(8,128)(2,1)S(1)} %bitcast.52, bf16[2048,128]{1,0:T(8,128)(2,1)S(1)} %bitcast.54, bf16[128,2048]{1,0:T(8,128)(2,1)S(1)} %bitcast.56), custom_call_target="tpu_custom_call" | custom-call | flops 1207959552 | bytes 16777216 | tf_op jit(solution)/shard_map/pallas_call | solution.py:192
  86.9 2.1 %collective-permute-start.2 = (bf16[768,256]{1,0:T(8,128)(2,1)S(1)}, bf16[768,256]{1,0:T(8,128)(2,1)S(1)}, u32[]{:S(2)}, u32[]{:S(2)}) collective-permute-start(bf16[768,256]{1,0:T(8,128)(2,1)S(1)} %get-tuple-element.42.own_ref.delta_ref), channel_id=1, source_target_pairs={{0,1},{1,0},{2,3},{3,2},{4,5},{5,4},{6,7},{7,6},{8,9},{9,8},{10,11... | collective-permute-start | bytes 1179656 | tf_op jit(solution)/shard_map/ppermute | solution.py:212
  89.0 1.5 collective-permute-done.2.partner_ref
  90.5 2.5 %shard_map.173 = bf16[8,768,128]{2,1,0:T(8,128)(2,1)} custom-call(bf16[768,256]{1,0:T(8,128)(2,1)S(1)} %get-tuple-element.42.own_ref.delta_ref, bf16[768,256]{1,0:T(8,128)(2,1)S(1)} %collective-permute-done.2.partner_ref, bf16[8,128,256]{2,1,0:T(8,128)(2,1)S(1)} %get-tuple-element.39.own_weight_ref, ...), custom_call_target="tpu_custom_call" | custom-call | flops 805306368 | bytes 4194304 | tf_op jit(solution)/shard_map/pallas_call | solution.py:205
  93.1 0.0 reduce-scatter.2.cloned.1.call-update
  93.1 0.0 copy-start
  93.1 0.0 copy-start.5
  93.1 7.8 %shard_map.174 = (bf16[2048,128]{1,0:T(8,128)(2,1)}, bf16[2048,128]{1,0:T(8,128)(2,1)}, bf16[128,2048]{1,0:T(8,128)(2,1)}) custom-call(bf16[16,768,256]{2,1,0:T(8,128)(2,1)} %bitcast.61, bf16[768,256]{1,0:T(8,128)(2,1)S(1)} %get-tuple-element.42.own_ref.delta_ref, bf16[768,128]{1,0:T(8,128)(2,1)S(1)} %get-tuple-element.43.hidden_ref), custom_call_target="tpu_custom_call" | custom-call | flops 1207959552 | bytes 16777216 | tf_op jit(solution)/shard_map/pallas_call | solution.py:216
  100.9 0.0 copy-start.4
  100.9 34.2 %reduce-scatter.2.cloned.1.call-done = bf16[1,768,128]{2,1,0:T(8,128)(2,1)} async-done(((bf16[8,768,128]{2,1,0:T(8,128)(2,1)}), bf16[1,768,128]{2,1,0:T(8,128)(2,1)}) %reduce-scatter.2.cloned.1.call-update) | async-done | bytes 196624 | tf_op jit(solution)/shard_map/reduce_scatter | solution.py:214
  135.1 19.8 %all_to_all.16 = bf16[32,24,128]{2,1,0:T(8,128)(2,1)S(1)} all-to-all(bf16[32,24,128]{2,1,0:T(8,128)(2,1)} %bitcast.65), channel_id=1, replica_groups=mesh['sp'=32,'y'=8,'c'=2] {'sp'}, dimensions={0} | all-to-all | bytes 393216 | tf_op jit(solution)/shard_map/all_to_all | solution.py:234
  155.0 0.0 copy-done
  155.0 0.0 copy-done.5
  155.0 0.3 shard_map.175
  155.2 17.0 %all-gather.1 = bf16[2048,128]{1,0:T(8,128)(2,1)S(1)} all-gather(bf16[128,128]{1,0:T(8,128)(2,1)S(1)} %shard_map.175), channel_id=3, replica_groups=mesh['sp'=32,'y'=8,'c'=2] {'y','c'}, dimensions={0}, use_global_device_ids=true | all-gather | bytes 557056 | tf_op jit(solution)/shard_map/all_gather | solution.py:258
  172.2 0.0 copy-done.4
  172.2 1.1 shard_map.176
  173.4 2.5 %collective-permute-start.3 = (f32[64,2]{1,0:T(8,128)S(1)}, f32[64,2]{1,0:T(8,128)S(1)}, u32[]{:S(2)}, u32[]{:S(2)}) collective-permute-start(f32[64,2]{1,0:T(8,128)S(1)} %bitcast.58), channel_id=1, source_target_pairs={{16,0},{32,16},{48,32},{64,48},{80,64},{96,80},{112,96},{128,112},... | collective-permute-start | bytes 1544 | tf_op jit(solution)/shard_map/ppermute | solution.py:267
  175.9 7.3 %all-to-all-start.2 = ((bf16[32,32,128]{2,1,0:T(8,128)(2,1)}), bf16[32,32,128]{2,1,0:T(8,128)(2,1)S(1)}, u32[]{:S(2)}, u32[]{:S(2)}) async-start(bf16[32,32,128]{2,1,0:T(8,128)(2,1)} %get-tuple-element.54), calls=%async_computation.3 | async-start | bytes 524288 | tf_op jit(solution)/shard_map/all_to_all | solution.py:259
  183.2 0.0 collective-permute-done.3
  183.2 0.7 fusion.10
  183.9 0.6 fusion.9
  184.5 10.1 %all-to-all-done.2.tiles_ref = bf16[32,32,128]{2,1,0:T(8,128)(2,1)S(1)} async-done(((bf16[32,32,128]{2,1,0:T(8,128)(2,1)}), bf16[32,32,128]{2,1,0:T(8,128)(2,1)S(1)}, u32[]{:S(2)}, u32[]{:S(2)}) %all-to-all-start.2) | async-done | bytes 262176 | tf_op jit(solution)/shard_map/all_to_all | solution.py:259
  194.6 0.8 shard_map.177
  (4 shorter events, 0.0 us)
Async XLA Ops:
  7.2 75.1 %all-gather.4.cloned.1.call-start = ((), (), s32[]{:S(2)}) async-start(), calls=%async_computation.5 | async-start | bytes 6684672 | tf_op jit(solution)/shard_map/all_gather | solution.py:175
  36.8 98.4 %reduce-scatter.2.cloned.1.call-start = ((), (), s32[]{:S(2)}) async-start(), calls=%async_computation.4 | async-start | bytes 1769472 | tf_op jit(solution)/shard_map/reduce_scatter | solution.py:214
  37.5 3.5 %copy-start.7 = (bf16[128,64]{0,1:T(8,128)(2,1)S(1)}, bf16[128,64]{0,1:T(8,128)(2,1)}, u32[]{:S(2)}) copy-start(bf16[128,64]{0,1:T(8,128)(2,1)} %param.20) | copy-start | bytes 49156
  37.5 3.5 %copy-start.8 = (bf16[128,64]{0,1:T(8,128)(2,1)S(1)}, bf16[128,64]{0,1:T(8,128)(2,1)}, u32[]{:S(2)}) copy-start(bf16[128,64]{0,1:T(8,128)(2,1)} %param.21) | copy-start | bytes 49156
  37.5 9.4 %copy-start.6 = (bf16[128,64]{0,1:T(8,128)(2,1)S(1)}, bf16[128,64]{0,1:T(8,128)(2,1)}, u32[]{:S(2)}) copy-start(bf16[128,64]{0,1:T(8,128)(2,1)} %param.19) | copy-start | bytes 49156
  37.5 44.7 %copy-start.1 = (bf16[1,2048,128]{2,1,0:T(8,128)(2,1)S(1)}, bf16[1,2048,128]{2,1,0:T(8,128)(2,1)}, u32[]{:S(2)}) copy-start(bf16[1,2048,128]{2,1,0:T(8,128)(2,1)} %param.16) | copy-start | bytes 1572868
  37.5 44.7 %copy-start.2 = (bf16[1,2048,128]{2,1,0:T(8,128)(2,1)S(1)}, bf16[1,2048,128]{2,1,0:T(8,128)(2,1)}, u32[]{:S(2)}) copy-start(bf16[1,2048,128]{2,1,0:T(8,128)(2,1)} %param.17) | copy-start | bytes 1572868
  37.5 44.7 %copy-start.3 = (bf16[1,128,2048]{2,1,0:T(8,128)(2,1)S(1)}, bf16[1,128,2048]{2,1,0:T(8,128)(2,1)}, u32[]{:S(2)}) copy-start(bf16[1,128,2048]{2,1,0:T(8,128)(2,1)} %param.18) | copy-start | bytes 1572868
  39.1 8.0 %collective-permute-start.1 = (bf16[8,128,256]{2,1,0:T(8,128)(2,1)S(1)}, bf16[8,128,256]{2,1,0:T(8,128)(2,1)S(1)}, u32[]{:S(2)}, u32[]{:S(2)}) collective-permute-start(bf16[8,128,256]{2,1,0:T(8,128)(2,1)S(1)} %get-tuple-element.61), channel_id=1, source_target_pairs={{0,1},{1,0},{2,3},{3,2},{4,5},{5,4},{6,7},{7,6},{8,9},{9,8},{10,11... | collective-permute-start | bytes 1572872 | tf_op jit(solution)/shard_map/ppermute | solution.py:178
  41.1 5.8 %collective-permute-start = (f32[64,2]{1,0:T(8,128)S(1)}, f32[64,2]{1,0:T(8,128)S(1)}, u32[]{:S(2)}, u32[]{:S(2)}) collective-permute-start(f32[64,2]{1,0:T(8,128)S(1)} %slice.39), channel_id=1, source_target_pairs={{0,16},{16,32},{32,48},{48,64},{64,80},{80,96},{96,112},{112,128},... | collective-permute-start | bytes 1544 | tf_op jit(solution)/shard_map/ppermute | solution.py:181
  86.9 3.6 %collective-permute-start.2 = (bf16[768,256]{1,0:T(8,128)(2,1)S(1)}, bf16[768,256]{1,0:T(8,128)(2,1)S(1)}, u32[]{:S(2)}, u32[]{:S(2)}) collective-permute-start(bf16[768,256]{1,0:T(8,128)(2,1)S(1)} %get-tuple-element.42.own_ref.delta_ref), channel_id=1, source_target_pairs={{0,1},{1,0},{2,3},{3,2},{4,5},{5,4},{6,7},{7,6},{8,9},{9,8},{10,11... | collective-permute-start | bytes 1179656 | tf_op jit(solution)/shard_map/ppermute | solution.py:212
  93.1 61.9 %copy-start = (bf16[128,2048]{1,0:T(8,128)(2,1)S(1)}, bf16[128,2048]{1,0:T(8,128)(2,1)}, u32[]{:S(2)}) copy-start(bf16[128,2048]{1,0:T(8,128)(2,1)} %cot_ref.3) | copy-start | bytes 1572868
  93.1 61.9 %copy-start.5 = (bf16[768,128]{1,0:T(8,128)(2,1)S(1)}, bf16[768,128]{1,0:T(8,128)(2,1)}, u32[]{:S(2)}) copy-start(bf16[768,128]{1,0:T(8,128)(2,1)} %get-tuple-element.51.select_ref) | copy-start | bytes 589828
  100.9 71.3 %copy-start.4 = (bf16[2048,64]{0,1:T(8,128)(2,1)S(1)}, bf16[2048,64]{0,1:T(8,128)(2,1)}, u32[]{:S(2)}) copy-start(bf16[2048,64]{0,1:T(8,128)(2,1)} %param.23) | copy-start | bytes 786436
  173.4 9.8 %collective-permute-start.3 = (f32[64,2]{1,0:T(8,128)S(1)}, f32[64,2]{1,0:T(8,128)S(1)}, u32[]{:S(2)}, u32[]{:S(2)}) collective-permute-start(f32[64,2]{1,0:T(8,128)S(1)} %bitcast.58), channel_id=1, source_target_pairs={{16,0},{32,16},{48,32},{64,48},{80,64},{96,80},{112,96},{128,112},... | collective-permute-start | bytes 1544 | tf_op jit(solution)/shard_map/ppermute | solution.py:267
  175.9 18.7 %all-to-all-start.2 = ((bf16[32,32,128]{2,1,0:T(8,128)(2,1)}), bf16[32,32,128]{2,1,0:T(8,128)(2,1)S(1)}, u32[]{:S(2)}, u32[]{:S(2)}) async-start(bf16[32,32,128]{2,1,0:T(8,128)(2,1)} %get-tuple-element.54), calls=%async_computation.3 | async-start | bytes 524288 | tf_op jit(solution)/shard_map/all_to_all | solution.py:259
Sparse Core Ops, SparseCore 0:
  36.9 45.3 all-gather.3
  93.2 41.8 reduce-scatter.1

commit v4 on v3

--- a/solution.py
+++ b/solution.py
@@ -60,31 +60,43 @@
     send_ref[:, LANES:] = (mm(select, cot_ref[...]) * scale).astype(BF16)
 
 
-def expert_body(steps, got_ref, gate_ref, up_ref, down_ref, delta_ref, hidden_ref):
-    rows = got_ref.shape[1]
-    pre = jnp.zeros((rows, 2 * LANES), F32)
-    back = jnp.zeros((rows, LANES), F32)
-    for k in range(steps):
-        ch = slice(k * 2 * LANES, (k + 1) * 2 * LANES)
-        x = jnp.concatenate([got_ref[2 * k, :, :LANES], got_ref[2 * k + 1, :, :LANES]], axis=1)
-        d = jnp.concatenate([got_ref[2 * k, :, LANES:], got_ref[2 * k + 1, :, LANES:]], axis=1)
-        pre = pre + mm(x, jnp.concatenate([gate_ref[ch, :], up_ref[ch, :]], axis=1))
-        back = back + mm(d, down_ref[:, ch], NT)
-    gate, up = pre[:, :LANES], pre[:, LANES:]
-    sigma = jax.nn.sigmoid(gate)
-    silu = gate * sigma
-    hidden_ref[...] = (silu * up).astype(BF16)
-    delta_ref[:, :LANES] = (back * up * sigma * (1.0 + gate * (1.0 - sigma))).astype(BF16)
-    delta_ref[:, LANES:] = (back * silu).astype(BF16)
-
-
-def chip_body(steps, own_ref, partner_ref, own_weight_ref, partner_weight_ref, chip_ref):
-    delta = jnp.concatenate([own_ref[...], partner_ref[...]], axis=1)
-    for y in range(0, steps, 2):
-        weight = [jnp.concatenate([own_weight_ref[k], partner_weight_ref[k]], axis=1) for k in (y, y + 1)]
-        part = mm(delta, jnp.concatenate(weight, axis=0), NT).astype(BF16)
-        chip_ref[y] = part[:, :LANES]
-        chip_ref[y + 1] = part[:, LANES:]
+def layout_body(core_ref, gate_ref, up_ref, down_ref, gate2_ref, up2_ref, down2_ref, fore_ref, back_ref, rows_ref):
+    for i, ref in enumerate((gate_ref, up_ref, gate2_ref, up2_ref)):
+        fore_ref[:, i * LANES : (i + 1) * LANES] = ref[...]
+    for k in range(back_ref.shape[0] // LANES):
+        at = slice(k * LANES, (k + 1) * LANES)
+        back_ref[at, :LANES] = down_ref[:, at].astype(F32).T.astype(BF16)
+        back_ref[at, LANES:] = down2_ref[:, at].astype(F32).T.astype(BF16)
+    for y in range(2 * rows_ref.shape[0]):
+        at = pl.ds(pl.multiple_of((2 * y + core_ref[0]) * LANES, LANES), LANES)
+        to = slice(y % 2 * LANES, (y % 2 + 1) * LANES)
+        for i, ref in enumerate((gate_ref, up_ref, gate2_ref, up2_ref)):
+            rows_ref[y // 2, i * LANES : (i + 1) * LANES, to] = ref[at, :].astype(F32).T.astype(BF16)
+
+
+def expert_body(count, got_ref, fore_ref, back_ref, rows_ref, delta_ref, hidden_ref, chip_ref):
+    x = jnp.concatenate([got_ref[t, :, :LANES] for t in range(count)], axis=1)
+    pre = mm(x, fore_ref[...])
+    d = jnp.concatenate([got_ref[t, :, LANES:] for t in range(count)], axis=1)
+    back = mm(d, back_ref[...])
+    deltas = []
+    for i in range(2):
+        gate = pre[:, 2 * i * LANES : (2 * i + 1) * LANES]
+        up = pre[:, (2 * i + 1) * LANES : (2 * i + 2) * LANES]
+        grad = back[:, i * LANES : (i + 1) * LANES]
+        sigma = jax.nn.sigmoid(gate)
+        silu = gate * sigma
+        if i == 0:
+            hidden_ref[...] = (silu * up).astype(BF16)
+        deltas.append((grad * up * sigma * (1.0 + gate * (1.0 - sigma))).astype(BF16))
+        deltas.append((grad * silu).astype(BF16))
+    delta_ref[:, :LANES] = deltas[0]
+    delta_ref[:, LANES:] = deltas[1]
+    delta = jnp.concatenate(deltas, axis=1)
+    for k in range(count // 4):
+        part = mm(delta, rows_ref[k]).astype(BF16)
+        chip_ref[2 * k] = part[:, :LANES]
+        chip_ref[2 * k + 1] = part[:, LANES:]
 
 
 def weight_body(got_ref, delta_ref, hidden_ref, gate_ref, up_ref, down_ref):
@@ -171,45 +183,43 @@
     ).reshape(slots, 2 * LANES)
 
     outer_t, inner_t, input_t, taps_t = (a.T for a in (outer_gate, inner_gate, conv_input, conv_taps))
-    recv, inner_t, gate_in, up_in = lax.optimization_barrier((recv, inner_t, gate_weight[0], up_weight[0]))
+    weights = (gate_weight[0], up_weight[0], down_weight[0])
+    recv, inner_t, *held = lax.optimization_barrier((recv, inner_t, *weights))
     got = lax.all_gather(recv, TP)
-    by_core = jnp.concatenate([gate_in, up_in], axis=1).reshape(ys, 2, LANES, 2 * units)
-    own_weight = lax.dynamic_index_in_dim(by_core, core[0], 1, keepdims=False)
-    partner_weight = lax.ppermute(lax.dynamic_index_in_dim(by_core, 1 - core[0], 1, keepdims=False), "c", swap)
+    laid = call(
+        layout_body,
+        (shape((width, 4 * units), BF16), shape((width, 2 * units), BF16), shape((ys // 2, 4 * units, 2 * LANES), BF16)),
+        (2**22, 2**23),
+        in_specs=[pl.BlockSpec(memory_space=pltpu.SMEM)] + [VMEM] * 6,
+        out_specs=[VMEM] * 3,
+    )(core, *held, *(lax.ppermute(a, "c", swap) for a in held))
     outer_f, inner_f, input_f, taps = (a.astype(F32) for a in (outer_t, inner_t, input_t, taps_t))
     mixed = inner_f * input_f
     before = lax.ppermute(mixed[:, -2:], "sp", [(i - 1, i) for i in range(1, groups)])
     padded = jnp.concatenate([before, mixed], axis=1)
     conv_sum = taps[:, 0:1] * padded[:, :-2] + taps[:, 1:2] * padded[:, 1:-1] + taps[:, 2:3] * padded[:, 2:]
     conv_out = (outer_f * conv_sum).astype(BF16)
-    got, conv_out, conv_sum, own_weight, partner_weight = lax.optimization_barrier(
-        (got, conv_out, conv_sum, own_weight, partner_weight)
-    )
+    got, conv_out, conv_sum, laid = lax.optimization_barrier((got, conv_out, conv_sum, laid))
 
     rows = 2 * LANES
     fixed = lambda *dims: pl.BlockSpec(dims, lambda i: (0,) * len(dims))
-    delta_block = pl.BlockSpec((rows, 2 * units), lambda i: (i, 0))
-    delta, hidden = call(
-        functools.partial(expert_body, ys),
-        (shape((slots, 2 * units), BF16), shape((slots, units), BF16)),
-        (6 * slots * width * units, 2**24),
+    delta, hidden, chip = call(
+        functools.partial(expert_body, tps),
+        (shape((slots, 2 * units), BF16), shape((slots, units), BF16), shape((ys, slots, LANES), BF16)),
+        (16 * slots * width * units, 2**24),
         grid=(slots // rows,),
         in_specs=[
             pl.BlockSpec((tps, rows, 2 * LANES), lambda i: (0, i, 0)),
-            fixed(width, units),
-            fixed(width, units),
-            fixed(units, width),
+            fixed(width, 4 * units),
+            fixed(width, 2 * units),
+            fixed(ys // 2, 4 * units, 2 * LANES),
         ],
-        out_specs=[delta_block, pl.BlockSpec((rows, units), lambda i: (i, 0))],
-    )(got, gate_weight[0], up_weight[0], down_weight[0])
-    chip = call(
-        functools.partial(chip_body, ys),
-        shape((ys, slots, LANES), BF16),
-        (4 * slots * width * units, 2**22),
-        grid=(slots // rows,),
-        in_specs=[delta_block, delta_block, fixed(ys, LANES, 2 * units), fixed(ys, LANES, 2 * units)],
-        out_specs=pl.BlockSpec((ys, rows, LANES), lambda i: (0, i, 0)),
-    )(delta, lax.ppermute(delta, "c", swap), own_weight, partner_weight)
+        out_specs=[
+            pl.BlockSpec((rows, 2 * units), lambda i: (i, 0)),
+            pl.BlockSpec((rows, units), lambda i: (i, 0)),
+            pl.BlockSpec((ys, rows, LANES), lambda i: (0, i, 0)),
+        ],
+    )(got, *laid)
     chip, delta = lax.optimization_barrier((chip, delta))
     half_sums = lax.psum_scatter(chip, "y", scatter_dimension=0)
 

time: 204 us -> 202 us (level)
  waiting for transfers between devices: 82.7 us -> 71.5 us
  Pallas kernels: 19.2 us -> 23 us
  local copies, waits for them, and re-layouts: 0.23 us -> 3.24 us
  starting transfers between devices: 18 us -> 20.1 us
    all_gather x1, waiting for transfers between devices: 35.2 us -> 25.5 us  [per_device(): got = lax.all_gather(recv, TP)]
    pallas_call x2, Pallas kernels: 7.2 us -> 11 us  [the longest x1 8.66 us: per_device(): call(functools.partial(expert_body, tps), (shape((slots, 2 * units), BF16...]
    unnamed x19, local copies, waits for them, and re-layouts: 0.05 us -> 3.15 us
    ppermute x2 -> x3, starting transfers between devices: 4.07 us -> 6.24 us  [per_device(): lax.ppermute(a, 'c', swap)]
  transfers between devices with their start and end apart: 7 -> 8, of which waited for: 5 -> 4; matrix products, arithmetic and copies ran while one was open for 2% -> 2% of each run, Pallas kernels for 4% -> 5%
where the time goes in v4:
time: 202 us; the launch traced here: 200 us
  waiting for transfers between devices  71.5 us (35%)
  blocking collectives  64.4 us (32%)
  Pallas kernels  23 us (11%)
  starting transfers between devices  20.1 us (10%)
  between operations  14.2 us (7%)
  other arithmetic  3.59 us (2%)
  local copies, waits for them, and re-layouts  3.24 us (2%)
    reduce_scatter x1, waiting for transfers between devices, per_device(): half_sums = lax.psum_scatter(chip, 'y', scatter_dimension=0)  34.1 us
    all_to_all x1, blocking collectives, per_device(): lax.all_to_all(send.reshape(groups, capacity, 2 * LANES), 'sp', split_axi...  27.5 us
    all_gather x1, waiting for transfers between devices, per_device(): got = lax.all_gather(recv, TP)  25.5 us
    all_to_all x1, blocking collectives, per_device(): lax.all_to_all(half_sums.reshape(groups, capacity, LANES), 'sp', split_ax...  19.8 us
    all_gather x1, blocking collectives, per_device(): lax.all_gather(stream_block, TP)  17.1 us
    all_to_all x1, waiting for transfers between devices, per_device(): lax.all_to_all(out_parts, 'sp', split_axis=0, concat_axis=0, tiled=True)  10.1 us
    pallas_call x1, Pallas kernels, per_device(): call(functools.partial(expert_body, tps), (shape((slots, 2 * units), BF16...  8.66 us
    pallas_call x1, Pallas kernels, per_device(): call(weight_body, (shape((width, units), BF16), shape((width, units), BF1...  7.83 us
  transfers between devices with their start and end apart: 8, of which 4 were waited for; matrix products, arithmetic and copies ran while one was open for 2% of the time, Pallas kernels for 5%

profile of v4, /device:TPU:6, one launch (start us, length us, event | category | flops | bytes accessed | tf_op | source)
XLA Modules:
  0.0 200.1 jit_solution(4307556854702542822)
XLA Ops:
  7.2 0.0 all-gather.4.cloned.1.call-start
  7.2 2.0 shard_map.171
  9.2 27.5 %all_to_all.15 = bf16[32,24,256]{2,1,0:T(8,128)(2,1)} all-to-all(bf16[32,24,256]{2,1,0:T(8,128)(2,1)} %bitcast.56), channel_id=1, replica_groups=mesh['sp'=32,'y'=8,'c'=2] {'sp'}, dimensions={0} | all-to-all | bytes 786432 | tf_op jit(solution)/shard_map/all_to_all | solution.py:181
  36.7 0.0 all-gather.4.cloned.1.call-update
  36.8 0.0 reduce-scatter.2.cloned.1.call-start
  36.8 0.7 convert_bitcast_fusion
  37.5 1.9 collective-permute-start.1
  39.4 2.4 %collective-permute-start.2 = (bf16[2048,128]{1,0:T(8,128)(2,1)}, bf16[2048,128]{1,0:T(8,128)(2,1)S(1)}, u32[]{:S(2)}, u32[]{:S(2)}) collective-permute-start(bf16[2048,128]{1,0:T(8,128)(2,1)} %bitcast.46), channel_id=1, source_target_pairs={{0,1},{1,0},{2,3},{3,2},{4,5},{5,4},{6,7},{7,6},{8,9},{9,8},{10,11... | collective-permute-start | bytes 1572872 | tf_op jit(solution)/shard_map/ppermute | solution.py:195
  41.8 1.9 collective-permute-start.3
  43.8 0.7 convert_multiply_fusion.1
  44.5 0.1 slice.39
  44.6 4.1 %collective-permute-start = (f32[64,2]{1,0:T(8,128)S(1)}, f32[64,2]{1,0:T(8,128)S(1)}, u32[]{:S(2)}, u32[]{:S(2)}) collective-permute-start(f32[64,2]{1,0:T(8,128)S(1)} %slice.39), channel_id=1, source_target_pairs={{0,16},{16,32},{32,48},{48,64},{64,80},{80,96},{96,112},{112,128},... | collective-permute-start | bytes 1544 | tf_op jit(solution)/shard_map/ppermute | solution.py:198
  48.6 1.7 collective-permute-done
  50.4 0.8 multiply_convert_fusion
  51.2 0.0 collective-permute-done.1.gate2_ref
  51.2 0.0 collective-permute-done.2.up2_ref
  51.2 0.0 collective-permute-done.3.down2_ref
  51.3 0.0 copy-start.1
  51.3 1.0 copy-done.1
  52.3 0.0 copy-start.2
  52.3 1.0 copy-done.2
  53.3 0.0 copy-start.3
  53.3 1.0 copy-done.3
  54.4 2.3 %shard_map.172 = (bf16[2048,512]{1,0:T(8,128)(2,1)}, bf16[2048,256]{1,0:T(8,128)(2,1)S(1)}, bf16[4,512,256]{2,1,0:T(8,128)(2,1)S(1)}) custom-call(s32[1]{0:T(128)} %bitcast.16.core_ref, bf16[2048,128]{1,0:T(8,128)(2,1)S(1)} %bitcast.45, bf16[2048,128]{1,0:T(8,128)(2,1)S(1)} %bitcast.47, bf16[128,2048]{1,0:T(8,128)(2,1)S(1)} %bitcast.49, ...), custom_call_target="tpu_custom_call" | custom-call | flops 4194304 | bytes 8388608 | tf_op jit(solution)/shard_map/pallas_call | solution.py:189
  56.7 25.5 %all-gather.4.cloned.1.call-done = bf16[12288,256]{1,0:T(8,128)(2,1)} async-done(((bf16[768,256]{1,0:T(8,128)(2,1)}), bf16[12288,256]{1,0:T(8,128)(2,1)}) %all-gather.4.cloned.1.call-update) | async-done | bytes 6291472 | tf_op jit(solution)/shard_map/all_gather | solution.py:188
  82.2 8.7 %shard_map.173 = (bf16[768,256]{1,0:T(8,128)(2,1)S(1)}, bf16[768,128]{1,0:T(8,128)(2,1)S(1)}, bf16[8,768,128]{2,1,0:T(8,128)(2,1)}) custom-call(bf16[16,768,256]{2,1,0:T(8,128)(2,1)} %bitcast.53, bf16[2048,512]{1,0:T(8,128)(2,1)} %get-tuple-element.48.fore_ref, bf16[2048,256]{1,0:T(8,128)(2,1)S(1)} %get-tuple-element.49.back_ref, ...), custom_call_target="tpu_custom_call" | custom-call | flops 3221225472 | bytes 16777216 | tf_op jit(solution)/shard_map/pallas_call | solution.py:206
  90.9 0.0 reduce-scatter.2.cloned.1.call-update
  90.9 0.0 copy-start
  90.9 0.0 copy-start.5
  90.9 0.0 copy-start.6
  90.9 7.8 %shard_map.174 = (bf16[2048,128]{1,0:T(8,128)(2,1)}, bf16[2048,128]{1,0:T(8,128)(2,1)}, bf16[128,2048]{1,0:T(8,128)(2,1)}) custom-call(bf16[16,768,256]{2,1,0:T(8,128)(2,1)} %bitcast.54, bf16[768,256]{1,0:T(8,128)(2,1)S(1)} %get-tuple-element.54.delta_ref, bf16[768,128]{1,0:T(8,128)(2,1)S(1)} %get-tuple-element.55.hidden_ref), custom_call_target="tpu_custom_call" | custom-call | flops 1207959552 | bytes 16777216 | tf_op jit(solution)/shard_map/pallas_call | solution.py:226
  98.8 0.0 copy-start.4
  98.8 0.0 copy-start.7
  98.8 0.0 copy-start.8
  98.8 34.1 %reduce-scatter.2.cloned.1.call-done = bf16[1,768,128]{2,1,0:T(8,128)(2,1)} async-done(((bf16[8,768,128]{2,1,0:T(8,128)(2,1)}), bf16[1,768,128]{2,1,0:T(8,128)(2,1)}) %reduce-scatter.2.cloned.1.call-update) | async-done | bytes 196624 | tf_op jit(solution)/shard_map/reduce_scatter | solution.py:224
  132.9 19.8 %all_to_all.16 = bf16[32,24,128]{2,1,0:T(8,128)(2,1)S(1)} all-to-all(bf16[32,24,128]{2,1,0:T(8,128)(2,1)} %bitcast.57), channel_id=1, replica_groups=mesh['sp'=32,'y'=8,'c'=2] {'sp'}, dimensions={0} | all-to-all | bytes 393216 | tf_op jit(solution)/shard_map/all_to_all | solution.py:244
  152.8 0.0 copy-done
  152.8 0.0 copy-done.5
  152.8 0.3 shard_map.175
  153.0 17.1 %all-gather.1 = bf16[2048,128]{1,0:T(8,128)(2,1)S(1)} all-gather(bf16[128,128]{1,0:T(8,128)(2,1)S(1)} %shard_map.175), channel_id=3, replica_groups=mesh['sp'=32,'y'=8,'c'=2] {'y','c'}, dimensions={0}, use_global_device_ids=true | all-gather | bytes 557056 | tf_op jit(solution)/shard_map/all_gather | solution.py:268
  170.1 0.0 copy-done.6
  170.1 0.0 copy-done.4
  170.1 1.1 shard_map.176
  171.2 2.5 %collective-permute-start.4 = (f32[64,2]{1,0:T(8,128)S(1)}, f32[64,2]{1,0:T(8,128)S(1)}, u32[]{:S(2)}, u32[]{:S(2)}) collective-permute-start(f32[64,2]{1,0:T(8,128)S(1)} %bitcast.51), channel_id=1, source_target_pairs={{16,0},{32,16},{48,32},{64,48},{80,64},{96,80},{112,96},{128,112},... | collective-permute-start | bytes 1544 | tf_op jit(solution)/shard_map/ppermute | solution.py:277
  173.8 7.3 %all-to-all-start.2 = ((bf16[32,32,128]{2,1,0:T(8,128)(2,1)}), bf16[32,32,128]{2,1,0:T(8,128)(2,1)S(1)}, u32[]{:S(2)}, u32[]{:S(2)}) async-start(bf16[32,32,128]{2,1,0:T(8,128)(2,1)} %get-tuple-element.66), calls=%async_computation.3 | async-start | bytes 524288 | tf_op jit(solution)/shard_map/all_to_all | solution.py:269
  181.0 0.0 collective-permute-done.4
  181.1 0.0 copy-done.7
  181.1 0.7 fusion.10
  181.8 0.0 copy-done.8
  181.8 0.6 fusion.9
  182.4 10.1 %all-to-all-done.2.tiles_ref = bf16[32,32,128]{2,1,0:T(8,128)(2,1)S(1)} async-done(((bf16[32,32,128]{2,1,0:T(8,128)(2,1)}), bf16[32,32,128]{2,1,0:T(8,128)(2,1)S(1)}, u32[]{:S(2)}, u32[]{:S(2)}) %all-to-all-start.2) | async-done | bytes 262176 | tf_op jit(solution)/shard_map/all_to_all | solution.py:269
  192.5 0.8 shard_map.177
  (3 shorter events, 0.0 us)
Async XLA Ops:
  7.2 75.1 %all-gather.4.cloned.1.call-start = ((), (), s32[]{:S(2)}) async-start(), calls=%async_computation.5 | async-start | bytes 6684672 | tf_op jit(solution)/shard_map/all_gather | solution.py:188
  36.8 96.2 %reduce-scatter.2.cloned.1.call-start = ((), (), s32[]{:S(2)}) async-start(), calls=%async_computation.4 | async-start | bytes 1769472 | tf_op jit(solution)/shard_map/reduce_scatter | solution.py:224
  37.5 13.7 %collective-permute-start.1 = (bf16[2048,128]{1,0:T(8,128)(2,1)}, bf16[2048,128]{1,0:T(8,128)(2,1)S(1)}, u32[]{:S(2)}, u32[]{:S(2)}) collective-permute-start(bf16[2048,128]{1,0:T(8,128)(2,1)} %bitcast.44), channel_id=1, source_target_pairs={{0,1},{1,0},{2,3},{3,2},{4,5},{5,4},{6,7},{7,6},{8,9},{9,8},{10,11... | collective-permute-start | bytes 1572872 | tf_op jit(solution)/shard_map/ppermute | solution.py:195
  39.4 11.8 %collective-permute-start.2 = (bf16[2048,128]{1,0:T(8,128)(2,1)}, bf16[2048,128]{1,0:T(8,128)(2,1)S(1)}, u32[]{:S(2)}, u32[]{:S(2)}) collective-permute-start(bf16[2048,128]{1,0:T(8,128)(2,1)} %bitcast.46), channel_id=1, source_target_pairs={{0,1},{1,0},{2,3},{3,2},{4,5},{5,4},{6,7},{7,6},{8,9},{9,8},{10,11... | collective-permute-start | bytes 1572872 | tf_op jit(solution)/shard_map/ppermute | solution.py:195
  41.8 9.4 %collective-permute-start.3 = (bf16[128,2048]{1,0:T(8,128)(2,1)}, bf16[128,2048]{1,0:T(8,128)(2,1)S(1)}, u32[]{:S(2)}, u32[]{:S(2)}) collective-permute-start(bf16[128,2048]{1,0:T(8,128)(2,1)} %bitcast.48), channel_id=1, source_target_pairs={{0,1},{1,0},{2,3},{3,2},{4,5},{5,4},{6,7},{7,6},{8,9},{9,8},{10,11... | collective-permute-start | bytes 1572872 | tf_op jit(solution)/shard_map/ppermute | solution.py:195
  44.6 5.8 %collective-permute-start = (f32[64,2]{1,0:T(8,128)S(1)}, f32[64,2]{1,0:T(8,128)S(1)}, u32[]{:S(2)}, u32[]{:S(2)}) collective-permute-start(f32[64,2]{1,0:T(8,128)S(1)} %slice.39), channel_id=1, source_target_pairs={{0,16},{16,32},{32,48},{48,64},{64,80},{80,96},{96,112},{112,128},... | collective-permute-start | bytes 1544 | tf_op jit(solution)/shard_map/ppermute | solution.py:198
  51.3 1.0 copy-start.1
  52.3 1.0 copy-start.2
  53.3 1.0 copy-start.3
  90.9 61.9 %copy-start = (bf16[128,2048]{1,0:T(8,128)(2,1)S(1)}, bf16[128,2048]{1,0:T(8,128)(2,1)}, u32[]{:S(2)}) copy-start(bf16[128,2048]{1,0:T(8,128)(2,1)} %cot_ref.3) | copy-start | bytes 1572868
  90.9 61.9 %copy-start.5 = (bf16[768,128]{1,0:T(8,128)(2,1)S(1)}, bf16[768,128]{1,0:T(8,128)(2,1)}, u32[]{:S(2)}) copy-start(bf16[768,128]{1,0:T(8,128)(2,1)} %get-tuple-element.63.select_ref) | copy-start | bytes 589828
  90.9 79.2 %copy-start.6 = (bf16[128,64]{0,1:T(8,128)(2,1)S(1)}, bf16[128,64]{0,1:T(8,128)(2,1)}, u32[]{:S(2)}) copy-start(bf16[128,64]{0,1:T(8,128)(2,1)} %param.19) | copy-start | bytes 49156
  98.8 71.3 %copy-start.4 = (bf16[2048,64]{0,1:T(8,128)(2,1)S(1)}, bf16[2048,64]{0,1:T(8,128)(2,1)}, u32[]{:S(2)}) copy-start(bf16[2048,64]{0,1:T(8,128)(2,1)} %param.23) | copy-start | bytes 786436
  98.8 82.3 %copy-start.7 = (bf16[128,64]{0,1:T(8,128)(2,1)S(1)}, bf16[128,64]{0,1:T(8,128)(2,1)}, u32[]{:S(2)}) copy-start(bf16[128,64]{0,1:T(8,128)(2,1)} %param.20) | copy-start | bytes 49156
  98.8 83.0 %copy-start.8 = (bf16[128,64]{0,1:T(8,128)(2,1)S(1)}, bf16[128,64]{0,1:T(8,128)(2,1)}, u32[]{:S(2)}) copy-start(bf16[128,64]{0,1:T(8,128)(2,1)} %param.21) | copy-start | bytes 49156
  171.2 9.8 %collective-permute-start.4 = (f32[64,2]{1,0:T(8,128)S(1)}, f32[64,2]{1,0:T(8,128)S(1)}, u32[]{:S(2)}, u32[]{:S(2)}) collective-permute-start(f32[64,2]{1,0:T(8,128)S(1)} %bitcast.51), channel_id=1, source_target_pairs={{16,0},{32,16},{48,32},{64,48},{80,64},{96,80},{112,96},{128,112},... | collective-permute-start | bytes 1544 | tf_op jit(solution)/shard_map/ppermute | solution.py:277
  173.8 18.7 %all-to-all-start.2 = ((bf16[32,32,128]{2,1,0:T(8,128)(2,1)}), bf16[32,32,128]{2,1,0:T(8,128)(2,1)S(1)}, u32[]{:S(2)}, u32[]{:S(2)}) async-start(bf16[32,32,128]{2,1,0:T(8,128)(2,1)} %get-tuple-element.66), calls=%async_computation.3 | async-start | bytes 524288 | tf_op jit(solution)/shard_map/all_to_all | solution.py:269
Sparse Core Ops, SparseCore 0:
  36.9 45.2 all-gather.3
  91.0 41.8 reduce-scatter.1

commit v5 on v4

--- a/solution.py
+++ b/solution.py
@@ -6,6 +6,7 @@
 from jax.experimental import pallas as pl
 from jax.experimental.pallas import tpu as pltpu
 from jax.sharding import Mesh, PartitionSpec as P
+
 
 BF16, F32, I32 = jnp.bfloat16, jnp.float32, jnp.int32
 TP = ("y", "c")
@@ -36,7 +37,13 @@
     return jax.ShapeDtypeStruct(dims, kind)
 
 
-def select_body(experts, capacity, at_ref, routes_ref, weights_ref, rows_ref, cot_ref, send_ref, select_ref):
+def select_body(experts, capacity, at_ref, routes_ref, weights_ref, rows_ref, cot_ref, send_ref, select_ref, held, sems):
+    at = pl.ds(pl.multiple_of(at_ref[0] * LANES, LANES), LANES)
+    copies = [
+        pltpu.make_async_copy(ref.at[:, at], held.at[i], sems.at[i]) for i, ref in enumerate((rows_ref, cot_ref))
+    ]
+    for copy in copies:
+        copy.start()
     tokens = routes_ref.shape[1]
     number = lax.broadcasted_iota(I32, (experts, tokens), 0)
     first = routes_ref[0:1, :] == number
@@ -56,8 +63,10 @@
     select = jnp.concatenate(picked, axis=0).astype(BF16)
     scale = jnp.concatenate(scales, axis=0)
     select_ref[...] = select
-    send_ref[:, :LANES] = mm(select, rows_ref[...]).astype(BF16)
-    send_ref[:, LANES:] = (mm(select, cot_ref[...]) * scale).astype(BF16)
+    for copy in copies:
+        copy.wait()
+    send_ref[:, :LANES] = mm(select, held[0]).astype(BF16)
+    send_ref[:, LANES:] = (mm(select, held[1]) * scale).astype(BF16)
 
 
 def layout_body(core_ref, gate_ref, up_ref, down_ref, gate2_ref, up2_ref, down2_ref, fore_ref, back_ref, rows_ref):
@@ -113,18 +122,22 @@
     grad_ref[...] = (cot_ref[...].astype(F32) + moe.astype(F32)).astype(BF16)
 
 
-def conv_body(steps, grads_ref, weight_ref, conv_ref, sum_ref, outer_ref, outer_grad_ref, scaled_ref, out_ref):
-    total = jnp.zeros(sum_ref.shape, F32)
+def part_body(grads_ref, conv_ref, out_ref):
     half = conv_ref.shape[0] // 2
     low = lax.broadcasted_iota(I32, (half, LANES), 1) < LANES // 2
-    for k in range(steps):
-        g = jnp.concatenate([grads_ref[2 * k], grads_ref[2 * k + 1]], axis=1)
-        total = total + mm(weight_ref[:, k * 2 * LANES : (k + 1) * 2 * LANES], g, NT)
-        parts = mm(conv_ref[...], g)
+    for k in range(0, grads_ref.shape[0], 2):
+        parts = mm(conv_ref[...], jnp.concatenate([grads_ref[k], grads_ref[k + 1]], axis=1))
         for t in range(2):
             top, bottom = (parts[r * half : (r + 1) * half, t * LANES : (t + 1) * LANES] for r in range(2))
-            out_ref[4 * k + 2 * t] = jnp.where(low, top, pltpu.roll(bottom, LANES // 2, 1)).astype(BF16)
-            out_ref[4 * k + 2 * t + 1] = jnp.where(low, pltpu.roll(top, LANES // 2, 1), bottom).astype(BF16)
+            out_ref[2 * k + 2 * t] = jnp.where(low, top, pltpu.roll(bottom, LANES // 2, 1)).astype(BF16)
+            out_ref[2 * k + 2 * t + 1] = jnp.where(low, pltpu.roll(top, LANES // 2, 1), bottom).astype(BF16)
+
+
+def conv_body(grads_ref, weight_ref, sum_ref, outer_ref, outer_grad_ref, scaled_ref):
+    total = jnp.zeros(sum_ref.shape, F32)
+    for k in range(0, grads_ref.shape[0], 2):
+        g = jnp.concatenate([grads_ref[k], grads_ref[k + 1]], axis=1)
+        total = total + mm(weight_ref[:, k * LANES : (k + 2) * LANES], g, NT)
     outer_grad_ref[...] = (total * sum_ref[...]).astype(BF16)
     scaled_ref[...] = total * outer_ref[...].astype(F32)
 
@@ -170,13 +183,10 @@
         functools.partial(select_body, experts, capacity),
         (shape((slots, 2 * LANES), BF16), shape((slots, LANES), BF16)),
         (2 * slots * tokens * 2 * LANES, 2**20),
-        room=67_043_328,
-        grid_spec=pltpu.PrefetchScalarGridSpec(
-            num_scalar_prefetch=1,
-            grid=(1,),
-            in_specs=[whole(2, tokens), whole(2, tokens), block, block],
-            out_specs=[whole(slots, 2 * LANES), whole(slots, LANES)],
-        ),
+        room=66_000_000,
+        in_specs=[pl.BlockSpec(memory_space=pltpu.SMEM)] + [VMEM] * 2 + [pl.BlockSpec(memory_space=pltpu.HBM)] * 2,
+        out_specs=[VMEM] * 2,
+        scratch_shapes=[pltpu.VMEM((2, tokens, LANES), BF16), pltpu.SemaphoreType.DMA((2,))],
     )(at, routes.T, route_weights.T, stream, cotangent)
     recv = lax.all_to_all(
         send.reshape(groups, capacity, 2 * LANES), "sp", split_axis=0, concat_axis=0, tiled=True
@@ -190,6 +200,7 @@
         layout_body,
         (shape((width, 4 * units), BF16), shape((width, 2 * units), BF16), shape((ys // 2, 4 * units, 2 * LANES), BF16)),
         (2**22, 2**23),
+        room=20 * 2**20,
         in_specs=[pl.BlockSpec(memory_space=pltpu.SMEM)] + [VMEM] * 6,
         out_specs=[VMEM] * 3,
     )(core, *held, *(lax.ppermute(a, "c", swap) for a in held))
@@ -207,6 +218,7 @@
         functools.partial(expert_body, tps),
         (shape((slots, 2 * units), BF16), shape((slots, units), BF16), shape((ys, slots, LANES), BF16)),
         (16 * slots * width * units, 2**24),
+        room=46 * 2**20,
         grid=(slots // rows,),
         in_specs=[
             pl.BlockSpec((tps, rows, 2 * LANES), lambda i: (0, i, 0)),
@@ -255,18 +267,23 @@
             out_specs=whole(tokens, LANES),
         ),
     )(at, returned.reshape(slots, LANES), select, cotangent)
-    outer_grad, scaled, out_parts = call(
-        functools.partial(conv_body, ys),
-        (
-            shape((channels, tokens), BF16),
-            shape((channels, tokens), F32),
-            shape((groups, channels // 2, LANES), BF16),
-        ),
-        (4 * tokens * width * channels, 2**20),
-        in_specs=[VMEM] * 5,
-        out_specs=[VMEM] * 3,
-    )(lax.all_gather(stream_block, TP), out_weight.T, conv_out, conv_sum, outer_t)
+    stream_all = lax.all_gather(stream_block, TP)
+    out_parts = call(
+        part_body,
+        shape((groups, channels // 2, LANES), BF16),
+        (2 * tokens * width * channels, 2**20),
+        in_specs=[VMEM] * 2,
+        out_specs=VMEM,
+    )(stream_all, conv_out)
     out_tiles = lax.all_to_all(out_parts, "sp", split_axis=0, concat_axis=0, tiled=True)
+    outer_grad, scaled = call(
+        conv_body,
+        (shape((channels, tokens), BF16), shape((channels, tokens), F32)),
+        (2 * tokens * width * channels, 2**20),
+        name="conv_grad",
+        in_specs=[VMEM] * 4,
+        out_specs=[VMEM] * 2,
+    )(stream_all, out_weight.T, conv_sum, outer_t)
     out_grad = call(
         out_body,
         shape((channels, width // groups), F32),
@@ -299,6 +316,7 @@
         P(None, TP),
         P(None, TP),
     )
+
     return jax.shard_map(
         per_device,
         mesh=fine,

time: 202 us -> 205 us (1.015)
  local copies, waits for them, and re-layouts: 3.24 us -> 7.42 us
  other arithmetic: 3.59 us -> 1.46 us
  waiting for transfers between devices: 71.5 us -> 73.6 us
    unnamed x19 -> x29, local copies, waits for them, and re-layouts: 3.15 us -> 7.34 us
  transfers between devices with their start and end apart: 8 -> 8, of which waited for: 4 -> 4; matrix products, arithmetic and copies ran while one was open for 2% -> 1% of each run, Pallas kernels for 5% -> 5%
where the time goes in v5:
time: 205 us; the launch traced here: 204 us
  waiting for transfers between devices  73.6 us (36%)
  blocking collectives  64.4 us (31%)
  Pallas kernels  22.3 us (11%)
  starting transfers between devices  20.1 us (10%)
  between operations  14.3 us (7%)
  local copies, waits for them, and re-layouts  7.42 us (4%)
    reduce_scatter x1, waiting for transfers between devices, per_device(): half_sums = lax.psum_scatter(chip, 'y', scatter_dimension=0)  34.1 us
    all_gather x1, waiting for transfers between devices, per_device(): got = lax.all_gather(recv, TP)  27.6 us
    all_to_all x1, blocking collectives, per_device(): lax.all_to_all(send.reshape(groups, capacity, 2 * LANES), 'sp', split_axi...  27.5 us
    all_to_all x1, blocking collectives, per_device(): lax.all_to_all(half_sums.reshape(groups, capacity, LANES), 'sp', split_ax...  19.8 us
    all_gather x1, blocking collectives, per_device(): stream_all = lax.all_gather(stream_block, TP)  17.1 us
    all_to_all x1, waiting for transfers between devices, per_device(): lax.all_to_all(out_parts, 'sp', split_axis=0, concat_axis=0, tiled=True)  10.1 us
    pallas_call x1, Pallas kernels, per_device(): call(functools.partial(expert_body, tps), (shape((slots, 2 * units), BF16...  8.02 us
    pallas_call x1, Pallas kernels, per_device(): call(weight_body, (shape((width, units), BF16), shape((width, units), BF1...  7.85 us
  transfers between devices with their start and end apart: 8, of which 4 were waited for; matrix products, arithmetic and copies ran while one was open for 1% of the time, Pallas kernels for 5%

profile of v5, /device:TPU:6, one launch (start us, length us, event | category | flops | bytes accessed | tf_op | source)
XLA Modules:
  0.0 203.7 jit_solution(13262838922828563447)
XLA Ops:
  7.2 0.0 copy-start.11
  7.2 0.0 copy-start.1
  7.2 0.0 copy-start.13
  7.2 0.0 copy-start.12
  7.2 0.0 copy-start.6
  7.2 0.0 all-gather.4.cloned.1.call-start
  7.3 2.5 %shard_map.171 = (bf16[768,256]{1,0:T(8,128)(2,1)}, bf16[768,128]{1,0:T(8,128)(2,1)}) custom-call(s32[1]{0:T(128)} %bitcast.at_ref, s32[2,128]{1,0:T(2,128)} %bitcast.61, f32[2,128]{1,0:T(2,128)} %bitcast.62, bf16[128,2048]{1,0:T(8,128)(2,1)} %rows_ref.1, bf16[128,2048]{1,0:T(8,128)(2,1)} %cot_ref.3), custom_call_target="tpu_custom_call" | custom-call | flops 50331648 | bytes 1048576 | tf_op jit(solution)/shard_map/pallas_call | solution.py:182
  9.8 27.5 %all_to_all.15 = bf16[32,24,256]{2,1,0:T(8,128)(2,1)} all-to-all(bf16[32,24,256]{2,1,0:T(8,128)(2,1)} %bitcast.57), channel_id=1, replica_groups=mesh['sp'=32,'y'=8,'c'=2] {'sp'}, dimensions={0} | all-to-all | bytes 786432 | tf_op jit(solution)/shard_map/all_to_all | solution.py:191
  37.4 0.0 all-gather.4.cloned.1.call-update
  37.4 0.0 reduce-scatter.2.cloned.1.call-start
  37.4 0.0 copy-done.13
  37.5 0.0 copy-done.1
  37.5 1.9 collective-permute-start.1
  39.4 2.4 %collective-permute-start.2 = (bf16[2048,128]{1,0:T(8,128)(2,1)}, bf16[2048,128]{1,0:T(8,128)(2,1)S(1)}, u32[]{:S(2)}, u32[]{:S(2)}) collective-permute-start(bf16[2048,128]{1,0:T(8,128)(2,1)} %bitcast.47), channel_id=1, source_target_pairs={{0,1},{1,0},{2,3},{3,2},{4,5},{5,4},{6,7},{7,6},{8,9},{9,8},{10,11... | collective-permute-start | bytes 1572872 | tf_op jit(solution)/shard_map/ppermute | solution.py:206
  41.8 1.9 collective-permute-start.3
  43.8 0.0 copy-done.11
  43.8 0.0 copy-done.12
  43.8 0.1 slice.39
  43.9 4.0 %collective-permute-start = (f32[64,2]{1,0:T(8,128)S(1)}, f32[64,2]{1,0:T(8,128)S(1)}, u32[]{:S(2)}, u32[]{:S(2)}) collective-permute-start(f32[64,2]{1,0:T(8,128)S(1)} %slice.39), channel_id=1, source_target_pairs={{0,16},{16,32},{32,48},{48,64},{64,80},{80,96},{96,112},{112,128},... | collective-permute-start | bytes 1544 | tf_op jit(solution)/shard_map/ppermute | solution.py:209
  47.9 1.7 collective-permute-done
  49.7 0.0 copy-done.6
  49.7 0.1 multiply_convert_fusion
  49.8 0.0 collective-permute-done.1.gate2_ref
  49.8 0.0 collective-permute-done.2.up2_ref
  49.8 0.0 collective-permute-done.3.down2_ref
  49.8 0.0 copy-start.2
  49.8 1.0 copy-done.2
  50.9 0.0 copy-start.3
  50.9 1.0 copy-done.3
  51.9 1.0 shard_map.172
  52.9 0.0 copy-start.7
  52.9 1.4 copy-done.7
  54.3 0.0 copy-start.9
  54.3 1.0 copy-done.9
  55.3 27.6 %all-gather.4.cloned.1.call-done = bf16[12288,256]{1,0:T(8,128)(2,1)} async-done(((bf16[768,256]{1,0:T(8,128)(2,1)}), bf16[12288,256]{1,0:T(8,128)(2,1)}) %all-gather.4.cloned.1.call-update) | async-done | bytes 6291472 | tf_op jit(solution)/shard_map/all_gather | solution.py:198
  82.9 0.0 copy-start.8
  82.9 1.6 copy-done.8
  84.5 0.0 copy-start.10
  84.5 1.2 copy-done.10
  85.7 8.0 %shard_map.173 = (bf16[768,256]{1,0:T(8,128)(2,1)S(1)}, bf16[768,128]{1,0:T(8,128)(2,1)S(1)}, bf16[8,768,128]{2,1,0:T(8,128)(2,1)}) custom-call(bf16[16,768,256]{2,1,0:T(8,128)(2,1)} %bitcast.54, bf16[2048,512]{1,0:T(8,128)(2,1)S(1)} %copy-done.8, bf16[2048,256]{1,0:T(8,128)(2,1)S(1)} %get-tuple-element.48.back_ref, bf16[4,512,256]{2,1,0:T(8,128)(2,1)S(1)} %copy-done.10), custom_call_target="tpu_custom_call" | custom-call | flops 3221225472 | bytes 16777216 | tf_op jit(solution)/shard_map/pallas_call | solution.py:217
  93.7 0.0 reduce-scatter.2.cloned.1.call-update
  93.7 0.0 copy-start
  93.7 0.0 copy-start.5
  93.7 7.9 %shard_map.174 = (bf16[2048,128]{1,0:T(8,128)(2,1)}, bf16[2048,128]{1,0:T(8,128)(2,1)}, bf16[128,2048]{1,0:T(8,128)(2,1)}) custom-call(bf16[16,768,256]{2,1,0:T(8,128)(2,1)} %bitcast.55, bf16[768,256]{1,0:T(8,128)(2,1)S(1)} %get-tuple-element.53.delta_ref, bf16[768,128]{1,0:T(8,128)(2,1)S(1)} %get-tuple-element.54.hidden_ref), custom_call_target="tpu_custom_call" | custom-call | flops 1207959552 | bytes 16777216 | tf_op jit(solution)/shard_map/pallas_call | solution.py:238
  101.6 0.0 copy-start.4
  101.6 34.1 %reduce-scatter.2.cloned.1.call-done = bf16[1,768,128]{2,1,0:T(8,128)(2,1)} async-done(((bf16[8,768,128]{2,1,0:T(8,128)(2,1)}), bf16[1,768,128]{2,1,0:T(8,128)(2,1)}) %reduce-scatter.2.cloned.1.call-update) | async-done | bytes 196624 | tf_op jit(solution)/shard_map/reduce_scatter | solution.py:236
  135.7 19.8 %all_to_all.16 = bf16[32,24,128]{2,1,0:T(8,128)(2,1)S(1)} all-to-all(bf16[32,24,128]{2,1,0:T(8,128)(2,1)} %bitcast.58), channel_id=1, replica_groups=mesh['sp'=32,'y'=8,'c'=2] {'sp'}, dimensions={0} | all-to-all | bytes 393216 | tf_op jit(solution)/shard_map/all_to_all | solution.py:256
  155.6 0.0 copy-done
  155.6 0.0 copy-done.5
  155.6 0.3 shard_map.175
  155.9 17.1 %all-gather.1 = bf16[2048,128]{1,0:T(8,128)(2,1)S(1)} all-gather(bf16[128,128]{1,0:T(8,128)(2,1)S(1)} %shard_map.175), channel_id=3, replica_groups=mesh['sp'=32,'y'=8,'c'=2] {'y','c'}, dimensions={0}, use_global_device_ids=true | all-gather | bytes 557056 | tf_op jit(solution)/shard_map/all_gather | solution.py:270
  172.9 0.0 copy-done.4
  172.9 0.9 conv_grad.1
  173.8 2.5 %collective-permute-start.4 = (f32[64,2]{1,0:T(8,128)S(1)}, f32[64,2]{1,0:T(8,128)S(1)}, u32[]{:S(2)}, u32[]{:S(2)}) collective-permute-start(f32[64,2]{1,0:T(8,128)S(1)} %bitcast.52), channel_id=1, source_target_pairs={{16,0},{32,16},{48,32},{64,48},{80,64},{96,80},{112,96},{128,112},... | collective-permute-start | bytes 1544 | tf_op jit(solution)/shard_map/ppermute | solution.py:294
  176.3 1.0 shard_map.176
  177.3 7.2 %all-to-all-start.2 = ((bf16[32,32,128]{2,1,0:T(8,128)(2,1)}), bf16[32,32,128]{2,1,0:T(8,128)(2,1)S(1)}, u32[]{:S(2)}, u32[]{:S(2)}) async-start(bf16[32,32,128]{2,1,0:T(8,128)(2,1)} %shard_map.176), calls=%async_computation.3 | async-start | bytes 524288 | tf_op jit(solution)/shard_map/all_to_all | solution.py:278
  184.6 0.0 collective-permute-done.4
  184.6 0.7 fusion.10
  185.3 0.6 fusion.9
  186.0 10.1 %all-to-all-done.2.tiles_ref = bf16[32,32,128]{2,1,0:T(8,128)(2,1)S(1)} async-done(((bf16[32,32,128]{2,1,0:T(8,128)(2,1)}), bf16[32,32,128]{2,1,0:T(8,128)(2,1)S(1)}, u32[]{:S(2)}, u32[]{:S(2)}) %all-to-all-start.2) | async-done | bytes 262176 | tf_op jit(solution)/shard_map/all_to_all | solution.py:278
  196.1 0.8 shard_map.177
  (5 shorter events, 0.0 us)
Async XLA Ops:
  7.2 36.6 %copy-start.11 = (bf16[128,64]{0,1:T(8,128)(2,1)S(1)}, bf16[128,64]{0,1:T(8,128)(2,1)}, u32[]{:S(2)}) copy-start(bf16[128,64]{0,1:T(8,128)(2,1)} %param.20) | copy-start | bytes 49156
  7.2 30.3 %copy-start.1 = (bf16[1,2048,128]{2,1,0:T(8,128)(2,1)S(1)}, bf16[1,2048,128]{2,1,0:T(8,128)(2,1)}, u32[]{:S(2)}) copy-start(bf16[1,2048,128]{2,1,0:T(8,128)(2,1)} %param.16) | copy-start | bytes 1572868
  7.2 30.3 %copy-start.13 = (bf16[3,64]{1,0:T(4,128)(2,1)S(1)}, bf16[3,64]{1,0:T(4,128)(2,1)}, u32[]{:S(2)}) copy-start(bf16[3,64]{1,0:T(4,128)(2,1)} %param.22) | copy-start | bytes 1156
  7.2 36.6 %copy-start.12 = (bf16[128,64]{0,1:T(8,128)(2,1)S(1)}, bf16[128,64]{0,1:T(8,128)(2,1)}, u32[]{:S(2)}) copy-start(bf16[128,64]{0,1:T(8,128)(2,1)} %param.21) | copy-start | bytes 49156
  7.2 42.5 %copy-start.6 = (bf16[128,64]{0,1:T(8,128)(2,1)S(1)}, bf16[128,64]{0,1:T(8,128)(2,1)}, u32[]{:S(2)}) copy-start(bf16[128,64]{0,1:T(8,128)(2,1)} %param.19) | copy-start | bytes 49156
  7.2 75.6 %all-gather.4.cloned.1.call-start = ((), (), s32[]{:S(2)}) async-start(), calls=%async_computation.5 | async-start | bytes 6684672 | tf_op jit(solution)/shard_map/all_gather | solution.py:198
  37.4 98.3 %reduce-scatter.2.cloned.1.call-start = ((), (), s32[]{:S(2)}) async-start(), calls=%async_computation.4 | async-start | bytes 1769472 | tf_op jit(solution)/shard_map/reduce_scatter | solution.py:236
  37.5 12.3 %collective-permute-start.1 = (bf16[2048,128]{1,0:T(8,128)(2,1)S(1)}, bf16[2048,128]{1,0:T(8,128)(2,1)S(1)}, u32[]{:S(2)}, u32[]{:S(2)}) collective-permute-start(bf16[2048,128]{1,0:T(8,128)(2,1)S(1)} %bitcast.45), channel_id=1, source_target_pairs={{0,1},{1,0},{2,3},{3,2},{4,5},{5,4},{6,7},{7,6},{8,9},{9,8},{10,11... | collective-permute-start | bytes 1572872 | tf_op jit(solution)/shard_map/ppermute | solution.py:206
  39.4 10.4 %collective-permute-start.2 = (bf16[2048,128]{1,0:T(8,128)(2,1)}, bf16[2048,128]{1,0:T(8,128)(2,1)S(1)}, u32[]{:S(2)}, u32[]{:S(2)}) collective-permute-start(bf16[2048,128]{1,0:T(8,128)(2,1)} %bitcast.47), channel_id=1, source_target_pairs={{0,1},{1,0},{2,3},{3,2},{4,5},{5,4},{6,7},{7,6},{8,9},{9,8},{10,11... | collective-permute-start | bytes 1572872 | tf_op jit(solution)/shard_map/ppermute | solution.py:206
  41.8 8.0 %collective-permute-start.3 = (bf16[128,2048]{1,0:T(8,128)(2,1)}, bf16[128,2048]{1,0:T(8,128)(2,1)S(1)}, u32[]{:S(2)}, u32[]{:S(2)}) collective-permute-start(bf16[128,2048]{1,0:T(8,128)(2,1)} %bitcast.49), channel_id=1, source_target_pairs={{0,1},{1,0},{2,3},{3,2},{4,5},{5,4},{6,7},{7,6},{8,9},{9,8},{10,11... | collective-permute-start | bytes 1572872 | tf_op jit(solution)/shard_map/ppermute | solution.py:206
  43.9 5.8 %collective-permute-start = (f32[64,2]{1,0:T(8,128)S(1)}, f32[64,2]{1,0:T(8,128)S(1)}, u32[]{:S(2)}, u32[]{:S(2)}) collective-permute-start(f32[64,2]{1,0:T(8,128)S(1)} %slice.39), channel_id=1, source_target_pairs={{0,16},{16,32},{32,48},{48,64},{64,80},{80,96},{96,112},{112,128},... | collective-permute-start | bytes 1544 | tf_op jit(solution)/shard_map/ppermute | solution.py:209
  49.8 1.0 copy-start.2
  50.9 1.0 copy-start.3
  52.9 1.4 copy-start.7
  54.3 1.0 copy-start.9
  82.9 1.6 copy-start.8
  84.5 1.2 copy-start.10
  93.7 61.9 %copy-start = (bf16[128,2048]{1,0:T(8,128)(2,1)S(1)}, bf16[128,2048]{1,0:T(8,128)(2,1)}, u32[]{:S(2)}) copy-start(bf16[128,2048]{1,0:T(8,128)(2,1)} %cot_ref.3) | copy-start | bytes 1572868
  93.7 61.9 %copy-start.5 = (bf16[768,128]{1,0:T(8,128)(2,1)S(1)}, bf16[768,128]{1,0:T(8,128)(2,1)}, u32[]{:S(2)}) copy-start(bf16[768,128]{1,0:T(8,128)(2,1)} %get-tuple-element.62.select_ref) | copy-start | bytes 589828
  101.6 71.3 %copy-start.4 = (bf16[2048,64]{0,1:T(8,128)(2,1)S(1)}, bf16[2048,64]{0,1:T(8,128)(2,1)}, u32[]{:S(2)}) copy-start(bf16[2048,64]{0,1:T(8,128)(2,1)} %param.23) | copy-start | bytes 786436
  173.8 10.8 %collective-permute-start.4 = (f32[64,2]{1,0:T(8,128)S(1)}, f32[64,2]{1,0:T(8,128)S(1)}, u32[]{:S(2)}, u32[]{:S(2)}) collective-permute-start(f32[64,2]{1,0:T(8,128)S(1)} %bitcast.52), channel_id=1, source_target_pairs={{16,0},{32,16},{48,32},{64,48},{80,64},{96,80},{112,96},{128,112},... | collective-permute-start | bytes 1544 | tf_op jit(solution)/shard_map/ppermute | solution.py:294
  177.3 18.7 %all-to-all-start.2 = ((bf16[32,32,128]{2,1,0:T(8,128)(2,1)}), bf16[32,32,128]{2,1,0:T(8,128)(2,1)S(1)}, u32[]{:S(2)}, u32[]{:S(2)}) async-start(bf16[32,32,128]{2,1,0:T(8,128)(2,1)} %shard_map.176), calls=%async_computation.3 | async-start | bytes 524288 | tf_op jit(solution)/shard_map/all_to_all | solution.py:278
Sparse Core Ops, SparseCore 0:
  37.5 45.2 all-gather.3
  93.8 41.8 reduce-scatter.1

commit v6 on v5

--- a/solution.py
+++ b/solution.py
@@ -37,13 +37,7 @@
     return jax.ShapeDtypeStruct(dims, kind)
 
 
-def select_body(experts, capacity, at_ref, routes_ref, weights_ref, rows_ref, cot_ref, send_ref, select_ref, held, sems):
-    at = pl.ds(pl.multiple_of(at_ref[0] * LANES, LANES), LANES)
-    copies = [
-        pltpu.make_async_copy(ref.at[:, at], held.at[i], sems.at[i]) for i, ref in enumerate((rows_ref, cot_ref))
-    ]
-    for copy in copies:
-        copy.start()
+def select_body(experts, capacity, at_ref, routes_ref, weights_ref, rows_ref, cot_ref, send_ref, select_ref):
     tokens = routes_ref.shape[1]
     number = lax.broadcasted_iota(I32, (experts, tokens), 0)
     first = routes_ref[0:1, :] == number
@@ -63,10 +57,8 @@
     select = jnp.concatenate(picked, axis=0).astype(BF16)
     scale = jnp.concatenate(scales, axis=0)
     select_ref[...] = select
-    for copy in copies:
-        copy.wait()
-    send_ref[:, :LANES] = mm(select, held[0]).astype(BF16)
-    send_ref[:, LANES:] = (mm(select, held[1]) * scale).astype(BF16)
+    send_ref[:, :LANES] = mm(select, rows_ref[...]).astype(BF16)
+    send_ref[:, LANES:] = (mm(select, cot_ref[...]) * scale).astype(BF16)
 
 
 def layout_body(core_ref, gate_ref, up_ref, down_ref, gate2_ref, up2_ref, down2_ref, fore_ref, back_ref, rows_ref):
@@ -183,10 +175,13 @@
         functools.partial(select_body, experts, capacity),
         (shape((slots, 2 * LANES), BF16), shape((slots, LANES), BF16)),
         (2 * slots * tokens * 2 * LANES, 2**20),
-        room=66_000_000,
-        in_specs=[pl.BlockSpec(memory_space=pltpu.SMEM)] + [VMEM] * 2 + [pl.BlockSpec(memory_space=pltpu.HBM)] * 2,
-        out_specs=[VMEM] * 2,
-        scratch_shapes=[pltpu.VMEM((2, tokens, LANES), BF16), pltpu.SemaphoreType.DMA((2,))],
+        room=67_043_328,
+        grid_spec=pltpu.PrefetchScalarGridSpec(
+            num_scalar_prefetch=1,
+            grid=(1,),
+            in_specs=[whole(2, tokens), whole(2, tokens), block, block],
+            out_specs=[whole(slots, 2 * LANES), whole(slots, LANES)],
+        ),
     )(at, routes.T, route_weights.T, stream, cotangent)
     recv = lax.all_to_all(
         send.reshape(groups, capacity, 2 * LANES), "sp", split_axis=0, concat_axis=0, tiled=True
@@ -200,7 +195,6 @@
         layout_body,
         (shape((width, 4 * units), BF16), shape((width, 2 * units), BF16), shape((ys // 2, 4 * units, 2 * LANES), BF16)),
         (2**22, 2**23),
-        room=20 * 2**20,
         in_specs=[pl.BlockSpec(memory_space=pltpu.SMEM)] + [VMEM] * 6,
         out_specs=[VMEM] * 3,
     )(core, *held, *(lax.ppermute(a, "c", swap) for a in held))
@@ -218,7 +212,6 @@
         functools.partial(expert_body, tps),
         (shape((slots, 2 * units), BF16), shape((slots, units), BF16), shape((ys, slots, LANES), BF16)),
         (16 * slots * width * units, 2**24),
-        room=46 * 2**20,
         grid=(slots // rows,),
         in_specs=[
             pl.BlockSpec((tps, rows, 2 * LANES), lambda i: (0, i, 0)),

time: 205 us -> 203 us (level)
  local copies, waits for them, and re-layouts: 7.42 us -> 3.23 us
  other arithmetic: 1.46 us -> 3.59 us
  waiting for transfers between devices: 73.6 us -> 71.5 us
    unnamed x29 -> x19, local copies, waits for them, and re-layouts: 7.34 us -> 3.15 us
  transfers between devices with their start and end apart: 8 -> 8, of which waited for: 4 -> 4; matrix products, arithmetic and copies ran while one was open for 1% -> 2% of each run, Pallas kernels for 5% -> 6%
where the time goes in v6:
time: 203 us; the launch traced here: 201 us
  waiting for transfers between devices  71.5 us (35%)
  blocking collectives  64.6 us (32%)
  Pallas kernels  23.8 us (12%)
  starting transfers between devices  20.1 us (10%)
  between operations  14.2 us (7%)
  other arithmetic  3.59 us (2%)
  local copies, waits for them, and re-layouts  3.23 us (2%)
    reduce_scatter x1, waiting for transfers between devices, per_device(): half_sums = lax.psum_scatter(chip, 'y', scatter_dimension=0)  34.2 us
    all_to_all x1, blocking collectives, per_device(): lax.all_to_all(send.reshape(groups, capacity, 2 * LANES), 'sp', split_axi...  27.5 us
    all_gather x1, waiting for transfers between devices, per_device(): got = lax.all_gather(recv, TP)  25.5 us
    all_to_all x1, blocking collectives, per_device(): lax.all_to_all(half_sums.reshape(groups, capacity, LANES), 'sp', split_ax...  20 us
    all_gather x1, blocking collectives, per_device(): stream_all = lax.all_gather(stream_block, TP)  17.1 us
    all_to_all x1, waiting for transfers between devices, per_device(): lax.all_to_all(out_parts, 'sp', split_axis=0, concat_axis=0, tiled=True)  10.1 us
    pallas_call x1, Pallas kernels, per_device(): call(functools.partial(expert_body, tps), (shape((slots, 2 * units), BF16...  8.66 us
    pallas_call x1, Pallas kernels, per_device(): call(weight_body, (shape((width, units), BF16), shape((width, units), BF1...  7.83 us
  transfers between devices with their start and end apart: 8, of which 4 were waited for; matrix products, arithmetic and copies ran while one was open for 2% of the time, Pallas kernels for 6%

profile of v6, /device:TPU:6, one launch (start us, length us, event | category | flops | bytes accessed | tf_op | source)
XLA Modules:
  0.0 201.0 jit_solution(9384427349819103247)
XLA Ops:
  7.2 0.0 all-gather.4.cloned.1.call-start
  7.2 2.0 shard_map.171
  9.2 27.5 %all_to_all.15 = bf16[32,24,256]{2,1,0:T(8,128)(2,1)} all-to-all(bf16[32,24,256]{2,1,0:T(8,128)(2,1)} %bitcast.57), channel_id=1, replica_groups=mesh['sp'=32,'y'=8,'c'=2] {'sp'}, dimensions={0} | all-to-all | bytes 786432 | tf_op jit(solution)/shard_map/all_to_all | solution.py:186
  36.7 0.0 all-gather.4.cloned.1.call-update
  36.8 0.0 reduce-scatter.2.cloned.1.call-start
  36.8 0.7 convert_bitcast_fusion
  37.5 1.9 collective-permute-start.1
  39.4 2.4 %collective-permute-start.2 = (bf16[2048,128]{1,0:T(8,128)(2,1)}, bf16[2048,128]{1,0:T(8,128)(2,1)S(1)}, u32[]{:S(2)}, u32[]{:S(2)}) collective-permute-start(bf16[2048,128]{1,0:T(8,128)(2,1)} %bitcast.47), channel_id=1, source_target_pairs={{0,1},{1,0},{2,3},{3,2},{4,5},{5,4},{6,7},{7,6},{8,9},{9,8},{10,11... | collective-permute-start | bytes 1572872 | tf_op jit(solution)/shard_map/ppermute | solution.py:200
  41.8 1.9 collective-permute-start.3
  43.8 0.7 convert_multiply_fusion.1
  44.5 0.1 slice.39
  44.6 4.1 %collective-permute-start = (f32[64,2]{1,0:T(8,128)S(1)}, f32[64,2]{1,0:T(8,128)S(1)}, u32[]{:S(2)}, u32[]{:S(2)}) collective-permute-start(f32[64,2]{1,0:T(8,128)S(1)} %slice.39), channel_id=1, source_target_pairs={{0,16},{16,32},{32,48},{48,64},{64,80},{80,96},{96,112},{112,128},... | collective-permute-start | bytes 1544 | tf_op jit(solution)/shard_map/ppermute | solution.py:203
  48.6 1.7 collective-permute-done
  50.4 0.8 multiply_convert_fusion
  51.2 0.0 collective-permute-done.1.gate2_ref
  51.2 0.0 collective-permute-done.2.up2_ref
  51.2 0.0 collective-permute-done.3.down2_ref
  51.3 0.0 copy-start.1
  51.3 1.0 copy-done.1
  52.3 0.0 copy-start.2
  52.3 1.0 copy-done.2
  53.3 0.0 copy-start.3
  53.3 1.0 copy-done.3
  54.4 2.3 %shard_map.172 = (bf16[2048,512]{1,0:T(8,128)(2,1)}, bf16[2048,256]{1,0:T(8,128)(2,1)S(1)}, bf16[4,512,256]{2,1,0:T(8,128)(2,1)S(1)}) custom-call(s32[1]{0:T(128)} %bitcast.16.core_ref, bf16[2048,128]{1,0:T(8,128)(2,1)S(1)} %bitcast.46, bf16[2048,128]{1,0:T(8,128)(2,1)S(1)} %bitcast.48, bf16[128,2048]{1,0:T(8,128)(2,1)S(1)} %bitcast.50, ...), custom_call_target="tpu_custom_call" | custom-call | flops 4194304 | bytes 8388608 | tf_op jit(solution)/shard_map/pallas_call | solution.py:194
  56.7 25.5 %all-gather.4.cloned.1.call-done = bf16[12288,256]{1,0:T(8,128)(2,1)} async-done(((bf16[768,256]{1,0:T(8,128)(2,1)}), bf16[12288,256]{1,0:T(8,128)(2,1)}) %all-gather.4.cloned.1.call-update) | async-done | bytes 6291472 | tf_op jit(solution)/shard_map/all_gather | solution.py:193
  82.2 8.7 %shard_map.173 = (bf16[768,256]{1,0:T(8,128)(2,1)S(1)}, bf16[768,128]{1,0:T(8,128)(2,1)S(1)}, bf16[8,768,128]{2,1,0:T(8,128)(2,1)}) custom-call(bf16[16,768,256]{2,1,0:T(8,128)(2,1)} %bitcast.54, bf16[2048,512]{1,0:T(8,128)(2,1)} %get-tuple-element.47.fore_ref, bf16[2048,256]{1,0:T(8,128)(2,1)S(1)} %get-tuple-element.48.back_ref, ...), custom_call_target="tpu_custom_call" | custom-call | flops 3221225472 | bytes 16777216 | tf_op jit(solution)/shard_map/pallas_call | solution.py:211
  90.9 0.0 reduce-scatter.2.cloned.1.call-update
  90.9 0.0 copy-start
  90.9 0.0 copy-start.5
  90.9 0.0 copy-start.6
  90.9 7.8 %shard_map.174 = (bf16[2048,128]{1,0:T(8,128)(2,1)}, bf16[2048,128]{1,0:T(8,128)(2,1)}, bf16[128,2048]{1,0:T(8,128)(2,1)}) custom-call(bf16[16,768,256]{2,1,0:T(8,128)(2,1)} %bitcast.55, bf16[768,256]{1,0:T(8,128)(2,1)S(1)} %get-tuple-element.53.delta_ref, bf16[768,128]{1,0:T(8,128)(2,1)S(1)} %get-tuple-element.54.hidden_ref), custom_call_target="tpu_custom_call" | custom-call | flops 1207959552 | bytes 16777216 | tf_op jit(solution)/shard_map/pallas_call | solution.py:231
  98.8 0.0 copy-start.4
  98.8 34.2 %reduce-scatter.2.cloned.1.call-done = bf16[1,768,128]{2,1,0:T(8,128)(2,1)} async-done(((bf16[8,768,128]{2,1,0:T(8,128)(2,1)}), bf16[1,768,128]{2,1,0:T(8,128)(2,1)}) %reduce-scatter.2.cloned.1.call-update) | async-done | bytes 196624 | tf_op jit(solution)/shard_map/reduce_scatter | solution.py:229
  132.9 0.0 copy-start.7
  132.9 0.0 copy-start.8
  132.9 20.0 %all_to_all.16 = bf16[32,24,128]{2,1,0:T(8,128)(2,1)S(1)} all-to-all(bf16[32,24,128]{2,1,0:T(8,128)(2,1)} %bitcast.58), channel_id=1, replica_groups=mesh['sp'=32,'y'=8,'c'=2] {'sp'}, dimensions={0} | all-to-all | bytes 393216 | tf_op jit(solution)/shard_map/all_to_all | solution.py:249
  152.9 0.0 copy-done
  152.9 0.0 copy-done.5
  152.9 0.3 shard_map.175
  153.2 17.1 %all-gather.1 = bf16[2048,128]{1,0:T(8,128)(2,1)S(1)} all-gather(bf16[128,128]{1,0:T(8,128)(2,1)S(1)} %shard_map.175), channel_id=3, replica_groups=mesh['sp'=32,'y'=8,'c'=2] {'y','c'}, dimensions={0}, use_global_device_ids=true | all-gather | bytes 557056 | tf_op jit(solution)/shard_map/all_gather | solution.py:263
  170.2 0.0 copy-done.6
  170.2 0.0 copy-done.4
  170.2 0.9 conv_grad.1
  171.2 2.5 %collective-permute-start.4 = (f32[64,2]{1,0:T(8,128)S(1)}, f32[64,2]{1,0:T(8,128)S(1)}, u32[]{:S(2)}, u32[]{:S(2)}) collective-permute-start(f32[64,2]{1,0:T(8,128)S(1)} %bitcast.52), channel_id=1, source_target_pairs={{16,0},{32,16},{48,32},{64,48},{80,64},{96,80},{112,96},{128,112},... | collective-permute-start | bytes 1544 | tf_op jit(solution)/shard_map/ppermute | solution.py:287
  173.7 1.0 shard_map.176
  174.7 7.2 %all-to-all-start.2 = ((bf16[32,32,128]{2,1,0:T(8,128)(2,1)}), bf16[32,32,128]{2,1,0:T(8,128)(2,1)S(1)}, u32[]{:S(2)}, u32[]{:S(2)}) async-start(bf16[32,32,128]{2,1,0:T(8,128)(2,1)} %shard_map.176), calls=%async_computation.3 | async-start | bytes 524288 | tf_op jit(solution)/shard_map/all_to_all | solution.py:271
  181.9 0.0 collective-permute-done.4
  182.0 0.0 copy-done.7
  182.0 0.7 fusion.10
  182.7 0.0 copy-done.8
  182.7 0.6 fusion.9
  183.3 10.1 %all-to-all-done.2.tiles_ref = bf16[32,32,128]{2,1,0:T(8,128)(2,1)S(1)} async-done(((bf16[32,32,128]{2,1,0:T(8,128)(2,1)}), bf16[32,32,128]{2,1,0:T(8,128)(2,1)S(1)}, u32[]{:S(2)}, u32[]{:S(2)}) %all-to-all-start.2) | async-done | bytes 262176 | tf_op jit(solution)/shard_map/all_to_all | solution.py:271
  193.4 0.8 shard_map.177
  (3 shorter events, 0.0 us)
Async XLA Ops:
  7.2 75.1 %all-gather.4.cloned.1.call-start = ((), (), s32[]{:S(2)}) async-start(), calls=%async_computation.5 | async-start | bytes 6684672 | tf_op jit(solution)/shard_map/all_gather | solution.py:193
  36.8 96.2 %reduce-scatter.2.cloned.1.call-start = ((), (), s32[]{:S(2)}) async-start(), calls=%async_computation.4 | async-start | bytes 1769472 | tf_op jit(solution)/shard_map/reduce_scatter | solution.py:229
  37.5 13.7 %collective-permute-start.1 = (bf16[2048,128]{1,0:T(8,128)(2,1)}, bf16[2048,128]{1,0:T(8,128)(2,1)S(1)}, u32[]{:S(2)}, u32[]{:S(2)}) collective-permute-start(bf16[2048,128]{1,0:T(8,128)(2,1)} %bitcast.45), channel_id=1, source_target_pairs={{0,1},{1,0},{2,3},{3,2},{4,5},{5,4},{6,7},{7,6},{8,9},{9,8},{10,11... | collective-permute-start | bytes 1572872 | tf_op jit(solution)/shard_map/ppermute | solution.py:200
  39.4 11.8 %collective-permute-start.2 = (bf16[2048,128]{1,0:T(8,128)(2,1)}, bf16[2048,128]{1,0:T(8,128)(2,1)S(1)}, u32[]{:S(2)}, u32[]{:S(2)}) collective-permute-start(bf16[2048,128]{1,0:T(8,128)(2,1)} %bitcast.47), channel_id=1, source_target_pairs={{0,1},{1,0},{2,3},{3,2},{4,5},{5,4},{6,7},{7,6},{8,9},{9,8},{10,11... | collective-permute-start | bytes 1572872 | tf_op jit(solution)/shard_map/ppermute | solution.py:200
  41.8 9.4 %collective-permute-start.3 = (bf16[128,2048]{1,0:T(8,128)(2,1)}, bf16[128,2048]{1,0:T(8,128)(2,1)S(1)}, u32[]{:S(2)}, u32[]{:S(2)}) collective-permute-start(bf16[128,2048]{1,0:T(8,128)(2,1)} %bitcast.49), channel_id=1, source_target_pairs={{0,1},{1,0},{2,3},{3,2},{4,5},{5,4},{6,7},{7,6},{8,9},{9,8},{10,11... | collective-permute-start | bytes 1572872 | tf_op jit(solution)/shard_map/ppermute | solution.py:200
  44.6 5.8 %collective-permute-start = (f32[64,2]{1,0:T(8,128)S(1)}, f32[64,2]{1,0:T(8,128)S(1)}, u32[]{:S(2)}, u32[]{:S(2)}) collective-permute-start(f32[64,2]{1,0:T(8,128)S(1)} %slice.39), channel_id=1, source_target_pairs={{0,16},{16,32},{32,48},{48,64},{64,80},{80,96},{96,112},{112,128},... | collective-permute-start | bytes 1544 | tf_op jit(solution)/shard_map/ppermute | solution.py:203
  51.3 1.0 copy-start.1
  52.3 1.0 copy-start.2
  53.3 1.0 copy-start.3
  90.9 62.0 %copy-start = (bf16[128,2048]{1,0:T(8,128)(2,1)S(1)}, bf16[128,2048]{1,0:T(8,128)(2,1)}, u32[]{:S(2)}) copy-start(bf16[128,2048]{1,0:T(8,128)(2,1)} %cot_ref.3) | copy-start | bytes 1572868
  90.9 62.0 %copy-start.5 = (bf16[768,128]{1,0:T(8,128)(2,1)S(1)}, bf16[768,128]{1,0:T(8,128)(2,1)}, u32[]{:S(2)}) copy-start(bf16[768,128]{1,0:T(8,128)(2,1)} %get-tuple-element.62.select_ref) | copy-start | bytes 589828
  90.9 79.3 %copy-start.6 = (bf16[128,64]{0,1:T(8,128)(2,1)S(1)}, bf16[128,64]{0,1:T(8,128)(2,1)}, u32[]{:S(2)}) copy-start(bf16[128,64]{0,1:T(8,128)(2,1)} %param.19) | copy-start | bytes 49156
  98.8 71.5 %copy-start.4 = (bf16[2048,64]{0,1:T(8,128)(2,1)S(1)}, bf16[2048,64]{0,1:T(8,128)(2,1)}, u32[]{:S(2)}) copy-start(bf16[2048,64]{0,1:T(8,128)(2,1)} %param.23) | copy-start | bytes 786436
  132.9 49.0 %copy-start.7 = (bf16[128,64]{0,1:T(8,128)(2,1)S(1)}, bf16[128,64]{0,1:T(8,128)(2,1)}, u32[]{:S(2)}) copy-start(bf16[128,64]{0,1:T(8,128)(2,1)} %param.20) | copy-start | bytes 49156
  132.9 49.8 %copy-start.8 = (bf16[128,64]{0,1:T(8,128)(2,1)S(1)}, bf16[128,64]{0,1:T(8,128)(2,1)}, u32[]{:S(2)}) copy-start(bf16[128,64]{0,1:T(8,128)(2,1)} %param.21) | copy-start | bytes 49156
  171.2 10.8 %collective-permute-start.4 = (f32[64,2]{1,0:T(8,128)S(1)}, f32[64,2]{1,0:T(8,128)S(1)}, u32[]{:S(2)}, u32[]{:S(2)}) collective-permute-start(f32[64,2]{1,0:T(8,128)S(1)} %bitcast.52), channel_id=1, source_target_pairs={{16,0},{32,16},{48,32},{64,48},{80,64},{96,80},{112,96},{128,112},... | collective-permute-start | bytes 1544 | tf_op jit(solution)/shard_map/ppermute | solution.py:287
  174.7 18.7 %all-to-all-start.2 = ((bf16[32,32,128]{2,1,0:T(8,128)(2,1)}), bf16[32,32,128]{2,1,0:T(8,128)(2,1)S(1)}, u32[]{:S(2)}, u32[]{:S(2)}) async-start(bf16[32,32,128]{2,1,0:T(8,128)(2,1)} %shard_map.176), calls=%async_computation.3 | async-start | bytes 524288 | tf_op jit(solution)/shard_map/all_to_all | solution.py:271
Sparse Core Ops, SparseCore 0:
  36.9 45.2 all-gather.3
  91.0 41.8 reduce-scatter.1

commit v7 on v6

--- a/solution.py
+++ b/solution.py
@@ -173,9 +173,9 @@
     whole = lambda *dims: pl.BlockSpec(dims, lambda i, at: (0,) * len(dims))
     send, select = call(
         functools.partial(select_body, experts, capacity),
-        (shape((slots, 2 * LANES), BF16), shape((slots, LANES), BF16)),
+        (pltpu.VMEM((slots, 2 * LANES), BF16), pltpu.VMEM((slots, LANES), BF16)),
         (2 * slots * tokens * 2 * LANES, 2**20),
-        room=67_043_328,
+        room=60_000_000,
         grid_spec=pltpu.PrefetchScalarGridSpec(
             num_scalar_prefetch=1,
             grid=(1,),
@@ -193,7 +193,7 @@
     got = lax.all_gather(recv, TP)
     laid = call(
         layout_body,
-        (shape((width, 4 * units), BF16), shape((width, 2 * units), BF16), shape((ys // 2, 4 * units, 2 * LANES), BF16)),
+        (pltpu.HBM((width, 4 * units), BF16), pltpu.HBM((width, 2 * units), BF16), pltpu.HBM((ys // 2, 4 * units, 2 * LANES), BF16)),
         (2**22, 2**23),
         in_specs=[pl.BlockSpec(memory_space=pltpu.SMEM)] + [VMEM] * 6,
         out_specs=[VMEM] * 3,
@@ -212,6 +212,7 @@
         functools.partial(expert_body, tps),
         (shape((slots, 2 * units), BF16), shape((slots, units), BF16), shape((ys, slots, LANES), BF16)),
         (16 * slots * width * units, 2**24),
+        room=56 * 2**20,
         grid=(slots // rows,),
         in_specs=[
             pl.BlockSpec((tps, rows, 2 * LANES), lambda i: (0, i, 0)),

time: 203 us -> 202 us (level)
  waiting for transfers between devices: 71.5 us -> 74.5 us
  other arithmetic: 3.59 us -> 1.46 us
    all_gather x1, waiting for transfers between devices: 25.5 us -> 30.4 us  [per_device(): got = lax.all_gather(recv, TP)]
  transfers between devices with their start and end apart: 8 -> 8, of which waited for: 4 -> 4; matrix products, arithmetic and copies ran while one was open for 2% -> 1% of each run, Pallas kernels for 6% -> 6%
where the time goes in v7:
time: 202 us; the launch traced here: 201 us
  waiting for transfers between devices  74.5 us (37%)
  blocking collectives  64.2 us (32%)
  Pallas kernels  24 us (12%)
  starting transfers between devices  20.1 us (10%)
  between operations  14.3 us (7%)
  local copies, waits for them, and re-layouts  2.04 us (1%)
    reduce_scatter x1, waiting for transfers between devices, per_device(): half_sums = lax.psum_scatter(chip, 'y', scatter_dimension=0)  32.3 us
    all_gather x1, waiting for transfers between devices, per_device(): got = lax.all_gather(recv, TP)  30.4 us
    all_to_all x1, blocking collectives, per_device(): lax.all_to_all(send.reshape(groups, capacity, 2 * LANES), 'sp', split_axi...  27.3 us
    all_to_all x1, blocking collectives, per_device(): lax.all_to_all(half_sums.reshape(groups, capacity, LANES), 'sp', split_ax...  19.9 us
    all_gather x1, blocking collectives, per_device(): stream_all = lax.all_gather(stream_block, TP)  17 us
    all_to_all x1, waiting for transfers between devices, per_device(): lax.all_to_all(out_parts, 'sp', split_axis=0, concat_axis=0, tiled=True)  10.1 us
    pallas_call x1, Pallas kernels, per_device(): call(functools.partial(expert_body, tps), (shape((slots, 2 * units), BF16...  9.23 us
    pallas_call x1, Pallas kernels, per_device(): call(weight_body, (shape((width, units), BF16), shape((width, units), BF1...  7.81 us
  transfers between devices with their start and end apart: 8, of which 4 were waited for; matrix products, arithmetic and copies ran while one was open for 1% of the time, Pallas kernels for 6%

profile of v7, /device:TPU:6, one launch (start us, length us, event | category | flops | bytes accessed | tf_op | source)
XLA Modules:
  0.0 200.7 jit_solution(6751355265651973165)
XLA Ops:
  7.2 0.0 copy-start.8
  7.2 0.0 copy-start.3
  7.2 0.0 copy-start.2
  7.2 0.0 copy-start.1
  7.2 0.0 copy-start.10
  7.2 0.0 copy-start.9
  7.2 0.0 copy-start.7
  7.2 0.0 all-gather.4.cloned.1.call-start
  7.3 1.3 shard_map.171
  8.6 27.3 %all_to_all.15 = bf16[32,24,256]{2,1,0:T(8,128)(2,1)} all-to-all(bf16[32,24,256]{2,1,0:T(8,128)(2,1)S(1)} %bitcast.51), channel_id=1, replica_groups=mesh['sp'=32,'y'=8,'c'=2] {'sp'}, dimensions={0} | all-to-all | bytes 786432 | tf_op jit(solution)/shard_map/all_to_all | solution.py:186
  36.0 0.0 all-gather.4.cloned.1.call-update
  36.0 0.0 reduce-scatter.2.cloned.1.call-start
  36.0 0.0 copy-done.10
  36.1 0.0 copy-done.1
  36.1 1.9 collective-permute-start.1
  38.0 0.0 copy-done.2
  38.0 2.4 %collective-permute-start.2 = (bf16[2048,128]{1,0:T(8,128)(2,1)S(1)}, bf16[2048,128]{1,0:T(8,128)(2,1)S(1)}, u32[]{:S(2)}, u32[]{:S(2)}) collective-permute-start(bf16[2048,128]{1,0:T(8,128)(2,1)S(1)} %bitcast.47), channel_id=1, source_target_pairs={{0,1},{1,0},{2,3},{3,2},{4,5},{5,4},{6,7},{7,6},{8,9},{9,8},{10,11... | collective-permute-start | bytes 1572872 | tf_op jit(solution)/shard_map/ppermute | solution.py:200
  40.4 0.0 copy-done.3
  40.4 1.9 collective-permute-start.3
  42.4 0.0 copy-done.8
  42.4 0.0 copy-done.9
  42.4 0.1 slice.39
  42.5 4.1 %collective-permute-start = (f32[64,2]{1,0:T(8,128)S(1)}, f32[64,2]{1,0:T(8,128)S(1)}, u32[]{:S(2)}, u32[]{:S(2)}) collective-permute-start(f32[64,2]{1,0:T(8,128)S(1)} %slice.39), channel_id=1, source_target_pairs={{0,16},{16,32},{32,48},{48,64},{64,80},{80,96},{96,112},{112,128},... | collective-permute-start | bytes 1544 | tf_op jit(solution)/shard_map/ppermute | solution.py:203
  46.6 1.7 collective-permute-done
  48.3 0.0 copy-done.7
  48.3 0.1 multiply_convert_fusion
  48.4 0.0 collective-permute-done.1.gate2_ref
  48.4 0.0 collective-permute-done.2.up2_ref
  48.4 0.0 collective-permute-done.3.down2_ref
  48.4 2.6 %shard_map.172 = (bf16[2048,512]{1,0:T(8,128)(2,1)}, bf16[2048,256]{1,0:T(8,128)(2,1)}, bf16[4,512,256]{2,1,0:T(8,128)(2,1)}) custom-call(s32[1]{0:T(128)} %bitcast.16.core_ref, bf16[2048,128]{1,0:T(8,128)(2,1)S(1)} %bitcast.46, bf16[2048,128]{1,0:T(8,128)(2,1)S(1)} %bitcast.48, bf16[128,2048]{1,0:T(8,128)(2,1)S(1)} %bitcast.50, ...), custom_call_target="tpu_custom_call" | custom-call | flops 4194304 | bytes 8388608 | tf_op jit(solution)/shard_map/pallas_call | solution.py:194
  51.1 30.4 %all-gather.4.cloned.1.call-done = bf16[12288,256]{1,0:T(8,128)(2,1)} async-done(((bf16[768,256]{1,0:T(8,128)(2,1)}), bf16[12288,256]{1,0:T(8,128)(2,1)}) %all-gather.4.cloned.1.call-update) | async-done | bytes 6291472 | tf_op jit(solution)/shard_map/all_gather | solution.py:193
  81.5 9.2 %shard_map.173 = (bf16[768,256]{1,0:T(8,128)(2,1)}, bf16[768,128]{1,0:T(8,128)(2,1)}, bf16[8,768,128]{2,1,0:T(8,128)(2,1)}) custom-call(bf16[16,768,256]{2,1,0:T(8,128)(2,1)} %bitcast.55, bf16[2048,512]{1,0:T(8,128)(2,1)} %get-tuple-element.47.fore_ref, bf16[2048,256]{1,0:T(8,128)(2,1)} %get-tuple-element.48.back_ref, ...), custom_call_target="tpu_custom_call" | custom-call | flops 3221225472 | bytes 16777216 | tf_op jit(solution)/shard_map/pallas_call | solution.py:211
  90.7 0.0 reduce-scatter.2.cloned.1.call-update
  90.7 0.0 copy-start.4
  90.7 1.0 copy-done.4
  91.7 0.0 copy-start.6
  91.7 0.9 copy-done.6
  92.6 0.0 copy-start
  92.6 7.8 %shard_map.174 = (bf16[2048,128]{1,0:T(8,128)(2,1)}, bf16[2048,128]{1,0:T(8,128)(2,1)}, bf16[128,2048]{1,0:T(8,128)(2,1)}) custom-call(bf16[16,768,256]{2,1,0:T(8,128)(2,1)} %bitcast.56, bf16[768,256]{1,0:T(8,128)(2,1)S(1)} %copy-done.4, bf16[768,128]{1,0:T(8,128)(2,1)S(1)} %copy-done.6), custom_call_target="tpu_custom_call" | custom-call | flops 1207959552 | bytes 16777216 | tf_op jit(solution)/shard_map/pallas_call | solution.py:232
  100.5 0.0 copy-start.5
  100.5 32.3 %reduce-scatter.2.cloned.1.call-done = bf16[1,768,128]{2,1,0:T(8,128)(2,1)} async-done(((bf16[8,768,128]{2,1,0:T(8,128)(2,1)}), bf16[1,768,128]{2,1,0:T(8,128)(2,1)}) %reduce-scatter.2.cloned.1.call-update) | async-done | bytes 196624 | tf_op jit(solution)/shard_map/reduce_scatter | solution.py:230
  132.7 19.9 %all_to_all.16 = bf16[32,24,128]{2,1,0:T(8,128)(2,1)S(1)} all-to-all(bf16[32,24,128]{2,1,0:T(8,128)(2,1)} %bitcast.58), channel_id=1, replica_groups=mesh['sp'=32,'y'=8,'c'=2] {'sp'}, dimensions={0} | all-to-all | bytes 393216 | tf_op jit(solution)/shard_map/all_to_all | solution.py:250
  152.6 0.0 copy-done
  152.6 0.3 shard_map.175
  152.9 17.0 %all-gather.1 = bf16[2048,128]{1,0:T(8,128)(2,1)S(1)} all-gather(bf16[128,128]{1,0:T(8,128)(2,1)S(1)} %shard_map.175), channel_id=3, replica_groups=mesh['sp'=32,'y'=8,'c'=2] {'y','c'}, dimensions={0}, use_global_device_ids=true | all-gather | bytes 557056 | tf_op jit(solution)/shard_map/all_gather | solution.py:264
  169.9 0.0 copy-done.5
  169.9 0.9 conv_grad.1
  170.8 2.5 %collective-permute-start.4 = (f32[64,2]{1,0:T(8,128)S(1)}, f32[64,2]{1,0:T(8,128)S(1)}, u32[]{:S(2)}, u32[]{:S(2)}) collective-permute-start(f32[64,2]{1,0:T(8,128)S(1)} %bitcast.53), channel_id=1, source_target_pairs={{16,0},{32,16},{48,32},{64,48},{80,64},{96,80},{112,96},{128,112},... | collective-permute-start | bytes 1544 | tf_op jit(solution)/shard_map/ppermute | solution.py:288
  173.3 1.0 shard_map.176
  174.3 7.3 %all-to-all-start.2 = ((bf16[32,32,128]{2,1,0:T(8,128)(2,1)}), bf16[32,32,128]{2,1,0:T(8,128)(2,1)S(1)}, u32[]{:S(2)}, u32[]{:S(2)}) async-start(bf16[32,32,128]{2,1,0:T(8,128)(2,1)} %shard_map.176), calls=%async_computation.3 | async-start | bytes 524288 | tf_op jit(solution)/shard_map/all_to_all | solution.py:272
  181.6 0.0 collective-permute-done.4
  181.6 0.7 fusion.10
  182.3 0.6 fusion.9
  182.9 10.1 %all-to-all-done.2.tiles_ref = bf16[32,32,128]{2,1,0:T(8,128)(2,1)S(1)} async-done(((bf16[32,32,128]{2,1,0:T(8,128)(2,1)}), bf16[32,32,128]{2,1,0:T(8,128)(2,1)S(1)}, u32[]{:S(2)}, u32[]{:S(2)}) %all-to-all-start.2) | async-done | bytes 262176 | tf_op jit(solution)/shard_map/all_to_all | solution.py:272
  193.0 0.8 shard_map.177
  (5 shorter events, 0.0 us)
Async XLA Ops:
  7.2 35.2 %copy-start.8 = (bf16[128,64]{0,1:T(8,128)(2,1)S(1)}, bf16[128,64]{0,1:T(8,128)(2,1)}, u32[]{:S(2)}) copy-start(bf16[128,64]{0,1:T(8,128)(2,1)} %param.20) | copy-start | bytes 49156
  7.2 33.3 %copy-start.3 = (bf16[1,128,2048]{2,1,0:T(8,128)(2,1)S(1)}, bf16[1,128,2048]{2,1,0:T(8,128)(2,1)}, u32[]{:S(2)}) copy-start(bf16[1,128,2048]{2,1,0:T(8,128)(2,1)} %param.18) | copy-start | bytes 1572868
  7.2 30.8 %copy-start.2 = (bf16[1,2048,128]{2,1,0:T(8,128)(2,1)S(1)}, bf16[1,2048,128]{2,1,0:T(8,128)(2,1)}, u32[]{:S(2)}) copy-start(bf16[1,2048,128]{2,1,0:T(8,128)(2,1)} %param.17) | copy-start | bytes 1572868
  7.2 28.9 %copy-start.1 = (bf16[1,2048,128]{2,1,0:T(8,128)(2,1)S(1)}, bf16[1,2048,128]{2,1,0:T(8,128)(2,1)}, u32[]{:S(2)}) copy-start(bf16[1,2048,128]{2,1,0:T(8,128)(2,1)} %param.16) | copy-start | bytes 1572868
  7.2 28.8 %copy-start.10 = (bf16[3,64]{1,0:T(4,128)(2,1)S(1)}, bf16[3,64]{1,0:T(4,128)(2,1)}, u32[]{:S(2)}) copy-start(bf16[3,64]{1,0:T(4,128)(2,1)} %param.22) | copy-start | bytes 1156
  7.2 35.2 %copy-start.9 = (bf16[128,64]{0,1:T(8,128)(2,1)S(1)}, bf16[128,64]{0,1:T(8,128)(2,1)}, u32[]{:S(2)}) copy-start(bf16[128,64]{0,1:T(8,128)(2,1)} %param.21) | copy-start | bytes 49156
  7.2 41.1 %copy-start.7 = (bf16[128,64]{0,1:T(8,128)(2,1)S(1)}, bf16[128,64]{0,1:T(8,128)(2,1)}, u32[]{:S(2)}) copy-start(bf16[128,64]{0,1:T(8,128)(2,1)} %param.19) | copy-start | bytes 49156
  7.2 74.2 %all-gather.4.cloned.1.call-start = ((), (), s32[]{:S(2)}) async-start(), calls=%async_computation.5 | async-start | bytes 6684672 | tf_op jit(solution)/shard_map/all_gather | solution.py:193
  36.0 96.7 %reduce-scatter.2.cloned.1.call-start = ((), (), s32[]{:S(2)}) async-start(), calls=%async_computation.4 | async-start | bytes 1769472 | tf_op jit(solution)/shard_map/reduce_scatter | solution.py:230
  36.1 12.3 %collective-permute-start.1 = (bf16[2048,128]{1,0:T(8,128)(2,1)S(1)}, bf16[2048,128]{1,0:T(8,128)(2,1)S(1)}, u32[]{:S(2)}, u32[]{:S(2)}) collective-permute-start(bf16[2048,128]{1,0:T(8,128)(2,1)S(1)} %bitcast.45), channel_id=1, source_target_pairs={{0,1},{1,0},{2,3},{3,2},{4,5},{5,4},{6,7},{7,6},{8,9},{9,8},{10,11... | collective-permute-start | bytes 1572872 | tf_op jit(solution)/shard_map/ppermute | solution.py:200
  38.0 10.4 %collective-permute-start.2 = (bf16[2048,128]{1,0:T(8,128)(2,1)S(1)}, bf16[2048,128]{1,0:T(8,128)(2,1)S(1)}, u32[]{:S(2)}, u32[]{:S(2)}) collective-permute-start(bf16[2048,128]{1,0:T(8,128)(2,1)S(1)} %bitcast.47), channel_id=1, source_target_pairs={{0,1},{1,0},{2,3},{3,2},{4,5},{5,4},{6,7},{7,6},{8,9},{9,8},{10,11... | collective-permute-start | bytes 1572872 | tf_op jit(solution)/shard_map/ppermute | solution.py:200
  40.4 8.0 %collective-permute-start.3 = (bf16[128,2048]{1,0:T(8,128)(2,1)S(1)}, bf16[128,2048]{1,0:T(8,128)(2,1)S(1)}, u32[]{:S(2)}, u32[]{:S(2)}) collective-permute-start(bf16[128,2048]{1,0:T(8,128)(2,1)S(1)} %bitcast.49), channel_id=1, source_target_pairs={{0,1},{1,0},{2,3},{3,2},{4,5},{5,4},{6,7},{7,6},{8,9},{9,8},{10,11... | collective-permute-start | bytes 1572872 | tf_op jit(solution)/shard_map/ppermute | solution.py:200
  42.5 5.8 %collective-permute-start = (f32[64,2]{1,0:T(8,128)S(1)}, f32[64,2]{1,0:T(8,128)S(1)}, u32[]{:S(2)}, u32[]{:S(2)}) collective-permute-start(f32[64,2]{1,0:T(8,128)S(1)} %slice.39), channel_id=1, source_target_pairs={{0,16},{16,32},{32,48},{48,64},{64,80},{80,96},{96,112},{112,128},... | collective-permute-start | bytes 1544 | tf_op jit(solution)/shard_map/ppermute | solution.py:203
  90.7 1.0 copy-start.4
  91.7 0.9 copy-start.6
  92.6 59.9 %copy-start = (bf16[128,2048]{1,0:T(8,128)(2,1)S(1)}, bf16[128,2048]{1,0:T(8,128)(2,1)}, u32[]{:S(2)}) copy-start(bf16[128,2048]{1,0:T(8,128)(2,1)} %cot_ref.3) | copy-start | bytes 1572868
  100.5 69.4 %copy-start.5 = (bf16[2048,64]{0,1:T(8,128)(2,1)S(1)}, bf16[2048,64]{0,1:T(8,128)(2,1)}, u32[]{:S(2)}) copy-start(bf16[2048,64]{0,1:T(8,128)(2,1)} %param.23) | copy-start | bytes 786436
  170.8 10.8 %collective-permute-start.4 = (f32[64,2]{1,0:T(8,128)S(1)}, f32[64,2]{1,0:T(8,128)S(1)}, u32[]{:S(2)}, u32[]{:S(2)}) collective-permute-start(f32[64,2]{1,0:T(8,128)S(1)} %bitcast.53), channel_id=1, source_target_pairs={{16,0},{32,16},{48,32},{64,48},{80,64},{96,80},{112,96},{128,112},... | collective-permute-start | bytes 1544 | tf_op jit(solution)/shard_map/ppermute | solution.py:288
  174.3 18.7 %all-to-all-start.2 = ((bf16[32,32,128]{2,1,0:T(8,128)(2,1)}), bf16[32,32,128]{2,1,0:T(8,128)(2,1)S(1)}, u32[]{:S(2)}, u32[]{:S(2)}) async-start(bf16[32,32,128]{2,1,0:T(8,128)(2,1)} %shard_map.176), calls=%async_computation.3 | async-start | bytes 524288 | tf_op jit(solution)/shard_map/all_to_all | solution.py:272
Sparse Core Ops, SparseCore 0:
  36.1 45.2 all-gather.3
  90.8 41.8 reduce-scatter.1
